TPU v7x, 128 devices: a whole 4x4x4 slice. The times are simulated.
128 devices in a mesh: rep: 2 (over x_hi), fs: 4 (over x_lo, core), tp: 16 (over z, y).
Axes of the slice: x: 4 (x_hi: 2, x_lo: 2; x = x_hi * 2 + x_lo), y: 4, z: 4, core: 2. Of those that a mesh axis runs over, the one named last changes fastest.
Arguments:
- inputs: bfloat16 [4096, 4096], P(('rep', 'fs', 'tp')), may hold values from -6 to 6
- w_gate: bfloat16 [4096, 11008], P('fs', 'tp'), may hold values from -0.09375 to 0.09375
- w_up: bfloat16 [4096, 11008], P('fs', 'tp'), may hold values from -0.09375 to 0.09375
- w_down: bfloat16 [11008, 4096], P('tp', 'fs'), may hold values from -0.0546875 to 0.0546875
- d_out: bfloat16 [4096, 4096], P(('rep', 'fs', 'tp')), may hold values from -24 to 24
Outputs:
- grad_inputs: bfloat16 [4096, 4096], P(('rep', 'fs', 'tp'))
- grad_gate: float32 [4096, 11008], P('fs', 'tp')
- grad_up: float32 [4096, 11008], P('fs', 'tp')
- grad_down: float32 [11008, 4096], P('tp', 'fs')
All inputs are finite; a program needn't handle non-finite values.
Results may differ from a plain program's by a relative error of at most 0.00185.
Values may be sent and summed in bfloat16 or wider, within the bound.
No kernel may reach another device: no remote copies, remote signals or barrier semaphores. Data moves between devices by JAX's collectives and lax.ppermute only.
A program may use at most 192 MiB of HBM per device.

v0:
```python
import functools

import jax
import jax.numpy as jnp
from jax import lax
from jax.experimental import pallas as pl
from jax.experimental.pallas import tpu as pltpu
from jax.sharding import PartitionSpec as P


AXES = ("rep", "fs", "tp")
BF, F32, F16 = jnp.bfloat16, jnp.float32, jnp.float16
W_MAX = 0.09375
ANY = pl.BlockSpec(memory_space=pl.ANY)
VMEM = pl.BlockSpec(memory_space=pltpu.VMEM)
LIMIT = 56 * 1024 * 1024

ROWS, DEPTH, UNITS = 32, 1024, 688
TOK, WIDE = 16 * ROWS, 4 * DEPTH
CUT = 336
LOW, HIGH = 1040, 1024
TAIL = 128


def index_of(x, c, z, y):
    x, z, y = x % 4, z % 4, y % 4
    return (x // 2) * 64 + ((x % 2) * 2 + c) * 16 + z * 4 + y


def moved(array, dx=0, flip=0, dz=0, dy=0):
    pairs = []
    for x in range(4):
        for c in range(2):
            for z in range(4):
                for y in range(4):
                    pairs.append((index_of(x + dx, c ^ flip, z + dz, y + dy), index_of(x, c, z, y)))
    return lax.ppermute(array, AXES, pairs)


def dot(a, b, ca, cb):
    return lax.dot_general(a, b, (((ca,), (cb,)), ((), ())), preferred_element_type=F32)


def place():
    tp = lax.axis_index("tp")
    return tp // 4, tp % 4


def call(body, out_shape, scratch, flops, ins, outs, args, nbytes):
    return pl.pallas_call(
        body,
        out_shape=out_shape,
        in_specs=ins,
        out_specs=outs,
        scratch_shapes=scratch,
        compiler_params=pltpu.CompilerParams(vmem_limit_bytes=LIMIT),
        cost_estimate=pl.CostEstimate(flops=flops, bytes_accessed=nbytes, transcendentals=0),
    )(*args)


FROM = ((0, 0, 4, 0), (1, 0, 4, 1), (2, 0, 4, 3), (3, 0, 2, 2), (4, 2, 2, 2))
WHOLE = ((0, 0, 4, 0), (1, 0, 4, 1), (2, 0, 4, 3), (3, 0, 4, 2))


def forward_kernel(*refs):
    xs, ds, was, wbs = refs[:5], refs[5:10], refs[10:14], refs[14:18]
    acts_l, acts_h, side, x_own, d_own = refs[18:23]
    v, w, sums, act, sx, sd, sw, so = refs[23:]
    z, y = place()
    x_copies, d_copies = [], []
    for i, first, count, off in FROM:
        for j in range(count):
            row = pl.multiple_of((lax.rem(z + first + j, 4) * 4 + lax.rem(y + off, 4)) * ROWS, ROWS)
            x_copies.append(
                pltpu.make_async_copy(xs[i].at[j], v.at[0, pl.ds(row, ROWS)], sx.at[len(x_copies)]))
            row = pl.multiple_of((lax.rem(z + off, 4) * 4 + lax.rem(y + first + j, 4)) * ROWS, ROWS)
            d_copies.append(
                pltpu.make_async_copy(ds[i].at[j], v.at[1, pl.ds(row, ROWS)], sd.at[len(d_copies)]))
    rest = UNITS - CUT
    w_copies = [
        [
            pltpu.make_async_copy(was[k].at[pl.ds(0, UNITS)], w.at[k, 0], sw.at[4 * k]),
            pltpu.make_async_copy(wbs[k].at[pl.ds(0, UNITS)], w.at[k, 1], sw.at[4 * k + 1]),
            pltpu.make_async_copy(was[k].at[pl.ds(UNITS, CUT)], w.at[k, 2, pl.ds(0, CUT)], sw.at[4 * k + 2]),
            pltpu.make_async_copy(wbs[k].at[pl.ds(UNITS, rest)], w.at[k, 2, pl.ds(CUT, rest)], sw.at[4 * k + 3]),
        ]
        for k in range(4)
    ]
    stages = [x_copies + w_copies[0][:2], d_copies + w_copies[0][2:], w_copies[1], w_copies[2], w_copies[3]]

    def begin(n):
        for c in stages[n]:
            c.start()

    def end(n):
        for c in stages[n]:
            c.wait()

    begin(0)
    begin(1)
    end(0)
    begin(2)

    def initial(i, _):
        @pl.when(i == 2)
        def _():
            end(1)
            begin(3)

        sums[i] = dot(w[0, i], v[i // 2, :, :DEPTH], 1, 1)
        return 0

    lax.fori_loop(0, 3, initial, 0)
    end(2)
    begin(4)
    outs = []
    for i, to in enumerate((x_own, d_own)):
        outs.append(pltpu.make_async_copy(v.at[i, :, pl.ds(0, DEPTH)], to, so.at[i]))
        for h in range(2):
            outs.append(pltpu.make_async_copy(
                v.at[i, :, pl.ds(DEPTH + h * TOK, TOK)],
                side.at[pl.ds(3 * UNITS + (2 * i + h) * TOK, TOK)], so.at[2 + 2 * i + h]))
    for k in (1, 2, 3):
        if k > 1:
            end(k + 1)
        if k == 3:
            for c in outs:
                c.start()

        def product(i, _):
            sums[i] = sums[i] + dot(w[k, i], v[i // 2, :, k * DEPTH:(k + 1) * DEPTH], 1, 1)
            return 0

        lax.fori_loop(0, 3, product, 0)

    def unit(i, _):
        r = pl.ds(pl.multiple_of(i * 16, 16), 16)
        g = sums[0, r, :].astype(BF).astype(F32)
        u = sums[1, r, :].astype(BF).astype(F32)
        b = sums[2, r, :].astype(BF).astype(F32)
        sigma = 1.0 / (1.0 + jnp.exp(-g))
        active = g * sigma
        act[r, :] = (b * u * sigma * (1.0 + g * (1.0 - sigma))).astype(BF)
        act[pl.ds(pl.multiple_of(UNITS + i * 16, 16), 16), :] = (b * active).astype(BF)
        act[pl.ds(pl.multiple_of(2 * UNITS + i * 16, 16), 16), :] = (active * u).astype(BF)
        return 0

    lax.fori_loop(0, UNITS // 16, unit, 0)
    outs.append(pltpu.make_async_copy(act.at[pl.ds(0, LOW)], acts_l, so.at[6]))
    outs.append(pltpu.make_async_copy(act.at[pl.ds(LOW, HIGH)], acts_h, so.at[7]))
    outs.append(pltpu.make_async_copy(act, side.at[pl.ds(0, 3 * UNITS)], so.at[8]))
    for c in outs[-3:]:
        c.start()
    for c in outs:
        c.wait()


def forward(xs, ds, was, wbs):
    shape = jax.ShapeDtypeStruct
    return call(
        forward_kernel,
        (shape((LOW, TOK), BF), shape((HIGH, TOK), BF), shape((3 * UNITS + 4 * TOK, TOK), BF),
         shape((TOK, DEPTH), BF), shape((TOK, DEPTH), BF)),
        [
            pltpu.VMEM((2, TOK, WIDE), BF), pltpu.VMEM((4, 3, UNITS, DEPTH), BF), pltpu.VMEM((3, UNITS, TOK), F32),
            pltpu.VMEM((3 * UNITS, TOK), BF),
            pltpu.SemaphoreType.DMA((16,)), pltpu.SemaphoreType.DMA((16,)),
            pltpu.SemaphoreType.DMA((16,)), pltpu.SemaphoreType.DMA((9,)),
        ],
        2 * TOK * WIDE * UNITS * 3,
        [ANY] * 18,
        (ANY,) * 5,
        (*xs, *ds, *was, *wbs),
        34 << 20,
    )


def input_kernel(*refs):
    acts, was, wbs, out = refs[0], refs[1:5], refs[5:9], refs[9]
    act, wa, wb, tg, tu, total, expo, sw, so = refs[10:]
    load = pltpu.make_async_copy(acts.at[pl.ds(0, 2 * UNITS)], act, so.at[5])
    load.start()
    copies = [
        (pltpu.make_async_copy(was[k].at[pl.ds(0, UNITS)], wa.at[k], sw.at[2 * k]),
         pltpu.make_async_copy(wbs[k].at[pl.ds(0, UNITS)], wb.at[k], sw.at[2 * k + 1]))
        for k in range(4)
    ]
    for pair in copies[:2]:
        for c in pair:
            c.start()
    load.wait()
    tg[...] = act[:UNITS, :].T
    tu[...] = act[UNITS:, :].T
    norm = jnp.sum(jnp.abs(tg[...].astype(F32)), axis=1, keepdims=True)
    norm = norm + jnp.sum(jnp.abs(tu[...].astype(F32)), axis=1, keepdims=True)
    e = jnp.ceil(jnp.log2(jnp.maximum(norm * (1.02 * W_MAX), 1e-30)))
    expo[...] = jnp.broadcast_to(e, (TOK, TAIL))
    puts = [pltpu.make_async_copy(expo, out.at[:, pl.ds(WIDE, TAIL)], so.at[4])]
    puts[0].start()
    for k in range(4):
        for c in copies[k]:
            c.wait()
        if k + 2 < 4:
            for c in copies[k + 2]:
                c.start()
        if k >= 2:
            puts[k - 1].wait()

        def tile(j, _):
            n = pl.ds(pl.multiple_of(j * 512, 512), 512)
            v = dot(tg[...], wa[k, :, n], 1, 0) + dot(tu[...], wb[k, :, n], 1, 0)
            total[k % 2, :, n] = v * jnp.exp2(14.0 - expo[:, :1])
            return 0

        lax.fori_loop(0, 2, tile, 0)
        puts.append(pltpu.make_async_copy(total.at[k % 2], out.at[:, pl.ds(k * DEPTH, DEPTH)], so.at[k]))
        puts[-1].start()
    for c in (puts[0], puts[3], puts[4]):
        c.wait()


def input_sums(acts, was, wbs):
    return call(
        input_kernel,
        jax.ShapeDtypeStruct((TOK, WIDE + TAIL), F32),
        [
            pltpu.VMEM((2 * UNITS, TOK), BF),
            pltpu.VMEM((4, UNITS, DEPTH), BF), pltpu.VMEM((4, UNITS, DEPTH), BF),
            pltpu.VMEM((TOK, UNITS), BF), pltpu.VMEM((TOK, UNITS), BF),
            pltpu.VMEM((2, TOK, DEPTH), F32), pltpu.VMEM((TOK, TAIL), F32),
            pltpu.SemaphoreType.DMA((8,)), pltpu.SemaphoreType.DMA((6,)),
        ],
        2 * TOK * WIDE * UNITS * 2,
        [ANY] * 9,
        ANY,
        (acts, *was, *wbs),
        22 << 20,
    )


def sum_kernel(got, out):
    v = None
    for i in range(16):
        w = got[i, :, :WIDE] * jnp.exp2(got[i, :, WIDE:WIDE + 1] - 14.0)
        v = w if v is None else v + w
    out[...] = v


def summed(got):
    return pl.pallas_call(
        sum_kernel,
        grid=(ROWS // 8,),
        out_shape=jax.ShapeDtypeStruct((ROWS, WIDE), F32),
        in_specs=[pl.BlockSpec((16, 8, WIDE + TAIL), lambda i: (0, i, 0))],
        out_specs=pl.BlockSpec((8, WIDE), lambda i: (i, 0)),
        compiler_params=pltpu.CompilerParams(vmem_limit_bytes=LIMIT),
        cost_estimate=pl.CostEstimate(flops=1 << 28, bytes_accessed=9 << 20, transcendentals=0),
    )(got)


def weight_kernel(acts, n_acts, columns, has_base, n_in, *refs):
    ins, outs = refs[:n_in], refs[n_in:n_in + 3]
    a, xc, dc, total, sa, sc, sb, so = refs[n_in + 3:]
    z, y = place()
    stages = [[], [], []]
    n = 0
    for g, pieces in enumerate(acts):
        for i, r0, r1 in pieces:
            for s in range(3):
                lo, hi = max(r0, s * UNITS), min(r1, (s + 1) * UNITS)
                if lo < hi:
                    stages[s].append(pltpu.make_async_copy(
                        ins[i].at[pl.ds(lo - r0, hi - lo)], a.at[pl.ds(lo, hi - lo), pl.ds(g * TOK, TOK)], sa.at[n]))
                    n += 1
    columns(ins[n_acts:], z, y, lambda src, to: stages[0].append(
        pltpu.make_async_copy(src, to, sc.at[0, len(stages[0])])), xc, 0)
    columns(ins[n_acts:], z, y, lambda src, to: stages[2].append(
        pltpu.make_async_copy(src, to, sc.at[1, len(stages[2])])), dc, 1)
    if has_base:
        for s in range(3):
            stages[s].append(pltpu.make_async_copy(ins[n_in - 3 + s], total.at[s], sb.at[s]))

    def begin(s):
        for c in stages[s]:
            c.start()

    begin(0)
    begin(1)
    done = [pltpu.make_async_copy(total.at[i], outs[i], so.at[i]) for i in range(3)]

    def product(i, cols):
        v = dot(a[pl.ds(pl.multiple_of(i * UNITS, 16), UNITS), :], cols[...].reshape(len(acts) * TOK, DEPTH), 1, 0)
        total[i] = total[i] + v if has_base else v

    def pair(i, _):
        @pl.when(i == 0)
        def _():
            for c in stages[0]:
                c.wait()
            begin(2)

        @pl.when(i == 1)
        def _():
            done[0].start()
            for c in stages[1]:
                c.wait()

        product(i, xc)
        return 0

    lax.fori_loop(0, 2, pair, 0)
    done[1].start()
    for c in stages[2]:
        c.wait()
    product(2, dc)
    done[2].start()
    for c in done:
        c.wait()


def near_columns(refs, z, y, add, buf, kind):
    x_own, d_own, side = refs[:3]
    add(d_own if kind else x_own, buf.at[0])
    for h in range(2):
        add(side.at[pl.ds(3 * UNITS + (2 * kind + h) * TOK, TOK)], buf.at[1, :, pl.ds(h * TOK, TOK)])


def plane_columns(first_group, count, refs, z, y, add, buf, kind):
    for i, first, n, off in WHOLE:
        for j in range(n):
            a, b = lax.rem(z + first + j, 4), lax.rem(y + off, 4)
            if kind:
                a, b = lax.rem(z + off, 4), lax.rem(y + first + j, 4)
            add(refs[4 * kind + i].at[j, pl.ds(first_group, count)], buf.at[:, a * 4 + b])


def weight_sums(groups, columns, arrays, base):
    ins, acts = [], []
    for pieces in groups:
        row, marks = 0, []
        for p, m in pieces:
            marks.append((len(ins), row, row + m))
            ins.append(p)
            row += m
        acts.append(marks)
    n_acts = len(ins)
    ins += list(arrays) + list(base or [])
    n = len(groups)
    col = (n, TOK, DEPTH) if columns is near_columns else (n, 16, ROWS, DEPTH)
    out = jax.ShapeDtypeStruct((UNITS, DEPTH), F32)
    return call(
        functools.partial(weight_kernel, acts, n_acts, columns, base is not None, len(ins)),
        (out,) * 3,
        [
            pltpu.VMEM((3 * UNITS, n * TOK), BF), pltpu.VMEM(col, BF), pltpu.VMEM(col, BF),
            pltpu.VMEM((3, UNITS, DEPTH), F32),
            pltpu.SemaphoreType.DMA((3 * n_acts,)), pltpu.SemaphoreType.DMA((2, 32)),
            pltpu.SemaphoreType.DMA((3,)), pltpu.SemaphoreType.DMA((3,)),
        ],
        2 * 3 * UNITS * DEPTH * n * TOK,
        [ANY] * len(ins),
        (ANY,) * 3,
        ins,
        n * (4 << 20) + (16 << 20),
    )


def block(inputs, w_gate, w_up, w_down, d_out):
    fs = lax.axis_index("fs")

    def relative(v):
        parts = [v[:, i * DEPTH:(i + 1) * DEPTH] for i in range(4)]
        out = []
        for k in range(4):
            w = parts[k]
            for f in range(1, 4):
                w = jnp.where(fs == f, parts[f ^ k], w)
            out.append(w)
        return out

    xp, dp = relative(inputs), relative(d_out)
    x_own, d_own = jnp.concatenate(xp, axis=1), jnp.concatenate(dp, axis=1)

    def spread(own, first, second, forward):
        line = jnp.concatenate(
            [own[None]] + [moved(own[None], **{first: d}) for d in (1, 2, 3)], axis=0)
        up, down = moved(line, **{second: 1}), moved(line, **{second: -1})
        if not forward:
            return line, up, down, moved(line, **{second: 2})
        low, high = up[:2], down[2:]
        return line, up, down, moved(low, **{second: 1}), moved(high, **{second: -1})

    xs = spread(x_own, "dz", "dy", True)
    ds = spread(d_own, "dy", "dz", True)

    side = moved(jnp.stack([xp[1], dp[1], xp[3], dp[3]]), flip=1)
    far = jnp.stack([xp[0], side[0], dp[0], side[1]])
    near = jnp.stack([xp[2], side[2], dp[2], side[3]])
    got = (moved(near, dx=1), moved(near, dx=-1), moved(far, dx=2))
    xcs = spread(jnp.concatenate([v[:2] for v in got], axis=0), "dz", "dy", False)
    dcs = spread(jnp.concatenate([v[2:] for v in got], axis=0), "dy", "dz", False)

    wa = jnp.concatenate([w_gate.T, w_down[:CUT]], axis=0)
    wb = jnp.concatenate([w_up.T, w_down[CUT:]], axis=0)
    wa2, wb2 = moved(wa, dx=1), moved(wb, dx=-1)
    wa1, wb1 = moved(wa, flip=1), moved(wb, flip=1)
    wa3, wb3 = moved(wa2, flip=1), moved(wb2, flip=1)
    was, wbs = (wa, wa1, wa2, wa3), (wb, wb1, wb2, wb3)

    acts_l, acts_h, own, x_cols, d_cols = forward(xs, ds, was, wbs)

    aml, aph = moved(acts_l, dx=1), moved(acts_h, dx=-1)
    amh, apl = moved(acts_h, dx=1), moved(acts_l, dx=-1)
    side = moved(own, flip=1)
    oa, ob = moved(aml, dx=1), moved(aph, dx=-1)
    sml, sph = moved(aml, flip=1), moved(aph, flip=1)
    smh, spl = moved(amh, flip=1), moved(apl, flip=1)
    soa, sob = moved(oa, flip=1), moved(ob, flip=1)

    packed = input_sums(own, was, wbs).astype(F16)
    got = lax.all_to_all(packed.reshape(16, ROWS, WIDE + TAIL), "tp", 0, 0)
    grad_inputs = jnp.concatenate(relative(summed(got.astype(F32)).astype(BF)), axis=1)

    full = 3 * UNITS

    def halves(low, high):
        return [(low, LOW), (high, HIGH)]

    sums = weight_sums(
        [[(own, full)], [(side, full)]], near_columns, (x_cols, d_cols, side), None)
    sums = weight_sums(
        [halves(aml, amh), halves(sml, smh), halves(apl, aph), halves(spl, sph)],
        functools.partial(plane_columns, 0, 4), (*xcs, *dcs), sums)
    sums = weight_sums(
        [halves(oa, ob), halves(soa, sob)], functools.partial(plane_columns, 4, 2), (*xcs, *dcs), sums)
    return grad_inputs, sums[0].T, sums[1].T, sums[2]


def solution(mesh):
    tok = P(AXES, None)
    return jax.shard_map(
        block,
        mesh=mesh,
        in_specs=(tok, P("fs", "tp"), P("fs", "tp"), P("tp", "fs"), tok),
        out_specs=(tok, P("fs", "tp"), P("fs", "tp"), P("tp", "fs")),
        check_vma=False,
    )
```

profile of v0, /device:TPU:1, one launch (start us, length us, event | category | flops | bytes accessed | tf_op | source)
XLA Modules:
  0.0 390.5 jit_solution(3154320016386323274)
XLA Ops:
  22.2 4.8 %collective-permute-done.29 = bf16[4,32,1024]{2,1,0:T(8,128)(2,1)S(1)} collective-permute-done((bf16[4,32,1024]{2,1,0:T(8,128)(2,1)S(1)}, bf16[4,32,1024]{2,1,0:T(8,128)(2,1)S(1)}, u32[]{:S(2)}, u32[]{:S(2)}) %collective-permute-start.29) | collective-permute-done | bytes 262176 | tf_op jit(solution)/shard_map/ppermute | solution.py:37
  29.5 4.6 %collective-permute-done.28 = bf16[4,32,1024]{2,1,0:T(8,128)(2,1)S(1)} collective-permute-done((bf16[4,32,1024]{2,1,0:T(8,128)(2,1)S(1)}, bf16[4,32,1024]{2,1,0:T(8,128)(2,1)S(1)}, u32[]{:S(2)}, u32[]{:S(2)}) %collective-permute-start.28) | collective-permute-done | bytes 262176 | tf_op jit(solution)/shard_map/ppermute | solution.py:37
  38.3 19.7 %collective-permute-done.32 = bf16[1,6,32,1024]{3,2,1,0:T(8,128)(2,1)S(1)} collective-permute-done((bf16[1,6,32,1024]{3,2,1,0:T(8,128)(2,1)S(1)}, bf16[1,6,32,1024]{3,2,1,0:T(8,128)(2,1)S(1)}, u32[]{:S(2)}, u32[]{:S(2)}) %collective-permute-start.32) | collective-permute-done | bytes 393248 | tf_op jit(solution)/shard_map/ppermute | solution.py:37
  58.2 9.2 %collective-permute-done.30 = bf16[1,6,32,1024]{3,2,1,0:T(8,128)(2,1)S(1)} collective-permute-done((bf16[1,6,32,1024]{3,2,1,0:T(8,128)(2,1)S(1)}, bf16[1,6,32,1024]{3,2,1,0:T(8,128)(2,1)S(1)}, u32[]{:S(2)}, u32[]{:S(2)}) %collective-permute-start.30) | collective-permute-done | bytes 393248 | tf_op jit(solution)/shard_map/ppermute | solution.py:37
  68.9 13.7 %collective-permute-done.4.refs_2_ = bf16[4,32,4096]{2,1,0:T(8,128)(2,1)S(1)} collective-permute-done((bf16[4,32,4096]{2,1,0:T(8,128)(2,1)S(1)}, bf16[4,32,4096]{2,1,0:T(8,128)(2,1)S(1)}, u32[]{:S(2)}, u32[]{:S(2)}) %collective-permute-start.4) | collective-permute-done | bytes 1048608 | tf_op jit(solution)/shard_map/ppermute | solution.py:37
  85.0 5.0 %collective-permute-done.10.refs_6_ = bf16[4,32,4096]{2,1,0:T(8,128)(2,1)S(1)} collective-permute-done((bf16[4,32,4096]{2,1,0:T(8,128)(2,1)S(1)}, bf16[4,32,4096]{2,1,0:T(8,128)(2,1)S(1)}, u32[]{:S(2)}, u32[]{:S(2)}) %collective-permute-start.10) | collective-permute-done | bytes 1048608 | tf_op jit(solution)/shard_map/ppermute | solution.py:37
  95.9 4.5 %collective-permute-done.5.refs_3_ = bf16[2,32,4096]{2,1,0:T(8,128)(2,1)S(1)} collective-permute-done((bf16[2,32,4096]{2,1,0:T(8,128)(2,1)S(1)}, bf16[2,32,4096]{2,1,0:T(8,128)(2,1)S(1)}, u32[]{:S(2)}, u32[]{:S(2)}) %collective-permute-start.5) | collective-permute-done | bytes 524320 | tf_op jit(solution)/shard_map/ppermute | solution.py:37
  100.5 11.1 %collective-permute-done.6.refs_4_ = bf16[2,32,4096]{2,1,0:T(8,128)(2,1)S(1)} collective-permute-done((bf16[2,32,4096]{2,1,0:T(8,128)(2,1)S(1)}, bf16[2,32,4096]{2,1,0:T(8,128)(2,1)S(1)}, u32[]{:S(2)}, u32[]{:S(2)}) %collective-permute-start.6) | collective-permute-done | bytes 524320 | tf_op jit(solution)/shard_map/ppermute | solution.py:37
  116.0 6.8 %collective-permute-done.12.refs_8_ = bf16[2,32,4096]{2,1,0:T(8,128)(2,1)S(1)} collective-permute-done((bf16[2,32,4096]{2,1,0:T(8,128)(2,1)S(1)}, bf16[2,32,4096]{2,1,0:T(8,128)(2,1)S(1)}, u32[]{:S(2)}, u32[]{:S(2)}) %collective-permute-start.12) | collective-permute-done | bytes 524320 | tf_op jit(solution)/shard_map/ppermute | solution.py:37
  123.9 9.3 %collective-permute-done.13.refs_9_ = bf16[2,32,4096]{2,1,0:T(8,128)(2,1)S(1)} collective-permute-done((bf16[2,32,4096]{2,1,0:T(8,128)(2,1)S(1)}, bf16[2,32,4096]{2,1,0:T(8,128)(2,1)S(1)}, u32[]{:S(2)}, u32[]{:S(2)}) %collective-permute-start.13) | collective-permute-done | bytes 524320 | tf_op jit(solution)/shard_map/ppermute | solution.py:37
  139.3 19.3 %shard_map.84 = (bf16[1040,512]{1,0:T(8,128)(2,1)}, bf16[1024,512]{1,0:T(8,128)(2,1)}, bf16[4112,512]{1,0:T(8,128)(2,1)}, bf16[512,1024]{1,0:T(8,128)(2,1)}, bf16[512,1024]{1,0:T(8,128)(2,1)}) custom-call(bf16[4,32,4096]{2,1,0:T(8,128)(2,1)} %copy-done.19, bf16[4,32,4096]{2,1,0:T(8,128)(2,1)} %copy-done.23, bf16[4,32,4096]{2,1,0:T(8,128)(2,1)} %copy-done.24, ...), custom_call_target="tpu_custom_call" | custom-call | flops 8657043456 | bytes 35651584 | tf_op jit(solution)/shard_map/pallas_call | solution.py:50
  158.5 12.7 %shard_map.85 = f32[512,4224]{1,0:T(8,128)} custom-call(bf16[4112,512]{1,0:T(8,128)(2,1)} %get-tuple-element.18.refs_0_, bf16[1024,1024]{1,0:T(8,128)(2,1)} %copy-done.1, bf16[1024,1024]{1,0:T(8,128)(2,1)} %copy-done.8, bf16[1024,1024]{1,0:T(8,128)(2,1)} %copy-done.7, bf16[1024,1024]{1,0:T(8,128)(2,1)} %copy-done.9, bf16[1040,1024]{1,0:T(8,128)(2,1)} %copy-done, ...), custom_call_target="tpu_custom_call" | custom-call | flops 5771362304 | bytes 23068672 | tf_op jit(solution)/shard_map/pallas_call | solution.py:50
  171.2 5.9 %convert_element_type.9 = f16[512,4224]{1,0:T(8,128)(2,1)} convert(f32[512,4224]{1,0:T(8,128)} %shard_map.85) | non-fusion elementwise | flops 2162688 | bytes 12976128 | tf_op jit(solution)/shard_map/convert_element_type | solution.py:420
  177.1 4.5 %all-to-all-start = ((f16[16,32,4224]{2,1,0:T(8,128)(2,1)}), f16[16,32,4224]{2,1,0:T(8,128)(2,1)}, u32[]{:S(2)}, u32[]{:S(2)}) async-start(f16[16,32,4224]{2,1,0:T(8,128)(2,1)} %bitcast.21), calls=%async_computation | async-start | bytes 8650752 | tf_op jit(solution)/shard_map/all_to_all | solution.py:421
  189.2 8.5 %collective-permute-start.48 = (bf16[4112,512]{1,0:T(8,128)(2,1)}, bf16[4112,512]{1,0:T(8,128)(2,1)}, u32[]{:S(2)}, u32[]{:S(2)}) collective-permute-start(bf16[4112,512]{1,0:T(8,128)(2,1)} %get-tuple-element.18.refs_0_), channel_id=1, source_target_pairs={{16,0},{17,1},{18,2},{19,3},{20,4},{21,5},{22,6},{23,7},{24,8},{25... | collective-permute-start | bytes 12632072 | tf_op jit(solution)/shard_map/ppermute | solution.py:37
  199.5 62.0 %collective-permute-done.35.refs_11_.refs_7_ = bf16[4,6,32,1024]{3,2,1,0:T(8,128)(2,1)S(1)} collective-permute-done((bf16[4,6,32,1024]{3,2,1,0:T(8,128)(2,1)S(1)}, bf16[4,6,32,1024]{3,2,1,0:T(8,128)(2,1)S(1)}, u32[]{:S(2)}, u32[]{:S(2)}) %collective-permute-start.35) | collective-permute-done | bytes 1572896 | tf_op jit(solution)/shard_map/ppermute | solution.py:37
  264.2 35.5 %collective-permute-done.40.refs_14_.refs_10_ = bf16[4,6,32,1024]{3,2,1,0:T(8,128)(2,1)S(1)} collective-permute-done((bf16[4,6,32,1024]{3,2,1,0:T(8,128)(2,1)S(1)}, bf16[4,6,32,1024]{3,2,1,0:T(8,128)(2,1)S(1)}, u32[]{:S(2)}, u32[]{:S(2)}) %collective-permute-start.40) | collective-permute-done | bytes 1572896 | tf_op jit(solution)/shard_map/ppermute | solution.py:37
  302.7 21.9 %collective-permute-done.20.refs_0_ = bf16[1040,512]{1,0:T(8,128)(2,1)} collective-permute-done((bf16[1040,512]{1,0:T(8,128)(2,1)}, bf16[1040,512]{1,0:T(8,128)(2,1)}, u32[]{:S(2)}, u32[]{:S(2)}) %collective-permute-start.20) | collective-permute-done | bytes 1064992 | tf_op jit(solution)/shard_map/ppermute | solution.py:37
  326.1 6.5 %convert_element_type.10.got = f32[16,32,4224]{2,1,0:T(8,128)} convert(f16[16,32,4224]{2,1,0:T(8,128)(2,1)} %all-to-all-done) | non-fusion elementwise | flops 2162688 | bytes 12976128 | tf_op jit(solution)/shard_map/convert_element_type | solution.py:422
  332.6 5.3 %shard_map.86 = f32[32,4096]{1,0:T(8,128)} custom-call(f32[16,32,4224]{2,1,0:T(8,128)} %convert_element_type.10.got), custom_call_target="tpu_custom_call" | custom-call | flops 268435456 | bytes 9437184 | tf_op jit(solution)/shard_map/pallas_call | solution.py:250
  340.5 7.9 %collective-permute-done.23.refs_1_ = bf16[1024,512]{1,0:T(8,128)(2,1)} collective-permute-done((bf16[1024,512]{1,0:T(8,128)(2,1)}, bf16[1024,512]{1,0:T(8,128)(2,1)}, u32[]{:S(2)}, u32[]{:S(2)}) %collective-permute-start.23) | collective-permute-done | bytes 1048608 | tf_op jit(solution)/shard_map/ppermute | solution.py:37
  351.2 9.3 %shard_map.87 = (f32[688,1024]{1,0:T(8,128)}, f32[688,1024]{1,0:T(8,128)}, f32[688,1024]{1,0:T(8,128)}) custom-call(bf16[4112,512]{1,0:T(8,128)(2,1)} %get-tuple-element.18.refs_0_, bf16[4112,512]{1,0:T(8,128)(2,1)} %collective-permute-done.48.refs_1_.refs_4_, bf16[512,1024]{1,0:T(8,128)(2,1)} %get-tuple-element.21.refs_2_, ...), custom_call_target="tpu_custom_call" | custom-call | flops 4328521728 | bytes 25165824 | tf_op jit(solution)/shard_map/pallas_call | solution.py:50
  362.2 16.3 %shard_map.88 = (f32[688,1024]{1,0:T(8,128)}, f32[688,1024]{1,0:T(8,128)}, f32[688,1024]{1,0:T(8,128)}) custom-call(bf16[1040,512]{1,0:T(8,128)(2,1)} %collective-permute-done.20.refs_0_, bf16[1024,512]{1,0:T(8,128)(2,1)} %collective-permute-done.42.refs_1_, bf16[1040,512]{1,0:T(8,128)(2,1)} %copy-done.27, ...), custom_call_target="tpu_custom_call" | custom-call | flops 8657043456 | bytes 33554432 | tf_op jit(solution)/shard_map/pallas_call | solution.py:50
  379.8 10.5 %shard_map.89 = (f32[688,1024]{1,0:T(8,128)}, f32[688,1024]{1,0:T(8,128)}, f32[688,1024]{1,0:T(8,128)}) custom-call(bf16[1040,512]{1,0:T(8,128)(2,1)} %copy-done.16, bf16[1024,512]{1,0:T(8,128)(2,1)} %collective-permute-done.23.refs_1_, bf16[1040,512]{1,0:T(8,128)(2,1)} %copy-done.17, bf16[1024,512]{1,0:T(8,128)(2,1)} %copy-done.18, ...), custom_call_target="tpu_custom_call" | custom-call | flops 4328521728 | bytes 25165824 | tf_op jit(solution)/shard_map/pallas_call | solution.py:50
  (184 shorter events, 74.2 us)
Async XLA Ops:
  34.1 61.7 %collective-permute-start.15 = (bf16[1024,1024]{1,0:T(8,128)(2,1)S(1)}, bf16[1024,1024]{1,0:T(8,128)(2,1)S(1)}, u32[]{:S(2)}, u32[]{:S(2)}) collective-permute-start(bf16[1024,1024]{1,0:T(8,128)(2,1)S(1)} %pad_maximum_fusion.1.refs_10_.refs_1_), channel_id=1, source_target_pairs={{32,0},{33,1},{34,2},{35,3},{36,4},{37,5},{38,6},{39,7},{40,8},{41... | collective-permute-start | bytes 6291464 | tf_op jit(solution)/shard_map/ppermute | solution.py:37
  34.1 50.7 %collective-permute-start.18 = (bf16[1040,1024]{1,0:T(8,128)(2,1)S(1)}, bf16[1040,1024]{1,0:T(8,128)(2,1)S(1)}, u32[]{:S(2)}, u32[]{:S(2)}) collective-permute-start(bf16[1040,1024]{1,0:T(8,128)(2,1)S(1)} %pad_maximum_fusion.refs_14_.refs_5_), channel_id=1, source_target_pairs={{96,0},{97,1},{98,2},{99,3},{100,4},{101,5},{102,6},{103,7},{104,8... | collective-permute-start | bytes 6389768 | tf_op jit(solution)/shard_map/ppermute | solution.py:37
  35.7 33.3 %collective-permute-start.3 = (bf16[4,32,4096]{2,1,0:T(8,128)(2,1)S(1)}, bf16[4,32,4096]{2,1,0:T(8,128)(2,1)S(1)}, u32[]{:S(2)}, u32[]{:S(2)}) collective-permute-start(bf16[4,32,4096]{2,1,0:T(8,128)(2,1)S(1)} %pad_maximum_fusion.4.refs_0_), channel_id=1, source_target_pairs={{1,0},{2,1},{3,2},{0,3},{5,4},{6,5},{7,6},{4,7},{9,8},{10,9},{11,1... | collective-permute-start | bytes 3145736 | tf_op jit(solution)/shard_map/ppermute | solution.py:37
  82.7 52.3 %collective-permute-start.17 = (bf16[1040,1024]{1,0:T(8,128)(2,1)S(1)}, bf16[1040,1024]{1,0:T(8,128)(2,1)S(1)}, u32[]{:S(2)}, u32[]{:S(2)}) collective-permute-start(bf16[1040,1024]{1,0:T(8,128)(2,1)S(1)} %pad_maximum_fusion.refs_14_.refs_5_), channel_id=1, source_target_pairs={{16,0},{17,1},{18,2},{19,3},{20,4},{21,5},{22,6},{23,7},{24,8},{25... | collective-permute-start | bytes 6389768 | tf_op jit(solution)/shard_map/ppermute | solution.py:37
  84.9 52.4 %collective-permute-start.19 = (bf16[1040,1024]{1,0:T(8,128)(2,1)S(1)}, bf16[1040,1024]{1,0:T(8,128)(2,1)S(1)}, u32[]{:S(2)}, u32[]{:S(2)}) collective-permute-start(bf16[1040,1024]{1,0:T(8,128)(2,1)S(1)} %collective-permute-done.18.refs_16_.refs_7_), channel_id=1, source_target_pairs={{16,0},{17,1},{18,2},{19,3},{20,4},{21,5},{22,6},{23,7},{24,8},{25... | collective-permute-start | bytes 6389768 | tf_op jit(solution)/shard_map/ppermute | solution.py:37
  92.7 41.3 %collective-permute-start.14 = (bf16[1024,1024]{1,0:T(8,128)(2,1)S(1)}, bf16[1024,1024]{1,0:T(8,128)(2,1)S(1)}, u32[]{:S(2)}, u32[]{:S(2)}) collective-permute-start(bf16[1024,1024]{1,0:T(8,128)(2,1)S(1)} %pad_maximum_fusion.1.refs_10_.refs_1_), channel_id=1, source_target_pairs={{16,0},{17,1},{18,2},{19,3},{20,4},{21,5},{22,6},{23,7},{24,8},{25... | collective-permute-start | bytes 6291464 | tf_op jit(solution)/shard_map/ppermute | solution.py:37
  95.8 40.5 %collective-permute-start.16 = (bf16[1024,1024]{1,0:T(8,128)(2,1)S(1)}, bf16[1024,1024]{1,0:T(8,128)(2,1)S(1)}, u32[]{:S(2)}, u32[]{:S(2)}) collective-permute-start(bf16[1024,1024]{1,0:T(8,128)(2,1)S(1)} %collective-permute-done.15.refs_12_.refs_3_), channel_id=1, source_target_pairs={{16,0},{17,1},{18,2},{19,3},{20,4},{21,5},{22,6},{23,7},{24,8},{25... | collective-permute-start | bytes 6291464 | tf_op jit(solution)/shard_map/ppermute | solution.py:37
  133.2 48.4 %collective-permute-start.38 = (bf16[1,6,32,1024]{3,2,1,0:T(8,128)(2,1)S(1)}, bf16[1,6,32,1024]{3,2,1,0:T(8,128)(2,1)S(1)}, u32[]{:S(2)}, u32[]{:S(2)}) collective-permute-start(bf16[1,6,32,1024]{3,2,1,0:T(8,128)(2,1)S(1)} %maximum_bitcast_fusion.1), channel_id=1, source_target_pairs={{3,0},{0,1},{1,2},{2,3},{7,4},{4,5},{5,6},{6,7},{11,8},{8,9},{9,10... | collective-permute-start | bytes 1179656 | tf_op jit(solution)/shard_map/ppermute | solution.py:37
  134.0 50.5 %collective-permute-start.37 = (bf16[1,6,32,1024]{3,2,1,0:T(8,128)(2,1)S(1)}, bf16[1,6,32,1024]{3,2,1,0:T(8,128)(2,1)S(1)}, u32[]{:S(2)}, u32[]{:S(2)}) collective-permute-start(bf16[1,6,32,1024]{3,2,1,0:T(8,128)(2,1)S(1)} %maximum_bitcast_fusion.1), channel_id=1, source_target_pairs={{2,0},{3,1},{0,2},{1,3},{6,4},{7,5},{4,6},{5,7},{10,8},{11,9},{8,1... | collective-permute-start | bytes 1179656 | tf_op jit(solution)/shard_map/ppermute | solution.py:37
  135.0 50.4 %collective-permute-start.36 = (bf16[1,6,32,1024]{3,2,1,0:T(8,128)(2,1)S(1)}, bf16[1,6,32,1024]{3,2,1,0:T(8,128)(2,1)}, u32[]{:S(2)}, u32[]{:S(2)}) collective-permute-start(bf16[1,6,32,1024]{3,2,1,0:T(8,128)(2,1)S(1)} %maximum_bitcast_fusion.1), channel_id=1, source_target_pairs={{1,0},{2,1},{3,2},{0,3},{5,4},{6,5},{7,6},{4,7},{9,8},{10,9},{11,1... | collective-permute-start | bytes 1179656 | tf_op jit(solution)/shard_map/ppermute | solution.py:37
  136.3 61.5 %collective-permute-start.33 = (bf16[4,6,32,1024]{3,2,1,0:T(8,128)(2,1)S(1)}, bf16[4,6,32,1024]{3,2,1,0:T(8,128)(2,1)}, u32[]{:S(2)}, u32[]{:S(2)}) collective-permute-start(bf16[4,6,32,1024]{3,2,1,0:T(8,128)(2,1)S(1)} %pad_maximum_fusion.2.refs_8_.refs_4_), channel_id=1, source_target_pairs={{1,0},{2,1},{3,2},{0,3},{5,4},{6,5},{7,6},{4,7},{9,8},{10,9},{11,1... | collective-permute-start | bytes 4718600 | tf_op jit(solution)/shard_map/ppermute | solution.py:37
  138.9 58.9 %collective-permute-start.34 = (bf16[4,6,32,1024]{3,2,1,0:T(8,128)(2,1)S(1)}, bf16[4,6,32,1024]{3,2,1,0:T(8,128)(2,1)}, u32[]{:S(2)}, u32[]{:S(2)}) collective-permute-start(bf16[4,6,32,1024]{3,2,1,0:T(8,128)(2,1)S(1)} %pad_maximum_fusion.2.refs_8_.refs_4_), channel_id=1, source_target_pairs={{3,0},{0,1},{1,2},{2,3},{7,4},{4,5},{5,6},{6,7},{11,8},{8,9},{9,10... | collective-permute-start | bytes 4718600 | tf_op jit(solution)/shard_map/ppermute | solution.py:37
  177.1 149.0 %all-to-all-start = ((f16[16,32,4224]{2,1,0:T(8,128)(2,1)}), f16[16,32,4224]{2,1,0:T(8,128)(2,1)}, u32[]{:S(2)}, u32[]{:S(2)}) async-start(f16[16,32,4224]{2,1,0:T(8,128)(2,1)} %bitcast.21), calls=%async_computation | async-start | bytes 8650752 | tf_op jit(solution)/shard_map/all_to_all | solution.py:421
  181.7 79.9 %collective-permute-start.35 = (bf16[4,6,32,1024]{3,2,1,0:T(8,128)(2,1)S(1)}, bf16[4,6,32,1024]{3,2,1,0:T(8,128)(2,1)S(1)}, u32[]{:S(2)}, u32[]{:S(2)}) collective-permute-start(bf16[4,6,32,1024]{3,2,1,0:T(8,128)(2,1)S(1)} %pad_maximum_fusion.2.refs_8_.refs_4_), channel_id=1, source_target_pairs={{2,0},{3,1},{0,2},{1,3},{6,4},{7,5},{4,6},{5,7},{10,8},{11,9},{8,1... | collective-permute-start | bytes 4718600 | tf_op jit(solution)/shard_map/ppermute | solution.py:37
  186.8 75.4 %collective-permute-start.39 = (bf16[4,6,32,1024]{3,2,1,0:T(8,128)(2,1)S(1)}, bf16[4,6,32,1024]{3,2,1,0:T(8,128)(2,1)S(1)}, u32[]{:S(2)}, u32[]{:S(2)}) collective-permute-start(bf16[4,6,32,1024]{3,2,1,0:T(8,128)(2,1)S(1)} %pad_maximum_fusion.3.refs_12_.refs_8_), channel_id=1, source_target_pairs={{4,0},{5,1},{6,2},{7,3},{8,4},{9,5},{10,6},{11,7},{12,8},{13,9},{1... | collective-permute-start | bytes 4718600 | tf_op jit(solution)/shard_map/ppermute | solution.py:37
  189.2 161.9 %collective-permute-start.48 = (bf16[4112,512]{1,0:T(8,128)(2,1)}, bf16[4112,512]{1,0:T(8,128)(2,1)}, u32[]{:S(2)}, u32[]{:S(2)}) collective-permute-start(bf16[4112,512]{1,0:T(8,128)(2,1)} %get-tuple-element.18.refs_0_), channel_id=1, source_target_pairs={{16,0},{17,1},{18,2},{19,3},{20,4},{21,5},{22,6},{23,7},{24,8},{25... | collective-permute-start | bytes 12632072 | tf_op jit(solution)/shard_map/ppermute | solution.py:37
  197.8 102.0 %collective-permute-start.40 = (bf16[4,6,32,1024]{3,2,1,0:T(8,128)(2,1)S(1)}, bf16[4,6,32,1024]{3,2,1,0:T(8,128)(2,1)S(1)}, u32[]{:S(2)}, u32[]{:S(2)}) collective-permute-start(bf16[4,6,32,1024]{3,2,1,0:T(8,128)(2,1)S(1)} %pad_maximum_fusion.3.refs_12_.refs_8_), channel_id=1, source_target_pairs={{12,0},{13,1},{14,2},{15,3},{0,4},{1,5},{2,6},{3,7},{4,8},{5,9},{6... | collective-permute-start | bytes 4718600 | tf_op jit(solution)/shard_map/ppermute | solution.py:37
  197.8 102.0 %collective-permute-start.41 = (bf16[4,6,32,1024]{3,2,1,0:T(8,128)(2,1)S(1)}, bf16[4,6,32,1024]{3,2,1,0:T(8,128)(2,1)S(1)}, u32[]{:S(2)}, u32[]{:S(2)}) collective-permute-start(bf16[4,6,32,1024]{3,2,1,0:T(8,128)(2,1)S(1)} %pad_maximum_fusion.3.refs_12_.refs_8_), channel_id=1, source_target_pairs={{8,0},{9,1},{10,2},{11,3},{12,4},{13,5},{14,6},{15,7},{0,8},{1,9},... | collective-permute-start | bytes 4718600 | tf_op jit(solution)/shard_map/ppermute | solution.py:37
  261.6 39.8 %collective-permute-start.22 = (bf16[1024,512]{1,0:T(8,128)(2,1)S(1)}, bf16[1024,512]{1,0:T(8,128)(2,1)}, u32[]{:S(2)}, u32[]{:S(2)}) collective-permute-start(bf16[1024,512]{1,0:T(8,128)(2,1)S(1)} %copy-done.29), channel_id=1, source_target_pairs={{96,0},{97,1},{98,2},{99,3},{100,4},{101,5},{102,6},{103,7},{104,8... | collective-permute-start | bytes 3145736 | tf_op jit(solution)/shard_map/ppermute | solution.py:37
  262.1 39.3 %collective-permute-start.42 = (bf16[1024,512]{1,0:T(8,128)(2,1)S(1)}, bf16[1024,512]{1,0:T(8,128)(2,1)}, u32[]{:S(2)}, u32[]{:S(2)}) collective-permute-start(bf16[1024,512]{1,0:T(8,128)(2,1)S(1)} %copy-done.29), channel_id=1, source_target_pairs={{32,0},{33,1},{34,2},{35,3},{36,4},{37,5},{38,6},{39,7},{40,8},{41... | collective-permute-start | bytes 3145736 | tf_op jit(solution)/shard_map/ppermute | solution.py:37
  299.8 39.2 %collective-permute-start.45 = (bf16[1040,512]{1,0:T(8,128)(2,1)}, bf16[1040,512]{1,0:T(8,128)(2,1)}, u32[]{:S(2)}, u32[]{:S(2)}) collective-permute-start(bf16[1040,512]{1,0:T(8,128)(2,1)} %get-tuple-element.19), channel_id=1, source_target_pairs={{96,0},{97,1},{98,2},{99,3},{100,4},{101,5},{102,6},{103,7},{104,8... | collective-permute-start | bytes 3194888 | tf_op jit(solution)/shard_map/ppermute | solution.py:37
  301.3 47.0 %collective-permute-start.23 = (bf16[1024,512]{1,0:T(8,128)(2,1)}, bf16[1024,512]{1,0:T(8,128)(2,1)}, u32[]{:S(2)}, u32[]{:S(2)}) collective-permute-start(bf16[1024,512]{1,0:T(8,128)(2,1)} %collective-permute-done.22.refs_5_), channel_id=1, source_target_pairs={{96,0},{97,1},{98,2},{99,3},{100,4},{101,5},{102,6},{103,7},{104,8... | collective-permute-start | bytes 3145736 | tf_op jit(solution)/shard_map/ppermute | solution.py:37
  301.4 48.4 %collective-permute-start.44 = (bf16[1024,512]{1,0:T(8,128)(2,1)}, bf16[1024,512]{1,0:T(8,128)(2,1)}, u32[]{:S(2)}, u32[]{:S(2)}) collective-permute-start(bf16[1024,512]{1,0:T(8,128)(2,1)} %collective-permute-done.42.refs_1_), channel_id=1, source_target_pairs={{16,0},{17,1},{18,2},{19,3},{20,4},{21,5},{22,6},{23,7},{24,8},{25... | collective-permute-start | bytes 3145736 | tf_op jit(solution)/shard_map/ppermute | solution.py:37
  350.6 27.9 %collective-permute-start.25 = (bf16[1024,512]{1,0:T(8,128)(2,1)}, bf16[1024,512]{1,0:T(8,128)(2,1)S(1)}, u32[]{:S(2)}, u32[]{:S(2)}) collective-permute-start(bf16[1024,512]{1,0:T(8,128)(2,1)} %collective-permute-done.23.refs_1_), channel_id=1, source_target_pairs={{16,0},{17,1},{18,2},{19,3},{20,4},{21,5},{22,6},{23,7},{24,8},{25... | collective-permute-start | bytes 3145736 | tf_op jit(solution)/shard_map/ppermute | solution.py:37
  (63 other events, 1296.6 us)
where the time goes:
time: 391 us
  waiting for transfers between devices  217 us (55%)
  Pallas kernels  73.3 us (19%)
  starting transfers between devices  70 us (18%)
  other arithmetic  18.6 us (5%)
  local copies, waits for them, and re-layouts  9.84 us (3%)
    ppermute x49, waiting for transfers between devices, moved(): return lax.ppermute(array, AXES, pairs)  217 us
    pallas_call x5, Pallas kernels, call(): pl.pallas_call(body, out_shape=out_shape, in_specs=ins, out_specs=outs, s...  68 us
    ppermute x49, starting transfers between devices, moved(): return lax.ppermute(array, AXES, pairs)  65.4 us
    unnamed x70, local copies, waits for them, and re-layouts  8.68 us
  transfers between devices with their start and end apart: 50, of which 16 were waited for; matrix products, arithmetic and copies ran while one was open for 5% of the time, Pallas kernels for 16%

commit v1 on v0

--- a/solution.py
+++ b/solution.py
@@ -58,18 +58,17 @@
     )(*args)
 
 
-FROM = ((0, 0, 4, 0), (1, 0, 4, 1), (2, 0, 4, 3), (3, 0, 2, 2), (4, 2, 2, 2))
-WHOLE = ((0, 0, 4, 0), (1, 0, 4, 1), (2, 0, 4, 3), (3, 0, 4, 2))
+FROM = ((0, 0), (2, 0), (0, 1), (2, 1), (0, 3), (2, 3), (0, 2), (2, 2))
 
 
 def forward_kernel(*refs):
-    xs, ds, was, wbs = refs[:5], refs[5:10], refs[10:14], refs[14:18]
-    acts_l, acts_h, side, x_own, d_own = refs[18:23]
-    v, w, sums, act, sx, sd, sw, so = refs[23:]
+    xs, ds, was, wbs = refs[:8], refs[8:16], refs[16:20], refs[20:24]
+    acts_l, acts_h, side, x_own, d_own = refs[24:29]
+    v, w, sums, act, sx, sd, sw, so = refs[29:]
     z, y = place()
     x_copies, d_copies = [], []
-    for i, first, count, off in FROM:
-        for j in range(count):
+    for i, (first, off) in enumerate(FROM):
+        for j in range(2):
             row = pl.multiple_of((lax.rem(z + first + j, 4) * 4 + lax.rem(y + off, 4)) * ROWS, ROWS)
             x_copies.append(
                 pltpu.make_async_copy(xs[i].at[j], v.at[0, pl.ds(row, ROWS)], sx.at[len(x_copies)]))
@@ -168,7 +167,7 @@
             pltpu.SemaphoreType.DMA((16,)), pltpu.SemaphoreType.DMA((9,)),
         ],
         2 * TOK * WIDE * UNITS * 3,
-        [ANY] * 18,
+        [ANY] * 24,
         (ANY,) * 5,
         (*xs, *ds, *was, *wbs),
         34 << 20,
@@ -193,29 +192,40 @@
     tu[...] = act[UNITS:, :].T
     norm = jnp.sum(jnp.abs(tg[...].astype(F32)), axis=1, keepdims=True)
     norm = norm + jnp.sum(jnp.abs(tu[...].astype(F32)), axis=1, keepdims=True)
-    e = jnp.ceil(jnp.log2(jnp.maximum(norm * (1.02 * W_MAX), 1e-30)))
+    e = jnp.ceil(jnp.log2(jnp.maximum(jnp.max(norm, axis=0, keepdims=True) * (1.02 * W_MAX), 1e-30)))
     expo[...] = jnp.broadcast_to(e, (TOK, TAIL))
-    puts = [pltpu.make_async_copy(expo, out.at[:, pl.ds(WIDE, TAIL)], so.at[4])]
-    puts[0].start()
-    for k in range(4):
-        for c in copies[k]:
-            c.wait()
-        if k + 2 < 4:
-            for c in copies[k + 2]:
-                c.start()
-        if k >= 2:
-            puts[k - 1].wait()
+    tail = pltpu.make_async_copy(expo, out.at[:, pl.ds(WIDE, TAIL)], so.at[4])
+    tail.start()
+
+    def put(k):
+        at = k * DEPTH if isinstance(k, int) else pl.multiple_of(k * DEPTH, DEPTH)
+        return pltpu.make_async_copy(total.at[k % 2 if isinstance(k, int) else lax.rem(k, 2)],
+                                     out.at[:, pl.ds(at, DEPTH)], so.at[k])
+
+    def part(k, _):
+        for n in range(4):
+            @pl.when(k == n)
+            def _():
+                for c in copies[n]:
+                    c.wait()
+                if n + 2 < 4:
+                    for c in copies[n + 2]:
+                        c.start()
+                if n >= 2:
+                    put(n - 2).wait()
 
         def tile(j, _):
             n = pl.ds(pl.multiple_of(j * 512, 512), 512)
             v = dot(tg[...], wa[k, :, n], 1, 0) + dot(tu[...], wb[k, :, n], 1, 0)
-            total[k % 2, :, n] = v * jnp.exp2(14.0 - expo[:, :1])
+            total[lax.rem(k, 2), :, n] = v * jnp.exp2(14.0 - expo[:, :1])
             return 0
 
         lax.fori_loop(0, 2, tile, 0)
-        puts.append(pltpu.make_async_copy(total.at[k % 2], out.at[:, pl.ds(k * DEPTH, DEPTH)], so.at[k]))
-        puts[-1].start()
-    for c in (puts[0], puts[3], puts[4]):
+        put(k).start()
+        return 0
+
+    lax.fori_loop(0, 4, part, 0)
+    for c in (tail, put(2), put(3)):
         c.wait()
 
 
@@ -238,29 +248,9 @@
     )
 
 
-def sum_kernel(got, out):
-    v = None
-    for i in range(16):
-        w = got[i, :, :WIDE] * jnp.exp2(got[i, :, WIDE:WIDE + 1] - 14.0)
-        v = w if v is None else v + w
-    out[...] = v
-
-
-def summed(got):
-    return pl.pallas_call(
-        sum_kernel,
-        grid=(ROWS // 8,),
-        out_shape=jax.ShapeDtypeStruct((ROWS, WIDE), F32),
-        in_specs=[pl.BlockSpec((16, 8, WIDE + TAIL), lambda i: (0, i, 0))],
-        out_specs=pl.BlockSpec((8, WIDE), lambda i: (i, 0)),
-        compiler_params=pltpu.CompilerParams(vmem_limit_bytes=LIMIT),
-        cost_estimate=pl.CostEstimate(flops=1 << 28, bytes_accessed=9 << 20, transcendentals=0),
-    )(got)
-
-
 def weight_kernel(acts, n_acts, columns, has_base, n_in, *refs):
     ins, outs = refs[:n_in], refs[n_in:n_in + 3]
-    a, xc, dc, total, sa, sc, sb, so = refs[n_in + 3:]
+    a, cols, total, sa, sc, sb, so = refs[n_in + 3:]
     z, y = place()
     stages = [[], [], []]
     n = 0
@@ -273,9 +263,9 @@
                         ins[i].at[pl.ds(lo - r0, hi - lo)], a.at[pl.ds(lo, hi - lo), pl.ds(g * TOK, TOK)], sa.at[n]))
                     n += 1
     columns(ins[n_acts:], z, y, lambda src, to: stages[0].append(
-        pltpu.make_async_copy(src, to, sc.at[0, len(stages[0])])), xc, 0)
+        pltpu.make_async_copy(src, to, sc.at[0, len(stages[0])])), cols.at[0], 0)
     columns(ins[n_acts:], z, y, lambda src, to: stages[2].append(
-        pltpu.make_async_copy(src, to, sc.at[1, len(stages[2])])), dc, 1)
+        pltpu.make_async_copy(src, to, sc.at[1, len(stages[2])])), cols.at[1], 1)
     if has_base:
         for s in range(3):
             stages[s].append(pltpu.make_async_copy(ins[n_in - 3 + s], total.at[s], sb.at[s]))
@@ -288,31 +278,23 @@
     begin(1)
     done = [pltpu.make_async_copy(total.at[i], outs[i], so.at[i]) for i in range(3)]
 
-    def product(i, cols):
-        v = dot(a[pl.ds(pl.multiple_of(i * UNITS, 16), UNITS), :], cols[...].reshape(len(acts) * TOK, DEPTH), 1, 0)
+    def product(i, _):
+        for n in range(3):
+            @pl.when(i == n)
+            def _():
+                if n:
+                    done[n - 1].start()
+                for c in stages[n]:
+                    c.wait()
+                if n == 0:
+                    begin(2)
+
+        rows = pl.ds(pl.multiple_of(i * UNITS, 16), UNITS)
+        v = dot(a[rows, :], cols[i // 2].reshape(len(acts) * TOK, DEPTH), 1, 0)
         total[i] = total[i] + v if has_base else v
-
-    def pair(i, _):
-        @pl.when(i == 0)
-        def _():
-            for c in stages[0]:
-                c.wait()
-            begin(2)
-
-        @pl.when(i == 1)
-        def _():
-            done[0].start()
-            for c in stages[1]:
-                c.wait()
-
-        product(i, xc)
         return 0
 
-    lax.fori_loop(0, 2, pair, 0)
-    done[1].start()
-    for c in stages[2]:
-        c.wait()
-    product(2, dc)
+    lax.fori_loop(0, 3, product, 0)
     done[2].start()
     for c in done:
         c.wait()
@@ -326,12 +308,12 @@
 
 
 def plane_columns(first_group, count, refs, z, y, add, buf, kind):
-    for i, first, n, off in WHOLE:
-        for j in range(n):
+    for i, (first, off) in enumerate(FROM):
+        for j in range(2):
             a, b = lax.rem(z + first + j, 4), lax.rem(y + off, 4)
             if kind:
                 a, b = lax.rem(z + off, 4), lax.rem(y + first + j, 4)
-            add(refs[4 * kind + i].at[j, pl.ds(first_group, count)], buf.at[:, a * 4 + b])
+            add(refs[8 * kind + i].at[j, pl.ds(first_group, count)], buf.at[:, a * 4 + b])
 
 
 def weight_sums(groups, columns, arrays, base):
@@ -346,15 +328,15 @@
     n_acts = len(ins)
     ins += list(arrays) + list(base or [])
     n = len(groups)
-    col = (n, TOK, DEPTH) if columns is near_columns else (n, 16, ROWS, DEPTH)
+    col = (2, n, TOK, DEPTH) if columns is near_columns else (2, n, 16, ROWS, DEPTH)
     out = jax.ShapeDtypeStruct((UNITS, DEPTH), F32)
     return call(
         functools.partial(weight_kernel, acts, n_acts, columns, base is not None, len(ins)),
         (out,) * 3,
         [
-            pltpu.VMEM((3 * UNITS, n * TOK), BF), pltpu.VMEM(col, BF), pltpu.VMEM(col, BF),
+            pltpu.VMEM((3 * UNITS, n * TOK), BF), pltpu.VMEM(col, BF),
             pltpu.VMEM((3, UNITS, DEPTH), F32),
-            pltpu.SemaphoreType.DMA((3 * n_acts,)), pltpu.SemaphoreType.DMA((2, 32)),
+            pltpu.SemaphoreType.DMA((3 * n_acts,)), pltpu.SemaphoreType.DMA((2, 48)),
             pltpu.SemaphoreType.DMA((3,)), pltpu.SemaphoreType.DMA((3,)),
         ],
         2 * 3 * UNITS * DEPTH * n * TOK,
@@ -368,7 +350,7 @@
 def block(inputs, w_gate, w_up, w_down, d_out):
     fs = lax.axis_index("fs")
 
-    def relative(v):
+    def relative(v, fs=fs):
         parts = [v[:, i * DEPTH:(i + 1) * DEPTH] for i in range(4)]
         out = []
         for k in range(4):
@@ -378,27 +360,30 @@
             out.append(w)
         return out
 
+    mark = lax.optimization_barrier(fs) * 3 - 1
+    mark = (mark + 1) // 3
+
     xp, dp = relative(inputs), relative(d_out)
     x_own, d_own = jnp.concatenate(xp, axis=1), jnp.concatenate(dp, axis=1)
 
-    def spread(own, first, second, forward):
-        line = jnp.concatenate(
-            [own[None]] + [moved(own[None], **{first: d}) for d in (1, 2, 3)], axis=0)
-        up, down = moved(line, **{second: 1}), moved(line, **{second: -1})
-        if not forward:
-            return line, up, down, moved(line, **{second: 2})
-        low, high = up[:2], down[2:]
-        return line, up, down, moved(low, **{second: 1}), moved(high, **{second: -1})
-
-    xs = spread(x_own, "dz", "dy", True)
-    ds = spread(d_own, "dy", "dz", True)
+    def spread(own, first, second):
+        own = own[None]
+        one, two, three = (moved(own, **{first: d}) for d in (1, 2, 3))
+        low, high = jnp.concatenate([own, one], axis=0), jnp.concatenate([two, three], axis=0)
+        up_l, up_h = moved(low, **{second: 1}), moved(high, **{second: 1})
+        down_l, down_h = moved(low, **{second: -1}), moved(high, **{second: -1})
+        far_l, far_h = moved(up_l, **{second: 1}), moved(down_h, **{second: -1})
+        return low, high, up_l, up_h, down_l, down_h, far_l, far_h
+
+    xs = spread(x_own, "dz", "dy")
+    ds = spread(d_own, "dy", "dz")
 
     side = moved(jnp.stack([xp[1], dp[1], xp[3], dp[3]]), flip=1)
     far = jnp.stack([xp[0], side[0], dp[0], side[1]])
     near = jnp.stack([xp[2], side[2], dp[2], side[3]])
     got = (moved(near, dx=1), moved(near, dx=-1), moved(far, dx=2))
-    xcs = spread(jnp.concatenate([v[:2] for v in got], axis=0), "dz", "dy", False)
-    dcs = spread(jnp.concatenate([v[2:] for v in got], axis=0), "dy", "dz", False)
+    xcs = spread(jnp.concatenate([v[:2] for v in got], axis=0), "dz", "dy")
+    dcs = spread(jnp.concatenate([v[2:] for v in got], axis=0), "dy", "dz")
 
     wa = jnp.concatenate([w_gate.T, w_down[:CUT]], axis=0)
     wb = jnp.concatenate([w_up.T, w_down[CUT:]], axis=0)
@@ -419,7 +404,11 @@
 
     packed = input_sums(own, was, wbs).astype(F16)
     got = lax.all_to_all(packed.reshape(16, ROWS, WIDE + TAIL), "tp", 0, 0)
-    grad_inputs = jnp.concatenate(relative(summed(got.astype(F32)).astype(BF)), axis=1)
+    back = lax.optimization_barrier(jnp.exp2(got[:, 0, WIDE].astype(F32) - 14.0))
+    total = 0.0
+    for i in range(16):
+        total = total + got[i, :, :WIDE].astype(F32) * back[i]
+    grad_inputs = jnp.concatenate(relative(total.astype(BF), mark), axis=1)
 
     full = 3 * UNITS
 

time: 391 us -> 478 us (1.22); the launches traced: 391 us -> 471 us
  waiting for transfers between devices: 217 us -> 257 us
  starting transfers between devices: 70 us -> 109 us
    ppermute x49 -> x59, waiting for transfers between devices: 217 us -> 257 us  [moved(): return lax.ppermute(array, AXES, pairs)]
    ppermute x49 -> x59, starting transfers between devices: 65.4 us -> 104 us  [moved(): return lax.ppermute(array, AXES, pairs)]
    convert_element_type x2 -> x1, other arithmetic: 7.59 us -> 13 us  [block(): grad_inputs = jnp.concatenate(relative(total.astype(BF), mark), axis=1)]
    pallas_call x1 -> x0, Pallas kernels: 5.3 us -> none  [summed(): pl.pallas_call(sum_kernel, grid=(ROWS // 8,), out_shape=jax.ShapeDtypeStr...]
  transfers between devices with their start and end apart: 50 -> 60, of which waited for: 16 -> 23; matrix products, arithmetic and copies ran while one was open for 5% -> 5% of each run, Pallas kernels for 16% -> 12%
where the time goes in v1:
time: 478 us; the launch traced here: 471 us
  waiting for transfers between devices  257 us (54%)
  starting transfers between devices  109 us (23%)
  Pallas kernels  69.2 us (14%)
  other arithmetic  22.6 us (5%)
  local copies, waits for them, and re-layouts  11.8 us (2%)
    ppermute x59, waiting for transfers between devices, moved(): return lax.ppermute(array, AXES, pairs)  257 us
    ppermute x59, starting transfers between devices, moved(): return lax.ppermute(array, AXES, pairs)  104 us
    pallas_call x5, Pallas kernels, call(): pl.pallas_call(body, out_shape=out_shape, in_specs=ins, out_specs=outs, s...  69.2 us
    convert_element_type x1, other arithmetic, block(): grad_inputs = jnp.concatenate(relative(total.astype(BF), mark), axis=1)  13 us
  transfers between devices with their start and end apart: 60, of which 23 were waited for; matrix products, arithmetic and copies ran while one was open for 5% of the time, Pallas kernels for 12%

profile of v1, /device:TPU:1, one launch (start us, length us, event | category | flops | bytes accessed | tf_op | source)
XLA Modules:
  0.0 470.9 jit_solution(5035304614149899176)
XLA Ops:
  28.8 48.4 %collective-permute-done.33 = bf16[4,32,1024]{2,1,0:T(8,128)(2,1)S(1)} collective-permute-done((bf16[4,32,1024]{2,1,0:T(8,128)(2,1)S(1)}, bf16[4,32,1024]{2,1,0:T(8,128)(2,1)S(1)}, u32[]{:S(2)}, u32[]{:S(2)}) %collective-permute-start.33) | collective-permute-done | bytes 262176 | tf_op jit(solution)/shard_map/ppermute | solution.py:37
  77.2 7.4 %collective-permute-done.32 = bf16[4,32,1024]{2,1,0:T(8,128)(2,1)S(1)} collective-permute-done((bf16[4,32,1024]{2,1,0:T(8,128)(2,1)S(1)}, bf16[4,32,1024]{2,1,0:T(8,128)(2,1)S(1)}, u32[]{:S(2)}, u32[]{:S(2)}) %collective-permute-start.32) | collective-permute-done | bytes 262176 | tf_op jit(solution)/shard_map/ppermute | solution.py:37
  90.4 6.5 %collective-permute-done.5.refs_4_ = bf16[2,32,4096]{2,1,0:T(8,128)(2,1)S(1)} collective-permute-done((bf16[2,32,4096]{2,1,0:T(8,128)(2,1)S(1)}, bf16[2,32,4096]{2,1,0:T(8,128)(2,1)S(1)}, u32[]{:S(2)}, u32[]{:S(2)}) %collective-permute-start.5) | collective-permute-done | bytes 524320 | tf_op jit(solution)/shard_map/ppermute | solution.py:37
  100.3 7.8 %collective-permute-done.6.refs_5_ = bf16[2,32,4096]{2,1,0:T(8,128)(2,1)S(1)} collective-permute-done((bf16[2,32,4096]{2,1,0:T(8,128)(2,1)S(1)}, bf16[2,32,4096]{2,1,0:T(8,128)(2,1)S(1)}, u32[]{:S(2)}, u32[]{:S(2)}) %collective-permute-start.6) | collective-permute-done | bytes 524320 | tf_op jit(solution)/shard_map/ppermute | solution.py:37
  113.9 7.0 %collective-permute-done.14.refs_12_ = bf16[2,32,4096]{2,1,0:T(8,128)(2,1)S(1)} collective-permute-done((bf16[2,32,4096]{2,1,0:T(8,128)(2,1)S(1)}, bf16[2,32,4096]{2,1,0:T(8,128)(2,1)S(1)}, u32[]{:S(2)}, u32[]{:S(2)}) %collective-permute-start.14) | collective-permute-done | bytes 524320 | tf_op jit(solution)/shard_map/ppermute | solution.py:37
  121.2 10.9 %collective-permute-done.15.refs_13_ = bf16[2,32,4096]{2,1,0:T(8,128)(2,1)S(1)} collective-permute-done((bf16[2,32,4096]{2,1,0:T(8,128)(2,1)S(1)}, bf16[2,32,4096]{2,1,0:T(8,128)(2,1)S(1)}, u32[]{:S(2)}, u32[]{:S(2)}) %collective-permute-start.15) | collective-permute-done | bytes 524320 | tf_op jit(solution)/shard_map/ppermute | solution.py:37
  136.0 13.4 %collective-permute-done.8.refs_7_ = bf16[2,32,4096]{2,1,0:T(8,128)(2,1)S(1)} collective-permute-done((bf16[2,32,4096]{2,1,0:T(8,128)(2,1)S(1)}, bf16[2,32,4096]{2,1,0:T(8,128)(2,1)S(1)}, u32[]{:S(2)}, u32[]{:S(2)}) %collective-permute-start.8) | collective-permute-done | bytes 524320 | tf_op jit(solution)/shard_map/ppermute | solution.py:37
  150.6 10.3 %collective-permute-done.16.refs_14_ = bf16[2,32,4096]{2,1,0:T(8,128)(2,1)S(1)} collective-permute-done((bf16[2,32,4096]{2,1,0:T(8,128)(2,1)S(1)}, bf16[2,32,4096]{2,1,0:T(8,128)(2,1)S(1)}, u32[]{:S(2)}, u32[]{:S(2)}) %collective-permute-start.16) | collective-permute-done | bytes 524320 | tf_op jit(solution)/shard_map/ppermute | solution.py:37
  160.9 11.7 %collective-permute-done.17.refs_15_ = bf16[2,32,4096]{2,1,0:T(8,128)(2,1)S(1)} collective-permute-done((bf16[2,32,4096]{2,1,0:T(8,128)(2,1)S(1)}, bf16[2,32,4096]{2,1,0:T(8,128)(2,1)S(1)}, u32[]{:S(2)}, u32[]{:S(2)}) %collective-permute-start.17) | collective-permute-done | bytes 524320 | tf_op jit(solution)/shard_map/ppermute | solution.py:37
  178.2 19.4 %shard_map.84 = (bf16[1040,512]{1,0:T(8,128)(2,1)}, bf16[1024,512]{1,0:T(8,128)(2,1)}, bf16[4112,512]{1,0:T(8,128)(2,1)}, bf16[512,1024]{1,0:T(8,128)(2,1)}, bf16[512,1024]{1,0:T(8,128)(2,1)}) custom-call(bf16[2,32,4096]{2,1,0:T(8,128)(2,1)} %copy-done.29, bf16[2,32,4096]{2,1,0:T(8,128)(2,1)} %copy-done.31, bf16[2,32,4096]{2,1,0:T(8,128)(2,1)} %copy-done.37, ...), custom_call_target="tpu_custom_call" | custom-call | flops 8657043456 | bytes 35651584 | tf_op jit(solution)/shard_map/pallas_call | solution.py:50
  197.7 12.7 %shard_map.85 = f32[512,4224]{1,0:T(8,128)} custom-call(bf16[4112,512]{1,0:T(8,128)(2,1)} %get-tuple-element.18.refs_0_, bf16[1024,1024]{1,0:T(8,128)(2,1)} %copy-done.1, bf16[1024,1024]{1,0:T(8,128)(2,1)} %copy-done.8, bf16[1024,1024]{1,0:T(8,128)(2,1)} %copy-done.7, bf16[1024,1024]{1,0:T(8,128)(2,1)} %copy-done.9, bf16[1040,1024]{1,0:T(8,128)(2,1)} %copy-done, ...), custom_call_target="tpu_custom_call" | custom-call | flops 5771362304 | bytes 23068672 | tf_op jit(solution)/shard_map/pallas_call | solution.py:50
  210.4 5.9 %convert_element_type.74 = f16[512,4224]{1,0:T(8,128)(2,1)} convert(f32[512,4224]{1,0:T(8,128)} %shard_map.85) | non-fusion elementwise | flops 2162688 | bytes 12976128 | tf_op jit(solution)/shard_map/convert_element_type | solution.py:405
  227.7 48.2 %collective-permute-done.34 = bf16[1,6,32,1024]{3,2,1,0:T(8,128)(2,1)S(1)} collective-permute-done((bf16[1,6,32,1024]{3,2,1,0:T(8,128)(2,1)S(1)}, bf16[1,6,32,1024]{3,2,1,0:T(8,128)(2,1)S(1)}, u32[]{:S(2)}, u32[]{:S(2)}) %collective-permute-start.34) | collective-permute-done | bytes 393248 | tf_op jit(solution)/shard_map/ppermute | solution.py:37
  279.1 6.4 %collective-permute-done.36 = bf16[1,6,32,1024]{3,2,1,0:T(8,128)(2,1)S(1)} collective-permute-done((bf16[1,6,32,1024]{3,2,1,0:T(8,128)(2,1)S(1)}, bf16[1,6,32,1024]{3,2,1,0:T(8,128)(2,1)S(1)}, u32[]{:S(2)}, u32[]{:S(2)}) %collective-permute-start.36) | collective-permute-done | bytes 393248 | tf_op jit(solution)/shard_map/ppermute | solution.py:37
  294.9 21.4 %collective-permute-done.45 = bf16[1,6,32,1024]{3,2,1,0:T(8,128)(2,1)S(1)} collective-permute-done((bf16[1,6,32,1024]{3,2,1,0:T(8,128)(2,1)S(1)}, bf16[1,6,32,1024]{3,2,1,0:T(8,128)(2,1)S(1)}, u32[]{:S(2)}, u32[]{:S(2)}) %collective-permute-start.45) | collective-permute-done | bytes 393248 | tf_op jit(solution)/shard_map/ppermute | solution.py:37
  334.1 13.5 %collective-permute-done.47.refs_19_.refs_15_ = bf16[2,6,32,1024]{3,2,1,0:T(8,128)(2,1)S(1)} collective-permute-done((bf16[2,6,32,1024]{3,2,1,0:T(8,128)(2,1)S(1)}, bf16[2,6,32,1024]{3,2,1,0:T(8,128)(2,1)S(1)}, u32[]{:S(2)}, u32[]{:S(2)}) %collective-permute-start.47) | collective-permute-done | bytes 786464 | tf_op jit(solution)/shard_map/ppermute | solution.py:37
  366.2 9.6 %collective-permute-done.51.refs_23_.refs_19_ = bf16[2,6,32,1024]{3,2,1,0:T(8,128)(2,1)} collective-permute-done((bf16[2,6,32,1024]{3,2,1,0:T(8,128)(2,1)S(1)}, bf16[2,6,32,1024]{3,2,1,0:T(8,128)(2,1)}, u32[]{:S(2)}, u32[]{:S(2)}) %collective-permute-start.51) | collective-permute-done | bytes 786464 | tf_op jit(solution)/shard_map/ppermute | solution.py:37
  377.7 11.5 %collective-permute-start.54 = (bf16[1024,512]{1,0:T(8,128)(2,1)}, bf16[1024,512]{1,0:T(8,128)(2,1)S(1)}, u32[]{:S(2)}, u32[]{:S(2)}) collective-permute-start(bf16[1024,512]{1,0:T(8,128)(2,1)} %collective-permute-done.52.refs_1_), channel_id=1, source_target_pairs={{16,0},{17,1},{18,2},{19,3},{20,4},{21,5},{22,6},{23,7},{24,8},{25... | collective-permute-start | bytes 3145736 | tf_op jit(solution)/shard_map/ppermute | solution.py:37
  389.9 9.7 %collective-permute-done.24.refs_0_ = bf16[1040,512]{1,0:T(8,128)(2,1)} collective-permute-done((bf16[1040,512]{1,0:T(8,128)(2,1)}, bf16[1040,512]{1,0:T(8,128)(2,1)}, u32[]{:S(2)}, u32[]{:S(2)}) %collective-permute-start.24) | collective-permute-done | bytes 1064992 | tf_op jit(solution)/shard_map/ppermute | solution.py:37
  403.0 13.0 %fusion = bf16[32,4096]{1,0:T(8,128)(2,1)S(1)} fusion(f16[16,32,4224]{2,1,0:T(8,128)(2,1)} %all-to-all-done, f32[]{:T(128)} %bitcast.22, f32[]{:T(128)} %bitcast.20, f32[]{:T(128)} %bitcast.19, f32[]{:T(128)} %bitcast.18, f32[]{:T(128)} %bitcast.17, f32[]{:T(128)} %bitcast.16, f32[]{:T(128)} %bitcast.15, f32[]{:T(128)} %bitcast.14, f32[]{:T(128)} %bitcast.13, ...), kind=kLoop, calls=%fused_computation.7 | loop fusion | flops 6291456 | bytes 4456512 | tf_op jit(solution)/shard_map/convert_element_type | solution.py:411
  416.1 8.5 %collective-permute-start.57 = (bf16[1024,512]{1,0:T(8,128)(2,1)}, bf16[1024,512]{1,0:T(8,128)(2,1)S(1)}, u32[]{:S(2)}, u32[]{:S(2)}) collective-permute-start(bf16[1024,512]{1,0:T(8,128)(2,1)} %collective-permute-done.26.refs_5_), channel_id=1, source_target_pairs={{16,0},{17,1},{18,2},{19,3},{20,4},{21,5},{22,6},{23,7},{24,8},{25... | collective-permute-start | bytes 3145736 | tf_op jit(solution)/shard_map/ppermute | solution.py:37
  430.6 9.6 %shard_map.86 = (f32[688,1024]{1,0:T(8,128)}, f32[688,1024]{1,0:T(8,128)}, f32[688,1024]{1,0:T(8,128)}) custom-call(bf16[4112,512]{1,0:T(8,128)(2,1)} %get-tuple-element.18.refs_0_, bf16[4112,512]{1,0:T(8,128)(2,1)} %collective-permute-done.58.refs_1_.refs_4_, bf16[512,1024]{1,0:T(8,128)(2,1)} %get-tuple-element.21.refs_2_, ...), custom_call_target="tpu_custom_call" | custom-call | flops 4328521728 | bytes 25165824 | tf_op jit(solution)/shard_map/pallas_call | solution.py:50
  441.9 16.6 %shard_map.87 = (f32[688,1024]{1,0:T(8,128)}, f32[688,1024]{1,0:T(8,128)}, f32[688,1024]{1,0:T(8,128)}) custom-call(bf16[1040,512]{1,0:T(8,128)(2,1)} %collective-permute-done.24.refs_0_, bf16[1024,512]{1,0:T(8,128)(2,1)} %collective-permute-done.52.refs_1_, bf16[1040,512]{1,0:T(8,128)(2,1)} %copy-done.33, bf16[1024,512]{1,0:T(8,128)(2,1)} %copy-done.35, ...), custom_call_target="tpu_custom_call" | custom-call | flops 8657043456 | bytes 33554432 | tf_op jit(solution)/shard_map/pallas_call | solution.py:50
  459.9 10.8 %shard_map.88 = (f32[688,1024]{1,0:T(8,128)}, f32[688,1024]{1,0:T(8,128)}, f32[688,1024]{1,0:T(8,128)}) custom-call(bf16[1040,512]{1,0:T(8,128)(2,1)} %copy-done.14, bf16[1024,512]{1,0:T(8,128)(2,1)} %copy-done.16, bf16[1040,512]{1,0:T(8,128)(2,1)} %copy-done.15, bf16[1024,512]{1,0:T(8,128)(2,1)} %copy-done.17, bf16[2,6,32,1024]{3,2,1,0:T(8,128)(2,1)} %copy-done.2, ...), custom_call_target="tpu_custom_call" | custom-call | flops 4328521728 | bytes 25165824 | tf_op jit(solution)/shard_map/pallas_call | solution.py:50
  (236 shorter events, 128.9 us)
Async XLA Ops:
  21.3 114.5 %collective-permute-start.19 = (bf16[1024,1024]{1,0:T(8,128)(2,1)S(1)}, bf16[1024,1024]{1,0:T(8,128)(2,1)S(1)}, u32[]{:S(2)}, u32[]{:S(2)}) collective-permute-start(bf16[1024,1024]{1,0:T(8,128)(2,1)S(1)} %pad_maximum_fusion.1.refs_16_.refs_1_), channel_id=1, source_target_pairs={{32,0},{33,1},{34,2},{35,3},{36,4},{37,5},{38,6},{39,7},{40,8},{41... | collective-permute-start | bytes 6291464 | tf_op jit(solution)/shard_map/ppermute | solution.py:37
  23.9 89.9 %collective-permute-start.22 = (bf16[1040,1024]{1,0:T(8,128)(2,1)S(1)}, bf16[1040,1024]{1,0:T(8,128)(2,1)S(1)}, u32[]{:S(2)}, u32[]{:S(2)}) collective-permute-start(bf16[1040,1024]{1,0:T(8,128)(2,1)S(1)} %pad_maximum_fusion.refs_20_.refs_5_), channel_id=1, source_target_pairs={{96,0},{97,1},{98,2},{99,3},{100,4},{101,5},{102,6},{103,7},{104,8... | collective-permute-start | bytes 6389768 | tf_op jit(solution)/shard_map/ppermute | solution.py:37
  24.0 53.1 %collective-permute-start.33 = (bf16[4,32,1024]{2,1,0:T(8,128)(2,1)S(1)}, bf16[4,32,1024]{2,1,0:T(8,128)(2,1)S(1)}, u32[]{:S(2)}, u32[]{:S(2)}) collective-permute-start(bf16[4,32,1024]{2,1,0:T(8,128)(2,1)S(1)} %pad_maximum_fusion.9), channel_id=1, source_target_pairs={{64,0},{65,1},{66,2},{67,3},{68,4},{69,5},{70,6},{71,7},{72,8},{73... | collective-permute-start | bytes 786440 | tf_op jit(solution)/shard_map/ppermute | solution.py:37
  25.7 60.2 %collective-permute-start.3 = (bf16[2,32,4096]{2,1,0:T(8,128)(2,1)S(1)}, bf16[2,32,4096]{2,1,0:T(8,128)(2,1)S(1)}, u32[]{:S(2)}, u32[]{:S(2)}) collective-permute-start(bf16[2,32,4096]{2,1,0:T(8,128)(2,1)S(1)} %pad_maximum_fusion.4.refs_0_), channel_id=1, source_target_pairs={{1,0},{2,1},{3,2},{0,3},{5,4},{6,5},{7,6},{4,7},{9,8},{10,9},{11,1... | collective-permute-start | bytes 1572872 | tf_op jit(solution)/shard_map/ppermute | solution.py:37
  27.6 59.4 %collective-permute-start.4 = (bf16[2,32,4096]{2,1,0:T(8,128)(2,1)S(1)}, bf16[2,32,4096]{2,1,0:T(8,128)(2,1)S(1)}, u32[]{:S(2)}, u32[]{:S(2)}) collective-permute-start(bf16[2,32,4096]{2,1,0:T(8,128)(2,1)S(1)} %constant_dynamic-update-slice_fusion.refs_1_), channel_id=1, source_target_pairs={{1,0},{2,1},{3,2},{0,3},{5,4},{6,5},{7,6},{4,7},{9,8},{10,9},{11,1... | collective-permute-start | bytes 1572872 | tf_op jit(solution)/shard_map/ppermute | solution.py:37
  108.3 65.9 %collective-permute-start.21 = (bf16[1040,1024]{1,0:T(8,128)(2,1)S(1)}, bf16[1040,1024]{1,0:T(8,128)(2,1)S(1)}, u32[]{:S(2)}, u32[]{:S(2)}) collective-permute-start(bf16[1040,1024]{1,0:T(8,128)(2,1)S(1)} %pad_maximum_fusion.refs_20_.refs_5_), channel_id=1, source_target_pairs={{16,0},{17,1},{18,2},{19,3},{20,4},{21,5},{22,6},{23,7},{24,8},{25... | collective-permute-start | bytes 6389768 | tf_op jit(solution)/shard_map/ppermute | solution.py:37
  113.8 63.1 %collective-permute-start.23 = (bf16[1040,1024]{1,0:T(8,128)(2,1)S(1)}, bf16[1040,1024]{1,0:T(8,128)(2,1)S(1)}, u32[]{:S(2)}, u32[]{:S(2)}) collective-permute-start(bf16[1040,1024]{1,0:T(8,128)(2,1)S(1)} %collective-permute-done.22.refs_22_.refs_7_), channel_id=1, source_target_pairs={{16,0},{17,1},{18,2},{19,3},{20,4},{21,5},{22,6},{23,7},{24,8},{25... | collective-permute-start | bytes 6389768 | tf_op jit(solution)/shard_map/ppermute | solution.py:37
  132.1 42.1 %collective-permute-start.18 = (bf16[1024,1024]{1,0:T(8,128)(2,1)S(1)}, bf16[1024,1024]{1,0:T(8,128)(2,1)S(1)}, u32[]{:S(2)}, u32[]{:S(2)}) collective-permute-start(bf16[1024,1024]{1,0:T(8,128)(2,1)S(1)} %pad_maximum_fusion.1.refs_16_.refs_1_), channel_id=1, source_target_pairs={{16,0},{17,1},{18,2},{19,3},{20,4},{21,5},{22,6},{23,7},{24,8},{25... | collective-permute-start | bytes 6291464 | tf_op jit(solution)/shard_map/ppermute | solution.py:37
  135.8 38.4 %collective-permute-start.20 = (bf16[1024,1024]{1,0:T(8,128)(2,1)S(1)}, bf16[1024,1024]{1,0:T(8,128)(2,1)S(1)}, u32[]{:S(2)}, u32[]{:S(2)}) collective-permute-start(bf16[1024,1024]{1,0:T(8,128)(2,1)S(1)} %collective-permute-done.19.refs_18_.refs_3_), channel_id=1, source_target_pairs={{16,0},{17,1},{18,2},{19,3},{20,4},{21,5},{22,6},{23,7},{24,8},{25... | collective-permute-start | bytes 6291464 | tf_op jit(solution)/shard_map/ppermute | solution.py:37
  172.7 48.2 %collective-permute-start.31 = (bf16[4,32,1024]{2,1,0:T(8,128)(2,1)S(1)}, bf16[4,32,1024]{2,1,0:T(8,128)(2,1)S(1)}, u32[]{:S(2)}, u32[]{:S(2)}) collective-permute-start(bf16[4,32,1024]{2,1,0:T(8,128)(2,1)S(1)} %pad_maximum_fusion.8), channel_id=1, source_target_pairs={{32,0},{33,1},{34,2},{35,3},{36,4},{37,5},{38,6},{39,7},{40,8},{41... | collective-permute-start | bytes 786440 | tf_op jit(solution)/shard_map/ppermute | solution.py:37
  216.3 149.0 %all-to-all-start = ((f16[16,32,4224]{2,1,0:T(8,128)(2,1)}), f16[16,32,4224]{2,1,0:T(8,128)(2,1)}, u32[]{:S(2)}, u32[]{:S(2)}) async-start(f16[16,32,4224]{2,1,0:T(8,128)(2,1)} %bitcast.45), calls=%async_computation | async-start | bytes 8650752 | tf_op jit(solution)/shard_map/all_to_all | solution.py:406
  221.0 55.0 %collective-permute-start.34 = (bf16[1,6,32,1024]{3,2,1,0:T(8,128)(2,1)S(1)}, bf16[1,6,32,1024]{3,2,1,0:T(8,128)(2,1)S(1)}, u32[]{:S(2)}, u32[]{:S(2)}) collective-permute-start(bf16[1,6,32,1024]{3,2,1,0:T(8,128)(2,1)S(1)} %maximum_bitcast_fusion), channel_id=1, source_target_pairs={{4,0},{5,1},{6,2},{7,3},{8,4},{9,5},{10,6},{11,7},{12,8},{13,9},{1... | collective-permute-start | bytes 1179656 | tf_op jit(solution)/shard_map/ppermute | solution.py:37
  223.5 55.6 %collective-permute-start.35 = (bf16[1,6,32,1024]{3,2,1,0:T(8,128)(2,1)S(1)}, bf16[1,6,32,1024]{3,2,1,0:T(8,128)(2,1)S(1)}, u32[]{:S(2)}, u32[]{:S(2)}) collective-permute-start(bf16[1,6,32,1024]{3,2,1,0:T(8,128)(2,1)S(1)} %maximum_bitcast_fusion), channel_id=1, source_target_pairs={{8,0},{9,1},{10,2},{11,3},{12,4},{13,5},{14,6},{15,7},{0,8},{1,9},... | collective-permute-start | bytes 1179656 | tf_op jit(solution)/shard_map/ppermute | solution.py:37
  224.0 61.5 %collective-permute-start.36 = (bf16[1,6,32,1024]{3,2,1,0:T(8,128)(2,1)S(1)}, bf16[1,6,32,1024]{3,2,1,0:T(8,128)(2,1)S(1)}, u32[]{:S(2)}, u32[]{:S(2)}) collective-permute-start(bf16[1,6,32,1024]{3,2,1,0:T(8,128)(2,1)S(1)} %maximum_bitcast_fusion), channel_id=1, source_target_pairs={{12,0},{13,1},{14,2},{15,3},{0,4},{1,5},{2,6},{3,7},{4,8},{5,9},{6... | collective-permute-start | bytes 1179656 | tf_op jit(solution)/shard_map/ppermute | solution.py:37
  224.7 64.7 %collective-permute-start.43 = (bf16[1,6,32,1024]{3,2,1,0:T(8,128)(2,1)S(1)}, bf16[1,6,32,1024]{3,2,1,0:T(8,128)(2,1)S(1)}, u32[]{:S(2)}, u32[]{:S(2)}) collective-permute-start(bf16[1,6,32,1024]{3,2,1,0:T(8,128)(2,1)S(1)} %maximum_bitcast_fusion.1), channel_id=1, source_target_pairs={{1,0},{2,1},{3,2},{0,3},{5,4},{6,5},{7,6},{4,7},{9,8},{10,9},{11,1... | collective-permute-start | bytes 1179656 | tf_op jit(solution)/shard_map/ppermute | solution.py:37
  227.2 67.6 %collective-permute-start.44 = (bf16[1,6,32,1024]{3,2,1,0:T(8,128)(2,1)S(1)}, bf16[1,6,32,1024]{3,2,1,0:T(8,128)(2,1)S(1)}, u32[]{:S(2)}, u32[]{:S(2)}) collective-permute-start(bf16[1,6,32,1024]{3,2,1,0:T(8,128)(2,1)S(1)} %maximum_bitcast_fusion.1), channel_id=1, source_target_pairs={{2,0},{3,1},{0,2},{1,3},{6,4},{7,5},{4,6},{5,7},{10,8},{11,9},{8,1... | collective-permute-start | bytes 1179656 | tf_op jit(solution)/shard_map/ppermute | solution.py:37
  276.1 42.5 %collective-permute-start.37 = (bf16[2,6,32,1024]{3,2,1,0:T(8,128)(2,1)S(1)}, bf16[2,6,32,1024]{3,2,1,0:T(8,128)(2,1)S(1)}, u32[]{:S(2)}, u32[]{:S(2)}) collective-permute-start(bf16[2,6,32,1024]{3,2,1,0:T(8,128)(2,1)S(1)} %pad_maximum_fusion.2.refs_8_.refs_4_), channel_id=1, source_target_pairs={{1,0},{2,1},{3,2},{0,3},{5,4},{6,5},{7,6},{4,7},{9,8},{10,9},{11,1... | collective-permute-start | bytes 2359304 | tf_op jit(solution)/shard_map/ppermute | solution.py:37
  285.5 38.5 %collective-permute-start.38 = (bf16[2,6,32,1024]{3,2,1,0:T(8,128)(2,1)S(1)}, bf16[2,6,32,1024]{3,2,1,0:T(8,128)(2,1)S(1)}, u32[]{:S(2)}, u32[]{:S(2)}) collective-permute-start(bf16[2,6,32,1024]{3,2,1,0:T(8,128)(2,1)S(1)} %constant_dynamic-update-slice_fusion.4.refs_9_.refs_5_), channel_id=1, source_target_pairs={{1,0},{2,1},{3,2},{0,3},{5,4},{6,5},{7,6},{4,7},{9,8},{10,9},{11,1... | collective-permute-start | bytes 2359304 | tf_op jit(solution)/shard_map/ppermute | solution.py:37
  289.3 35.3 %collective-permute-start.39 = (bf16[2,6,32,1024]{3,2,1,0:T(8,128)(2,1)S(1)}, bf16[2,6,32,1024]{3,2,1,0:T(8,128)(2,1)S(1)}, u32[]{:S(2)}, u32[]{:S(2)}) collective-permute-start(bf16[2,6,32,1024]{3,2,1,0:T(8,128)(2,1)S(1)} %pad_maximum_fusion.2.refs_8_.refs_4_), channel_id=1, source_target_pairs={{3,0},{0,1},{1,2},{2,3},{7,4},{4,5},{5,6},{6,7},{11,8},{8,9},{9,10... | collective-permute-start | bytes 2359304 | tf_op jit(solution)/shard_map/ppermute | solution.py:37
  294.8 38.3 %collective-permute-start.40 = (bf16[2,6,32,1024]{3,2,1,0:T(8,128)(2,1)S(1)}, bf16[2,6,32,1024]{3,2,1,0:T(8,128)(2,1)S(1)}, u32[]{:S(2)}, u32[]{:S(2)}) collective-permute-start(bf16[2,6,32,1024]{3,2,1,0:T(8,128)(2,1)S(1)} %constant_dynamic-update-slice_fusion.4.refs_9_.refs_5_), channel_id=1, source_target_pairs={{3,0},{0,1},{1,2},{2,3},{7,4},{4,5},{5,6},{6,7},{11,8},{8,9},{9,10... | collective-permute-start | bytes 2359304 | tf_op jit(solution)/shard_map/ppermute | solution.py:37
  324.6 105.8 %collective-permute-start.58 = (bf16[4112,512]{1,0:T(8,128)(2,1)}, bf16[4112,512]{1,0:T(8,128)(2,1)}, u32[]{:S(2)}, u32[]{:S(2)}) collective-permute-start(bf16[4112,512]{1,0:T(8,128)(2,1)} %get-tuple-element.18.refs_0_), channel_id=1, source_target_pairs={{16,0},{17,1},{18,2},{19,3},{20,4},{21,5},{22,6},{23,7},{24,8},{25... | collective-permute-start | bytes 12632072 | tf_op jit(solution)/shard_map/ppermute | solution.py:37
  375.8 40.2 %collective-permute-start.55 = (bf16[1040,512]{1,0:T(8,128)(2,1)}, bf16[1040,512]{1,0:T(8,128)(2,1)}, u32[]{:S(2)}, u32[]{:S(2)}) collective-permute-start(bf16[1040,512]{1,0:T(8,128)(2,1)} %get-tuple-element.19), channel_id=1, source_target_pairs={{96,0},{97,1},{98,2},{99,3},{100,4},{101,5},{102,6},{103,7},{104,8... | collective-permute-start | bytes 3194888 | tf_op jit(solution)/shard_map/ppermute | solution.py:37
  377.7 46.9 %collective-permute-start.27 = (bf16[1024,512]{1,0:T(8,128)(2,1)}, bf16[1024,512]{1,0:T(8,128)(2,1)S(1)}, u32[]{:S(2)}, u32[]{:S(2)}) collective-permute-start(bf16[1024,512]{1,0:T(8,128)(2,1)} %collective-permute-done.26.refs_5_), channel_id=1, source_target_pairs={{96,0},{97,1},{98,2},{99,3},{100,4},{101,5},{102,6},{103,7},{104,8... | collective-permute-start | bytes 3145736 | tf_op jit(solution)/shard_map/ppermute | solution.py:37
  377.7 51.3 %collective-permute-start.54 = (bf16[1024,512]{1,0:T(8,128)(2,1)}, bf16[1024,512]{1,0:T(8,128)(2,1)S(1)}, u32[]{:S(2)}, u32[]{:S(2)}) collective-permute-start(bf16[1024,512]{1,0:T(8,128)(2,1)} %collective-permute-done.52.refs_1_), channel_id=1, source_target_pairs={{16,0},{17,1},{18,2},{19,3},{20,4},{21,5},{22,6},{23,7},{24,8},{25... | collective-permute-start | bytes 3145736 | tf_op jit(solution)/shard_map/ppermute | solution.py:37
  (86 other events, 2638.3 us)

commit v2 on v1

--- a/solution.py
+++ b/solution.py
@@ -59,6 +59,7 @@
 
 
 FROM = ((0, 0), (2, 0), (0, 1), (2, 1), (0, 3), (2, 3), (0, 2), (2, 2))
+WHOLE = (0, 1, 3, 2)
 
 
 def forward_kernel(*refs):
@@ -308,12 +309,12 @@
 
 
 def plane_columns(first_group, count, refs, z, y, add, buf, kind):
-    for i, (first, off) in enumerate(FROM):
-        for j in range(2):
-            a, b = lax.rem(z + first + j, 4), lax.rem(y + off, 4)
+    for i, off in enumerate(WHOLE):
+        for j in range(4):
+            a, b = lax.rem(z + j, 4), lax.rem(y + off, 4)
             if kind:
-                a, b = lax.rem(z + off, 4), lax.rem(y + first + j, 4)
-            add(refs[8 * kind + i].at[j, pl.ds(first_group, count)], buf.at[:, a * 4 + b])
+                a, b = lax.rem(z + off, 4), lax.rem(y + j, 4)
+            add(refs[4 * kind + i].at[j, pl.ds(first_group, count)], buf.at[:, a * 4 + b])
 
 
 def weight_sums(groups, columns, arrays, base):
@@ -366,9 +367,12 @@
     xp, dp = relative(inputs), relative(d_out)
     x_own, d_own = jnp.concatenate(xp, axis=1), jnp.concatenate(dp, axis=1)
 
-    def spread(own, first, second):
+    def spread(own, first, second, whole=False):
         own = own[None]
         one, two, three = (moved(own, **{first: d}) for d in (1, 2, 3))
+        if whole:
+            line = jnp.concatenate([own, one, two, three], axis=0)
+            return (line, *(moved(line, **{second: d}) for d in (1, -1, 2)))
         low, high = jnp.concatenate([own, one], axis=0), jnp.concatenate([two, three], axis=0)
         up_l, up_h = moved(low, **{second: 1}), moved(high, **{second: 1})
         down_l, down_h = moved(low, **{second: -1}), moved(high, **{second: -1})
@@ -382,8 +386,8 @@
     far = jnp.stack([xp[0], side[0], dp[0], side[1]])
     near = jnp.stack([xp[2], side[2], dp[2], side[3]])
     got = (moved(near, dx=1), moved(near, dx=-1), moved(far, dx=2))
-    xcs = spread(jnp.concatenate([v[:2] for v in got], axis=0), "dz", "dy")
-    dcs = spread(jnp.concatenate([v[2:] for v in got], axis=0), "dy", "dz")
+    xcs = spread(jnp.concatenate([v[:2] for v in got], axis=0), "dz", "dy", True)
+    dcs = spread(jnp.concatenate([v[2:] for v in got], axis=0), "dy", "dz", True)
 
     wa = jnp.concatenate([w_gate.T, w_down[:CUT]], axis=0)
     wb = jnp.concatenate([w_up.T, w_down[CUT:]], axis=0)

time: 478 us -> 532 us (1.11)
  the two profiles are of different devices: /device:TPU:1 before, /device:TPU:9 now
where the time goes in v2:
time: 532 us; the launch traced here: 531 us
  waiting for transfers between devices  345 us (65%)
  starting transfers between devices  80.4 us (15%)
  Pallas kernels  69.3 us (13%)
  other arithmetic  23.9 us (4%)
  local copies, waits for them, and re-layouts  11 us (2%)
    ppermute x53, waiting for transfers between devices, moved(): return lax.ppermute(array, AXES, pairs)  345 us
    ppermute x53, starting transfers between devices, moved(): return lax.ppermute(array, AXES, pairs)  73.5 us
    pallas_call x5, Pallas kernels, call(): pl.pallas_call(body, out_shape=out_shape, in_specs=ins, out_specs=outs, s...  69.3 us
    convert_element_type x1, other arithmetic, block(): grad_inputs = jnp.concatenate(relative(total.astype(BF), mark), axis=1)  12.9 us
  transfers between devices with their start and end apart: 54, of which 20 were waited for; matrix products, arithmetic and copies ran while one was open for 5% of the time, Pallas kernels for 11%

profile of v2, /device:TPU:9, one launch (start us, length us, event | category | flops | bytes accessed | tf_op | source)
XLA Modules:
  0.0 531.4 jit_solution(13236329378235000886)
XLA Ops:
  26.7 49.6 %collective-permute-done.33 = bf16[4,32,1024]{2,1,0:T(8,128)(2,1)S(1)} collective-permute-done((bf16[4,32,1024]{2,1,0:T(8,128)(2,1)S(1)}, bf16[4,32,1024]{2,1,0:T(8,128)(2,1)S(1)}, u32[]{:S(2)}, u32[]{:S(2)}) %collective-permute-start.33) | collective-permute-done | bytes 262176 | tf_op jit(solution)/shard_map/ppermute | solution.py:37
  76.5 6.3 %collective-permute-done.32 = bf16[4,32,1024]{2,1,0:T(8,128)(2,1)S(1)} collective-permute-done((bf16[4,32,1024]{2,1,0:T(8,128)(2,1)S(1)}, bf16[4,32,1024]{2,1,0:T(8,128)(2,1)S(1)}, u32[]{:S(2)}, u32[]{:S(2)}) %collective-permute-start.32) | collective-permute-done | bytes 262176 | tf_op jit(solution)/shard_map/ppermute | solution.py:37
  83.0 6.3 %collective-permute-done.31 = bf16[4,32,1024]{2,1,0:T(8,128)(2,1)S(1)} collective-permute-done((bf16[4,32,1024]{2,1,0:T(8,128)(2,1)S(1)}, bf16[4,32,1024]{2,1,0:T(8,128)(2,1)S(1)}, u32[]{:S(2)}, u32[]{:S(2)}) %collective-permute-start.31) | collective-permute-done | bytes 262176 | tf_op jit(solution)/shard_map/ppermute | solution.py:37
  93.8 6.5 %collective-permute-done.5.refs_4_ = bf16[2,32,4096]{2,1,0:T(8,128)(2,1)S(1)} collective-permute-done((bf16[2,32,4096]{2,1,0:T(8,128)(2,1)S(1)}, bf16[2,32,4096]{2,1,0:T(8,128)(2,1)S(1)}, u32[]{:S(2)}, u32[]{:S(2)}) %collective-permute-start.5) | collective-permute-done | bytes 524320 | tf_op jit(solution)/shard_map/ppermute | solution.py:37
  103.8 7.8 %collective-permute-done.6.refs_5_ = bf16[2,32,4096]{2,1,0:T(8,128)(2,1)S(1)} collective-permute-done((bf16[2,32,4096]{2,1,0:T(8,128)(2,1)S(1)}, bf16[2,32,4096]{2,1,0:T(8,128)(2,1)S(1)}, u32[]{:S(2)}, u32[]{:S(2)}) %collective-permute-start.6) | collective-permute-done | bytes 524320 | tf_op jit(solution)/shard_map/ppermute | solution.py:37
  113.2 10.9 %collective-permute-done.14.refs_12_ = bf16[2,32,4096]{2,1,0:T(8,128)(2,1)S(1)} collective-permute-done((bf16[2,32,4096]{2,1,0:T(8,128)(2,1)S(1)}, bf16[2,32,4096]{2,1,0:T(8,128)(2,1)S(1)}, u32[]{:S(2)}, u32[]{:S(2)}) %collective-permute-start.14) | collective-permute-done | bytes 524320 | tf_op jit(solution)/shard_map/ppermute | solution.py:37
  124.1 7.2 %collective-permute-start.21 = (bf16[1040,1024]{1,0:T(8,128)(2,1)S(1)}, bf16[1040,1024]{1,0:T(8,128)(2,1)S(1)}, u32[]{:S(2)}, u32[]{:S(2)}) collective-permute-start(bf16[1040,1024]{1,0:T(8,128)(2,1)S(1)} %pad_maximum_fusion.refs_20_.refs_5_), channel_id=1, source_target_pairs={{16,0},{17,1},{18,2},{19,3},{20,4},{21,5},{22,6},{23,7},{24,8},{25... | collective-permute-start | bytes 6389768 | tf_op jit(solution)/shard_map/ppermute | solution.py:37
  140.2 12.1 %collective-permute-done.8.refs_7_ = bf16[2,32,4096]{2,1,0:T(8,128)(2,1)S(1)} collective-permute-done((bf16[2,32,4096]{2,1,0:T(8,128)(2,1)S(1)}, bf16[2,32,4096]{2,1,0:T(8,128)(2,1)S(1)}, u32[]{:S(2)}, u32[]{:S(2)}) %collective-permute-start.8) | collective-permute-done | bytes 524320 | tf_op jit(solution)/shard_map/ppermute | solution.py:37
  153.8 10.7 %collective-permute-done.16.refs_14_ = bf16[2,32,4096]{2,1,0:T(8,128)(2,1)S(1)} collective-permute-done((bf16[2,32,4096]{2,1,0:T(8,128)(2,1)S(1)}, bf16[2,32,4096]{2,1,0:T(8,128)(2,1)S(1)}, u32[]{:S(2)}, u32[]{:S(2)}) %collective-permute-start.16) | collective-permute-done | bytes 524320 | tf_op jit(solution)/shard_map/ppermute | solution.py:37
  164.7 12.4 %collective-permute-done.17.refs_15_ = bf16[2,32,4096]{2,1,0:T(8,128)(2,1)S(1)} collective-permute-done((bf16[2,32,4096]{2,1,0:T(8,128)(2,1)S(1)}, bf16[2,32,4096]{2,1,0:T(8,128)(2,1)S(1)}, u32[]{:S(2)}, u32[]{:S(2)}) %collective-permute-start.17) | collective-permute-done | bytes 524320 | tf_op jit(solution)/shard_map/ppermute | solution.py:37
  183.1 19.4 %shard_map.84 = (bf16[1040,512]{1,0:T(8,128)(2,1)}, bf16[1024,512]{1,0:T(8,128)(2,1)}, bf16[4112,512]{1,0:T(8,128)(2,1)}, bf16[512,1024]{1,0:T(8,128)(2,1)}, bf16[512,1024]{1,0:T(8,128)(2,1)}) custom-call(bf16[2,32,4096]{2,1,0:T(8,128)(2,1)} %copy-done.21, bf16[2,32,4096]{2,1,0:T(8,128)(2,1)} %copy-done.23, bf16[2,32,4096]{2,1,0:T(8,128)(2,1)} %copy-done.29, ...), custom_call_target="tpu_custom_call" | custom-call | flops 8657043456 | bytes 35651584 | tf_op jit(solution)/shard_map/pallas_call | solution.py:50
  202.5 12.7 %shard_map.85 = f32[512,4224]{1,0:T(8,128)} custom-call(bf16[4112,512]{1,0:T(8,128)(2,1)} %get-tuple-element.18.refs_0_, bf16[1024,1024]{1,0:T(8,128)(2,1)} %copy-done.1, bf16[1024,1024]{1,0:T(8,128)(2,1)} %copy-done.8, bf16[1024,1024]{1,0:T(8,128)(2,1)} %copy-done.7, bf16[1024,1024]{1,0:T(8,128)(2,1)} %copy-done.9, bf16[1040,1024]{1,0:T(8,128)(2,1)} %copy-done, ...), custom_call_target="tpu_custom_call" | custom-call | flops 5771362304 | bytes 23068672 | tf_op jit(solution)/shard_map/pallas_call | solution.py:50
  221.2 6.9 %all-to-all-start = ((f16[16,32,4224]{2,1,0:T(8,128)(2,1)}), f16[16,32,4224]{2,1,0:T(8,128)(2,1)}, u32[]{:S(2)}, u32[]{:S(2)}) async-start(f16[16,32,4224]{2,1,0:T(8,128)(2,1)} %bitcast.45), calls=%async_computation | async-start | bytes 8650752 | tf_op jit(solution)/shard_map/all_to_all | solution.py:410
  235.5 59.6 %collective-permute-done.42 = bf16[1,6,32,1024]{3,2,1,0:T(8,128)(2,1)S(1)} collective-permute-done((bf16[1,6,32,1024]{3,2,1,0:T(8,128)(2,1)S(1)}, bf16[1,6,32,1024]{3,2,1,0:T(8,128)(2,1)S(1)}, u32[]{:S(2)}, u32[]{:S(2)}) %collective-permute-start.42) | collective-permute-done | bytes 393248 | tf_op jit(solution)/shard_map/ppermute | solution.py:37
  295.1 25.9 %collective-permute-done.41 = bf16[1,6,32,1024]{3,2,1,0:T(8,128)(2,1)S(1)} collective-permute-done((bf16[1,6,32,1024]{3,2,1,0:T(8,128)(2,1)S(1)}, bf16[1,6,32,1024]{3,2,1,0:T(8,128)(2,1)S(1)}, u32[]{:S(2)}, u32[]{:S(2)}) %collective-permute-start.41) | collective-permute-done | bytes 393248 | tf_op jit(solution)/shard_map/ppermute | solution.py:37
  321.1 47.0 %collective-permute-done.40 = bf16[1,6,32,1024]{3,2,1,0:T(8,128)(2,1)S(1)} collective-permute-done((bf16[1,6,32,1024]{3,2,1,0:T(8,128)(2,1)S(1)}, bf16[1,6,32,1024]{3,2,1,0:T(8,128)(2,1)S(1)}, u32[]{:S(2)}, u32[]{:S(2)}) %collective-permute-start.40) | collective-permute-done | bytes 393248 | tf_op jit(solution)/shard_map/ppermute | solution.py:37
  374.5 28.7 %collective-permute-done.43.refs_13_.refs_9_ = bf16[4,6,32,1024]{3,2,1,0:T(8,128)(2,1)S(1)} collective-permute-done((bf16[4,6,32,1024]{3,2,1,0:T(8,128)(2,1)S(1)}, bf16[4,6,32,1024]{3,2,1,0:T(8,128)(2,1)S(1)}, u32[]{:S(2)}, u32[]{:S(2)}) %collective-permute-start.43) | collective-permute-done | bytes 1572896 | tf_op jit(solution)/shard_map/ppermute | solution.py:37
  408.6 30.9 %collective-permute-done.45.refs_15_.refs_11_ = bf16[4,6,32,1024]{3,2,1,0:T(8,128)(2,1)} collective-permute-done((bf16[4,6,32,1024]{3,2,1,0:T(8,128)(2,1)S(1)}, bf16[4,6,32,1024]{3,2,1,0:T(8,128)(2,1)}, u32[]{:S(2)}, u32[]{:S(2)}) %collective-permute-start.45) | collective-permute-done | bytes 1572896 | tf_op jit(solution)/shard_map/ppermute | solution.py:37
  450.3 12.9 %fusion = bf16[32,4096]{1,0:T(8,128)(2,1)S(1)} fusion(f16[16,32,4224]{2,1,0:T(8,128)(2,1)} %all-to-all-done, f32[]{:T(128)} %bitcast.22, f32[]{:T(128)} %bitcast.20, f32[]{:T(128)} %bitcast.19, f32[]{:T(128)} %bitcast.18, f32[]{:T(128)} %bitcast.17, f32[]{:T(128)} %bitcast.16, f32[]{:T(128)} %bitcast.15, f32[]{:T(128)} %bitcast.14, f32[]{:T(128)} %bitcast.13, ...), kind=kLoop, calls=%fused_computation.7 | loop fusion | flops 6291456 | bytes 4456512 | tf_op jit(solution)/shard_map/convert_element_type | solution.py:415
  463.7 6.0 %collective-permute-start.51 = (bf16[1024,512]{1,0:T(8,128)(2,1)}, bf16[1024,512]{1,0:T(8,128)(2,1)S(1)}, u32[]{:S(2)}, u32[]{:S(2)}) collective-permute-start(bf16[1024,512]{1,0:T(8,128)(2,1)} %collective-permute-done.26.refs_5_), channel_id=1, source_target_pairs={{16,0},{17,1},{18,2},{19,3},{20,4},{21,5},{22,6},{23,7},{24,8},{25... | collective-permute-start | bytes 3145736 | tf_op jit(solution)/shard_map/ppermute | solution.py:37
  469.7 16.4 %collective-permute-done.27.refs_1_ = bf16[1024,512]{1,0:T(8,128)(2,1)S(1)} collective-permute-done((bf16[1024,512]{1,0:T(8,128)(2,1)}, bf16[1024,512]{1,0:T(8,128)(2,1)S(1)}, u32[]{:S(2)}, u32[]{:S(2)}) %collective-permute-start.27) | collective-permute-done | bytes 1048608 | tf_op jit(solution)/shard_map/ppermute | solution.py:37
  490.8 9.6 %shard_map.86 = (f32[688,1024]{1,0:T(8,128)}, f32[688,1024]{1,0:T(8,128)}, f32[688,1024]{1,0:T(8,128)}) custom-call(bf16[4112,512]{1,0:T(8,128)(2,1)} %get-tuple-element.18.refs_0_, bf16[4112,512]{1,0:T(8,128)(2,1)} %collective-permute-done.52.refs_1_.refs_4_, bf16[512,1024]{1,0:T(8,128)(2,1)} %get-tuple-element.21.refs_2_, ...), custom_call_target="tpu_custom_call" | custom-call | flops 4328521728 | bytes 25165824 | tf_op jit(solution)/shard_map/pallas_call | solution.py:50
  502.2 16.8 %shard_map.87 = (f32[688,1024]{1,0:T(8,128)}, f32[688,1024]{1,0:T(8,128)}, f32[688,1024]{1,0:T(8,128)}) custom-call(bf16[1040,512]{1,0:T(8,128)(2,1)} %collective-permute-done.24.refs_0_, bf16[1024,512]{1,0:T(8,128)(2,1)} %collective-permute-done.46.refs_1_, bf16[1040,512]{1,0:T(8,128)(2,1)} %copy-done.25, bf16[1024,512]{1,0:T(8,128)(2,1)} %copy-done.27, ...), custom_call_target="tpu_custom_call" | custom-call | flops 8657043456 | bytes 33554432 | tf_op jit(solution)/shard_map/pallas_call | solution.py:50
  520.3 10.9 %shard_map.88 = (f32[688,1024]{1,0:T(8,128)}, f32[688,1024]{1,0:T(8,128)}, f32[688,1024]{1,0:T(8,128)}) custom-call(bf16[1040,512]{1,0:T(8,128)(2,1)} %copy-done.17, bf16[1024,512]{1,0:T(8,128)(2,1)} %copy-done.19, bf16[1040,512]{1,0:T(8,128)(2,1)} %copy-done.18, bf16[1024,512]{1,0:T(8,128)(2,1)} %copy-done.20, bf16[4,6,32,1024]{3,2,1,0:T(8,128)(2,1)} %copy-done.2, ...), custom_call_target="tpu_custom_call" | custom-call | flops 4328521728 | bytes 25165824 | tf_op jit(solution)/shard_map/pallas_call | solution.py:50
  (206 shorter events, 96.4 us)
Async XLA Ops:
  20.5 118.6 %collective-permute-start.19 = (bf16[1024,1024]{1,0:T(8,128)(2,1)S(1)}, bf16[1024,1024]{1,0:T(8,128)(2,1)S(1)}, u32[]{:S(2)}, u32[]{:S(2)}) collective-permute-start(bf16[1024,1024]{1,0:T(8,128)(2,1)S(1)} %pad_maximum_fusion.1.refs_16_.refs_1_), channel_id=1, source_target_pairs={{32,0},{33,1},{34,2},{35,3},{36,4},{37,5},{38,6},{39,7},{40,8},{41... | collective-permute-start | bytes 6291464 | tf_op jit(solution)/shard_map/ppermute | solution.py:37
  23.1 108.2 %collective-permute-start.22 = (bf16[1040,1024]{1,0:T(8,128)(2,1)S(1)}, bf16[1040,1024]{1,0:T(8,128)(2,1)S(1)}, u32[]{:S(2)}, u32[]{:S(2)}) collective-permute-start(bf16[1040,1024]{1,0:T(8,128)(2,1)S(1)} %pad_maximum_fusion.refs_20_.refs_5_), channel_id=1, source_target_pairs={{96,0},{97,1},{98,2},{99,3},{100,4},{101,5},{102,6},{103,7},{104,8... | collective-permute-start | bytes 6389768 | tf_op jit(solution)/shard_map/ppermute | solution.py:37
  23.2 53.1 %collective-permute-start.33 = (bf16[4,32,1024]{2,1,0:T(8,128)(2,1)S(1)}, bf16[4,32,1024]{2,1,0:T(8,128)(2,1)S(1)}, u32[]{:S(2)}, u32[]{:S(2)}) collective-permute-start(bf16[4,32,1024]{2,1,0:T(8,128)(2,1)S(1)} %pad_maximum_fusion.9), channel_id=1, source_target_pairs={{64,0},{65,1},{66,2},{67,3},{68,4},{69,5},{70,6},{71,7},{72,8},{73... | collective-permute-start | bytes 786440 | tf_op jit(solution)/shard_map/ppermute | solution.py:37
  24.9 57.9 %collective-permute-start.32 = (bf16[4,32,1024]{2,1,0:T(8,128)(2,1)S(1)}, bf16[4,32,1024]{2,1,0:T(8,128)(2,1)S(1)}, u32[]{:S(2)}, u32[]{:S(2)}) collective-permute-start(bf16[4,32,1024]{2,1,0:T(8,128)(2,1)S(1)} %pad_maximum_fusion.8), channel_id=1, source_target_pairs={{96,0},{97,1},{98,2},{99,3},{100,4},{101,5},{102,6},{103,7},{104,8... | collective-permute-start | bytes 786440 | tf_op jit(solution)/shard_map/ppermute | solution.py:37
  26.5 63.7 %collective-permute-start.3 = (bf16[2,32,4096]{2,1,0:T(8,128)(2,1)S(1)}, bf16[2,32,4096]{2,1,0:T(8,128)(2,1)S(1)}, u32[]{:S(2)}, u32[]{:S(2)}) collective-permute-start(bf16[2,32,4096]{2,1,0:T(8,128)(2,1)S(1)} %pad_maximum_fusion.4.refs_0_), channel_id=1, source_target_pairs={{1,0},{2,1},{3,2},{0,3},{5,4},{6,5},{7,6},{4,7},{9,8},{10,9},{11,1... | collective-permute-start | bytes 1572872 | tf_op jit(solution)/shard_map/ppermute | solution.py:37
  124.1 55.7 %collective-permute-start.21 = (bf16[1040,1024]{1,0:T(8,128)(2,1)S(1)}, bf16[1040,1024]{1,0:T(8,128)(2,1)S(1)}, u32[]{:S(2)}, u32[]{:S(2)}) collective-permute-start(bf16[1040,1024]{1,0:T(8,128)(2,1)S(1)} %pad_maximum_fusion.refs_20_.refs_5_), channel_id=1, source_target_pairs={{16,0},{17,1},{18,2},{19,3},{20,4},{21,5},{22,6},{23,7},{24,8},{25... | collective-permute-start | bytes 6389768 | tf_op jit(solution)/shard_map/ppermute | solution.py:37
  131.3 50.5 %collective-permute-start.23 = (bf16[1040,1024]{1,0:T(8,128)(2,1)S(1)}, bf16[1040,1024]{1,0:T(8,128)(2,1)S(1)}, u32[]{:S(2)}, u32[]{:S(2)}) collective-permute-start(bf16[1040,1024]{1,0:T(8,128)(2,1)S(1)} %collective-permute-done.22.refs_22_.refs_7_), channel_id=1, source_target_pairs={{16,0},{17,1},{18,2},{19,3},{20,4},{21,5},{22,6},{23,7},{24,8},{25... | collective-permute-start | bytes 6389768 | tf_op jit(solution)/shard_map/ppermute | solution.py:37
  135.3 41.8 %collective-permute-start.18 = (bf16[1024,1024]{1,0:T(8,128)(2,1)S(1)}, bf16[1024,1024]{1,0:T(8,128)(2,1)S(1)}, u32[]{:S(2)}, u32[]{:S(2)}) collective-permute-start(bf16[1024,1024]{1,0:T(8,128)(2,1)S(1)} %pad_maximum_fusion.1.refs_16_.refs_1_), channel_id=1, source_target_pairs={{16,0},{17,1},{18,2},{19,3},{20,4},{21,5},{22,6},{23,7},{24,8},{25... | collective-permute-start | bytes 6291464 | tf_op jit(solution)/shard_map/ppermute | solution.py:37
  177.1 50.9 %collective-permute-start.36 = (bf16[1,6,32,1024]{3,2,1,0:T(8,128)(2,1)S(1)}, bf16[1,6,32,1024]{3,2,1,0:T(8,128)(2,1)S(1)}, u32[]{:S(2)}, u32[]{:S(2)}) collective-permute-start(bf16[1,6,32,1024]{3,2,1,0:T(8,128)(2,1)S(1)} %maximum_bitcast_fusion), channel_id=1, source_target_pairs={{12,0},{13,1},{14,2},{15,3},{0,4},{1,5},{2,6},{3,7},{4,8},{5,9},{6... | collective-permute-start | bytes 1179656 | tf_op jit(solution)/shard_map/ppermute | solution.py:37
  177.1 50.9 %collective-permute-start.35 = (bf16[1,6,32,1024]{3,2,1,0:T(8,128)(2,1)S(1)}, bf16[1,6,32,1024]{3,2,1,0:T(8,128)(2,1)}, u32[]{:S(2)}, u32[]{:S(2)}) collective-permute-start(bf16[1,6,32,1024]{3,2,1,0:T(8,128)(2,1)S(1)} %maximum_bitcast_fusion), channel_id=1, source_target_pairs={{8,0},{9,1},{10,2},{11,3},{12,4},{13,5},{14,6},{15,7},{0,8},{1,9},... | collective-permute-start | bytes 1179656 | tf_op jit(solution)/shard_map/ppermute | solution.py:37
  179.8 48.3 %collective-permute-start.34 = (bf16[1,6,32,1024]{3,2,1,0:T(8,128)(2,1)S(1)}, bf16[1,6,32,1024]{3,2,1,0:T(8,128)(2,1)}, u32[]{:S(2)}, u32[]{:S(2)}) collective-permute-start(bf16[1,6,32,1024]{3,2,1,0:T(8,128)(2,1)S(1)} %maximum_bitcast_fusion), channel_id=1, source_target_pairs={{4,0},{5,1},{6,2},{7,3},{8,4},{9,5},{10,6},{11,7},{12,8},{13,9},{1... | collective-permute-start | bytes 1179656 | tf_op jit(solution)/shard_map/ppermute | solution.py:37
  221.2 186.6 %all-to-all-start = ((f16[16,32,4224]{2,1,0:T(8,128)(2,1)}), f16[16,32,4224]{2,1,0:T(8,128)(2,1)}, u32[]{:S(2)}, u32[]{:S(2)}) async-start(f16[16,32,4224]{2,1,0:T(8,128)(2,1)} %bitcast.45), calls=%async_computation | async-start | bytes 8650752 | tf_op jit(solution)/shard_map/all_to_all | solution.py:410
  229.4 140.4 %collective-permute-start.37 = (bf16[4,6,32,1024]{3,2,1,0:T(8,128)(2,1)S(1)}, bf16[4,6,32,1024]{3,2,1,0:T(8,128)(2,1)S(1)}, u32[]{:S(2)}, u32[]{:S(2)}) collective-permute-start(bf16[4,6,32,1024]{3,2,1,0:T(8,128)(2,1)S(1)} %pad_maximum_fusion.2.refs_8_.refs_4_), channel_id=1, source_target_pairs={{1,0},{2,1},{3,2},{0,3},{5,4},{6,5},{7,6},{4,7},{9,8},{10,9},{11,1... | collective-permute-start | bytes 4718600 | tf_op jit(solution)/shard_map/ppermute | solution.py:37
  229.8 65.3 %collective-permute-start.42 = (bf16[1,6,32,1024]{3,2,1,0:T(8,128)(2,1)S(1)}, bf16[1,6,32,1024]{3,2,1,0:T(8,128)(2,1)S(1)}, u32[]{:S(2)}, u32[]{:S(2)}) collective-permute-start(bf16[1,6,32,1024]{3,2,1,0:T(8,128)(2,1)S(1)} %maximum_bitcast_fusion.1), channel_id=1, source_target_pairs={{3,0},{0,1},{1,2},{2,3},{7,4},{4,5},{5,6},{6,7},{11,8},{8,9},{9,10... | collective-permute-start | bytes 1179656 | tf_op jit(solution)/shard_map/ppermute | solution.py:37
  231.0 90.0 %collective-permute-start.41 = (bf16[1,6,32,1024]{3,2,1,0:T(8,128)(2,1)S(1)}, bf16[1,6,32,1024]{3,2,1,0:T(8,128)(2,1)S(1)}, u32[]{:S(2)}, u32[]{:S(2)}) collective-permute-start(bf16[1,6,32,1024]{3,2,1,0:T(8,128)(2,1)S(1)} %maximum_bitcast_fusion.1), channel_id=1, source_target_pairs={{2,0},{3,1},{0,2},{1,3},{6,4},{7,5},{4,6},{5,7},{10,8},{11,9},{8,1... | collective-permute-start | bytes 1179656 | tf_op jit(solution)/shard_map/ppermute | solution.py:37
  234.1 134.0 %collective-permute-start.40 = (bf16[1,6,32,1024]{3,2,1,0:T(8,128)(2,1)S(1)}, bf16[1,6,32,1024]{3,2,1,0:T(8,128)(2,1)S(1)}, u32[]{:S(2)}, u32[]{:S(2)}) collective-permute-start(bf16[1,6,32,1024]{3,2,1,0:T(8,128)(2,1)S(1)} %maximum_bitcast_fusion.1), channel_id=1, source_target_pairs={{1,0},{2,1},{3,2},{0,3},{5,4},{6,5},{7,6},{4,7},{9,8},{10,9},{11,1... | collective-permute-start | bytes 1179656 | tf_op jit(solution)/shard_map/ppermute | solution.py:37
  234.1 137.5 %collective-permute-start.38 = (bf16[4,6,32,1024]{3,2,1,0:T(8,128)(2,1)S(1)}, bf16[4,6,32,1024]{3,2,1,0:T(8,128)(2,1)S(1)}, u32[]{:S(2)}, u32[]{:S(2)}) collective-permute-start(bf16[4,6,32,1024]{3,2,1,0:T(8,128)(2,1)S(1)} %pad_maximum_fusion.2.refs_8_.refs_4_), channel_id=1, source_target_pairs={{3,0},{0,1},{1,2},{2,3},{7,4},{4,5},{5,6},{6,7},{11,8},{8,9},{9,10... | collective-permute-start | bytes 4718600 | tf_op jit(solution)/shard_map/ppermute | solution.py:37
  295.1 79.3 %collective-permute-start.39 = (bf16[4,6,32,1024]{3,2,1,0:T(8,128)(2,1)S(1)}, bf16[4,6,32,1024]{3,2,1,0:T(8,128)(2,1)S(1)}, u32[]{:S(2)}, u32[]{:S(2)}) collective-permute-start(bf16[4,6,32,1024]{3,2,1,0:T(8,128)(2,1)S(1)} %pad_maximum_fusion.2.refs_8_.refs_4_), channel_id=1, source_target_pairs={{2,0},{3,1},{0,2},{1,3},{6,4},{7,5},{4,6},{5,7},{10,8},{11,9},{8,1... | collective-permute-start | bytes 4718600 | tf_op jit(solution)/shard_map/ppermute | solution.py:37
  369.8 120.9 %collective-permute-start.52 = (bf16[4112,512]{1,0:T(8,128)(2,1)}, bf16[4112,512]{1,0:T(8,128)(2,1)}, u32[]{:S(2)}, u32[]{:S(2)}) collective-permute-start(bf16[4112,512]{1,0:T(8,128)(2,1)} %get-tuple-element.18.refs_0_), channel_id=1, source_target_pairs={{16,0},{17,1},{18,2},{19,3},{20,4},{21,5},{22,6},{23,7},{24,8},{25... | collective-permute-start | bytes 12632072 | tf_op jit(solution)/shard_map/ppermute | solution.py:37
  371.6 67.9 %collective-permute-start.45 = (bf16[4,6,32,1024]{3,2,1,0:T(8,128)(2,1)S(1)}, bf16[4,6,32,1024]{3,2,1,0:T(8,128)(2,1)}, u32[]{:S(2)}, u32[]{:S(2)}) collective-permute-start(bf16[4,6,32,1024]{3,2,1,0:T(8,128)(2,1)S(1)} %pad_maximum_fusion.3.refs_12_.refs_8_), channel_id=1, source_target_pairs={{8,0},{9,1},{10,2},{11,3},{12,4},{13,5},{14,6},{15,7},{0,8},{1,9},... | collective-permute-start | bytes 4718600 | tf_op jit(solution)/shard_map/ppermute | solution.py:37
  374.4 65.0 %collective-permute-start.26 = (bf16[1024,512]{1,0:T(8,128)(2,1)}, bf16[1024,512]{1,0:T(8,128)(2,1)}, u32[]{:S(2)}, u32[]{:S(2)}) collective-permute-start(bf16[1024,512]{1,0:T(8,128)(2,1)} %get-tuple-element.20), channel_id=1, source_target_pairs={{96,0},{97,1},{98,2},{99,3},{100,4},{101,5},{102,6},{103,7},{104,8... | collective-permute-start | bytes 3145736 | tf_op jit(solution)/shard_map/ppermute | solution.py:37
  439.5 46.6 %collective-permute-start.27 = (bf16[1024,512]{1,0:T(8,128)(2,1)}, bf16[1024,512]{1,0:T(8,128)(2,1)S(1)}, u32[]{:S(2)}, u32[]{:S(2)}) collective-permute-start(bf16[1024,512]{1,0:T(8,128)(2,1)} %collective-permute-done.26.refs_5_), channel_id=1, source_target_pairs={{96,0},{97,1},{98,2},{99,3},{100,4},{101,5},{102,6},{103,7},{104,8... | collective-permute-start | bytes 3145736 | tf_op jit(solution)/shard_map/ppermute | solution.py:37
  439.5 49.8 %collective-permute-start.48 = (bf16[1024,512]{1,0:T(8,128)(2,1)}, bf16[1024,512]{1,0:T(8,128)(2,1)S(1)}, u32[]{:S(2)}, u32[]{:S(2)}) collective-permute-start(bf16[1024,512]{1,0:T(8,128)(2,1)} %collective-permute-done.46.refs_1_), channel_id=1, source_target_pairs={{16,0},{17,1},{18,2},{19,3},{20,4},{21,5},{22,6},{23,7},{24,8},{25... | collective-permute-start | bytes 3145736 | tf_op jit(solution)/shard_map/ppermute | solution.py:37
  447.3 43.0 %collective-permute-start.25 = (bf16[1040,512]{1,0:T(8,128)(2,1)}, bf16[1040,512]{1,0:T(8,128)(2,1)S(1)}, u32[]{:S(2)}, u32[]{:S(2)}) collective-permute-start(bf16[1040,512]{1,0:T(8,128)(2,1)} %collective-permute-done.24.refs_0_), channel_id=1, source_target_pairs={{32,0},{33,1},{34,2},{35,3},{36,4},{37,5},{38,6},{39,7},{40,8},{41... | collective-permute-start | bytes 3194888 | tf_op jit(solution)/shard_map/ppermute | solution.py:37
  (73 other events, 2325.1 us)

commit v3 on v2

--- a/solution.py
+++ b/solution.py
@@ -19,6 +19,7 @@
 TOK, WIDE = 16 * ROWS, 4 * DEPTH
 CUT = 336
 LOW, HIGH = 1040, 1024
+HALF = 2 * DEPTH
 TAIL = 128
 
 
@@ -98,21 +99,10 @@
 
     begin(0)
     begin(1)
+    sums[...] = jnp.zeros_like(sums)
     end(0)
     begin(2)
 
-    def initial(i, _):
-        @pl.when(i == 2)
-        def _():
-            end(1)
-            begin(3)
-
-        sums[i] = dot(w[0, i], v[i // 2, :, :DEPTH], 1, 1)
-        return 0
-
-    lax.fori_loop(0, 3, initial, 0)
-    end(2)
-    begin(4)
     outs = []
     for i, to in enumerate((x_own, d_own)):
         outs.append(pltpu.make_async_copy(v.at[i, :, pl.ds(0, DEPTH)], to, so.at[i]))
@@ -120,18 +110,34 @@
             outs.append(pltpu.make_async_copy(
                 v.at[i, :, pl.ds(DEPTH + h * TOK, TOK)],
                 side.at[pl.ds(3 * UNITS + (2 * i + h) * TOK, TOK)], so.at[2 + 2 * i + h]))
-    for k in (1, 2, 3):
-        if k > 1:
-            end(k + 1)
-        if k == 3:
+
+    def product(n, _):
+        k, i = n // 3, lax.rem(n, 3)
+
+        @pl.when(n == 2)
+        def _():
+            end(1)
+            begin(3)
+
+        @pl.when(n == 3)
+        def _():
+            end(2)
+            begin(4)
+
+        @pl.when(n == 6)
+        def _():
+            end(3)
+
+        @pl.when(n == 9)
+        def _():
+            end(4)
             for c in outs:
                 c.start()
 
-        def product(i, _):
-            sums[i] = sums[i] + dot(w[k, i], v[i // 2, :, k * DEPTH:(k + 1) * DEPTH], 1, 1)
-            return 0
-
-        lax.fori_loop(0, 3, product, 0)
+        sums[i] = sums[i] + dot(w[k, i], v[i // 2, :, pl.ds(pl.multiple_of(k * DEPTH, DEPTH), DEPTH)], 1, 1)
+        return 0
+
+    lax.fori_loop(0, 12, product, 0)
 
     def unit(i, _):
         r = pl.ds(pl.multiple_of(i * 16, 16), 16)
@@ -176,9 +182,11 @@
 
 
 def input_kernel(*refs):
-    acts, was, wbs, out = refs[0], refs[1:5], refs[5:9], refs[9]
-    act, wa, wb, tg, tu, total, expo, sw, so = refs[10:]
-    load = pltpu.make_async_copy(acts.at[pl.ds(0, 2 * UNITS)], act, so.at[5])
+    acts, was, wbs = refs[0], refs[1:5], refs[5:9]
+    own, away = refs[9:11], refs[11:13]
+    act, wa, wb, tg, tu, total, expo, sw, so, st, sl = refs[13:]
+    z, y = place()
+    load = pltpu.make_async_copy(acts.at[pl.ds(0, 2 * UNITS)], act, sl.at[0])
     load.start()
     copies = [
         (pltpu.make_async_copy(was[k].at[pl.ds(0, UNITS)], wa.at[k], sw.at[2 * k]),
@@ -195,13 +203,24 @@
     norm = norm + jnp.sum(jnp.abs(tu[...].astype(F32)), axis=1, keepdims=True)
     e = jnp.ceil(jnp.log2(jnp.maximum(jnp.max(norm, axis=0, keepdims=True) * (1.02 * W_MAX), 1e-30)))
     expo[...] = jnp.broadcast_to(e, (TOK, TAIL))
-    tail = pltpu.make_async_copy(expo, out.at[:, pl.ds(WIDE, TAIL)], so.at[4])
-    tail.start()
-
-    def put(k):
-        at = k * DEPTH if isinstance(k, int) else pl.multiple_of(k * DEPTH, DEPTH)
-        return pltpu.make_async_copy(total.at[k % 2 if isinstance(k, int) else lax.rem(k, 2)],
-                                     out.at[:, pl.ds(at, DEPTH)], so.at[k])
+
+    def puts(src, side, cols, sems):
+        out = []
+        for s in range(4):
+            to = own[side] if s == 0 else away[side].at[s - 1]
+            if side == 0:
+                r = pl.ds(pl.multiple_of(lax.rem(z + s, 4) * (4 * ROWS), 4 * ROWS), 4 * ROWS)
+                out.append(pltpu.make_async_copy(src.at[r], to.at[:, cols], sems.at[s]))
+            else:
+                for i in range(4):
+                    r = pl.ds(pl.multiple_of((i * 4 + lax.rem(y + s, 4)) * ROWS, ROWS), ROWS)
+                    out.append(pltpu.make_async_copy(src.at[r], to.at[pl.ds(i * ROWS, ROWS), cols], sems.at[4 * s + i]))
+        return out
+
+    tails = [c for side in range(2) for c in puts(expo, side, pl.ds(HALF, TAIL), st.at[side])]
+    for c in tails:
+        c.start()
+    parts = [puts(total.at[k % 2], k // 2, pl.ds((k % 2) * DEPTH, DEPTH), so.at[k]) for k in range(4)]
 
     def part(k, _):
         for n in range(4):
@@ -213,7 +232,8 @@
                     for c in copies[n + 2]:
                         c.start()
                 if n >= 2:
-                    put(n - 2).wait()
+                    for c in parts[n - 2]:
+                        c.wait()
 
         def tile(j, _):
             n = pl.ds(pl.multiple_of(j * 512, 512), 512)
@@ -222,31 +242,54 @@
             return 0
 
         lax.fori_loop(0, 2, tile, 0)
-        put(k).start()
+        for n in range(4):
+            @pl.when(k == n)
+            def _():
+                for c in parts[n]:
+                    c.start()
         return 0
 
     lax.fori_loop(0, 4, part, 0)
-    for c in (tail, put(2), put(3)):
+    for c in parts[2] + parts[3] + tails:
         c.wait()
 
 
 def input_sums(acts, was, wbs):
+    shape = jax.ShapeDtypeStruct
+    own, away = shape((4 * ROWS, HALF + TAIL), F32), shape((3, 4 * ROWS, HALF + TAIL), F32)
     return call(
         input_kernel,
-        jax.ShapeDtypeStruct((TOK, WIDE + TAIL), F32),
+        (own, own, away, away),
         [
             pltpu.VMEM((2 * UNITS, TOK), BF),
             pltpu.VMEM((4, UNITS, DEPTH), BF), pltpu.VMEM((4, UNITS, DEPTH), BF),
             pltpu.VMEM((TOK, UNITS), BF), pltpu.VMEM((TOK, UNITS), BF),
             pltpu.VMEM((2, TOK, DEPTH), F32), pltpu.VMEM((TOK, TAIL), F32),
-            pltpu.SemaphoreType.DMA((8,)), pltpu.SemaphoreType.DMA((6,)),
+            pltpu.SemaphoreType.DMA((8,)), pltpu.SemaphoreType.DMA((4, 16)), pltpu.SemaphoreType.DMA((2, 16)),
+            pltpu.SemaphoreType.DMA((1,)),
         ],
         2 * TOK * WIDE * UNITS * 2,
         [ANY] * 9,
-        ANY,
+        (ANY,) * 4,
         (acts, *was, *wbs),
         22 << 20,
     )
+
+
+def join_kernel(own_a, own_b, got, to_a, to_b):
+    z, y = place()
+    for own, first, to, at in ((own_a, 0, to_a, y), (own_b, 3, to_b, z)):
+        for s in range(4):
+            r = pl.ds(pl.multiple_of(lax.rem(at + s, 4) * ROWS, ROWS), ROWS)
+            v = own[r, :HALF] * jnp.exp2(own[r, HALF:HALF + 1] - 14.0)
+            for i in range(first, first + 3):
+                v = v + got[i, r, :HALF] * jnp.exp2(got[i, r, HALF:HALF + 1] - 14.0)
+            to[s] = v
+
+
+def joined(own_a, own_b, got):
+    out = jax.ShapeDtypeStruct((4, ROWS, HALF), F32)
+    return call(join_kernel, (out, out), [], 1 << 30, [VMEM] * 3, (VMEM,) * 2, (own_a, own_b, got), 12 << 20)
 
 
 def weight_kernel(acts, n_acts, columns, has_base, n_in, *refs):
@@ -406,12 +449,13 @@
     smh, spl = moved(amh, flip=1), moved(apl, flip=1)
     soa, sob = moved(oa, flip=1), moved(ob, flip=1)
 
-    packed = input_sums(own, was, wbs).astype(F16)
-    got = lax.all_to_all(packed.reshape(16, ROWS, WIDE + TAIL), "tp", 0, 0)
-    back = lax.optimization_barrier(jnp.exp2(got[:, 0, WIDE].astype(F32) - 14.0))
-    total = 0.0
-    for i in range(16):
-        total = total + got[i, :, :WIDE].astype(F32) * back[i]
+    own_a, own_b, qa, qb = input_sums(own, was, wbs)
+    qa, qb = qa.astype(F16), qb.astype(F16)
+    got = [moved(qa[d - 1], dz=-d) for d in (1, 2, 3)] + [moved(qb[d - 1], dy=-d) for d in (1, 2, 3)]
+    fa, fb = joined(own_a, own_b, jnp.stack(got).astype(F32))
+    fa = fa[0] + moved(fa[1], dy=-1) + moved(fa[2], dy=-2) + moved(fa[3], dy=-3)
+    fb = fb[0] + moved(fb[1], dz=-1) + moved(fb[2], dz=-2) + moved(fb[3], dz=-3)
+    total = jnp.concatenate([fa, fb], axis=1)
     grad_inputs = jnp.concatenate(relative(total.astype(BF), mark), axis=1)
 
     full = 3 * UNITS

time: 532 us -> 470 us (0.88)
  the two profiles are of different devices: /device:TPU:9 before, /device:TPU:1 now
where the time goes in v3:
time: 470 us
  waiting for transfers between devices  227 us (48%)
  starting transfers between devices  144 us (31%)
  Pallas kernels  76.4 us (16%)
  other arithmetic  11.3 us (2%)
  local copies, waits for them, and re-layouts  10.6 us (2%)
    ppermute x65, waiting for transfers between devices, moved(): return lax.ppermute(array, AXES, pairs)  227 us
    ppermute x65, starting transfers between devices, moved(): return lax.ppermute(array, AXES, pairs)  144 us
    pallas_call x6, Pallas kernels, call(): pl.pallas_call(body, out_shape=out_shape, in_specs=ins, out_specs=outs, s...  76.4 us
  transfers between devices with their start and end apart: 65, of which 27 were waited for; matrix products, arithmetic and copies ran while one was open for 3% of the time, Pallas kernels for 14%

profile of v3, /device:TPU:1, one launch (start us, length us, event | category | flops | bytes accessed | tf_op | source)
XLA Modules:
  0.0 469.8 jit_solution(8328721333966943692)
XLA Ops:
  35.1 50.1 %collective-permute-done.44 = bf16[4,32,1024]{2,1,0:T(8,128)(2,1)S(1)} collective-permute-done((bf16[4,32,1024]{2,1,0:T(8,128)(2,1)S(1)}, bf16[4,32,1024]{2,1,0:T(8,128)(2,1)S(1)}, u32[]{:S(2)}, u32[]{:S(2)}) %collective-permute-start.44) | collective-permute-done | bytes 262176 | tf_op jit(solution)/shard_map/ppermute | solution.py:38
  88.8 9.8 %collective-permute-done.5.refs_4_ = bf16[2,32,4096]{2,1,0:T(8,128)(2,1)S(1)} collective-permute-done((bf16[2,32,4096]{2,1,0:T(8,128)(2,1)S(1)}, bf16[2,32,4096]{2,1,0:T(8,128)(2,1)S(1)}, u32[]{:S(2)}, u32[]{:S(2)}) %collective-permute-start.5) | collective-permute-done | bytes 524320 | tf_op jit(solution)/shard_map/ppermute | solution.py:38
  98.6 11.2 %collective-permute-done.6.refs_5_ = bf16[2,32,4096]{2,1,0:T(8,128)(2,1)S(1)} collective-permute-done((bf16[2,32,4096]{2,1,0:T(8,128)(2,1)S(1)}, bf16[2,32,4096]{2,1,0:T(8,128)(2,1)S(1)}, u32[]{:S(2)}, u32[]{:S(2)}) %collective-permute-start.6) | collective-permute-done | bytes 524320 | tf_op jit(solution)/shard_map/ppermute | solution.py:38
  113.0 9.3 %collective-permute-done.13.refs_11_ = bf16[2,32,4096]{2,1,0:T(8,128)(2,1)S(1)} collective-permute-done((bf16[2,32,4096]{2,1,0:T(8,128)(2,1)S(1)}, bf16[2,32,4096]{2,1,0:T(8,128)(2,1)S(1)}, u32[]{:S(2)}, u32[]{:S(2)}) %collective-permute-start.13) | collective-permute-done | bytes 524320 | tf_op jit(solution)/shard_map/ppermute | solution.py:38
  126.9 9.0 %collective-permute-done.48 = bf16[1,6,32,1024]{3,2,1,0:T(8,128)(2,1)S(1)} collective-permute-done((bf16[1,6,32,1024]{3,2,1,0:T(8,128)(2,1)S(1)}, bf16[1,6,32,1024]{3,2,1,0:T(8,128)(2,1)S(1)}, u32[]{:S(2)}, u32[]{:S(2)}) %collective-permute-start.48) | collective-permute-done | bytes 393248 | tf_op jit(solution)/shard_map/ppermute | solution.py:38
  144.0 13.3 %collective-permute-start.21 = (bf16[1040,1024]{1,0:T(8,128)(2,1)S(1)}, bf16[1040,1024]{1,0:T(8,128)(2,1)S(1)}, u32[]{:S(2)}, u32[]{:S(2)}) collective-permute-start(bf16[1040,1024]{1,0:T(8,128)(2,1)S(1)} %pad_maximum_fusion.refs_20_.refs_5_), channel_id=1, source_target_pairs={{16,0},{17,1},{18,2},{19,3},{20,4},{21,5},{22,6},{23,7},{24,8},{25... | collective-permute-start | bytes 6389768 | tf_op jit(solution)/shard_map/ppermute | solution.py:38
  160.9 9.7 %collective-permute-done.7.refs_6_ = bf16[2,32,4096]{2,1,0:T(8,128)(2,1)S(1)} collective-permute-done((bf16[2,32,4096]{2,1,0:T(8,128)(2,1)S(1)}, bf16[2,32,4096]{2,1,0:T(8,128)(2,1)S(1)}, u32[]{:S(2)}, u32[]{:S(2)}) %collective-permute-start.7) | collective-permute-done | bytes 524320 | tf_op jit(solution)/shard_map/ppermute | solution.py:38
  172.9 11.1 %collective-permute-done.8.refs_7_ = bf16[2,32,4096]{2,1,0:T(8,128)(2,1)S(1)} collective-permute-done((bf16[2,32,4096]{2,1,0:T(8,128)(2,1)S(1)}, bf16[2,32,4096]{2,1,0:T(8,128)(2,1)S(1)}, u32[]{:S(2)}, u32[]{:S(2)}) %collective-permute-start.8) | collective-permute-done | bytes 524320 | tf_op jit(solution)/shard_map/ppermute | solution.py:38
  184.0 11.4 %collective-permute-done.16.refs_14_ = bf16[2,32,4096]{2,1,0:T(8,128)(2,1)S(1)} collective-permute-done((bf16[2,32,4096]{2,1,0:T(8,128)(2,1)S(1)}, bf16[2,32,4096]{2,1,0:T(8,128)(2,1)S(1)}, u32[]{:S(2)}, u32[]{:S(2)}) %collective-permute-start.16) | collective-permute-done | bytes 524320 | tf_op jit(solution)/shard_map/ppermute | solution.py:38
  198.1 9.9 %collective-permute-done.17.refs_15_ = bf16[2,32,4096]{2,1,0:T(8,128)(2,1)S(1)} collective-permute-done((bf16[2,32,4096]{2,1,0:T(8,128)(2,1)S(1)}, bf16[2,32,4096]{2,1,0:T(8,128)(2,1)S(1)}, u32[]{:S(2)}, u32[]{:S(2)}) %collective-permute-start.17) | collective-permute-done | bytes 524320 | tf_op jit(solution)/shard_map/ppermute | solution.py:38
  214.4 20.0 %shard_map.84 = (bf16[1040,512]{1,0:T(8,128)(2,1)}, bf16[1024,512]{1,0:T(8,128)(2,1)}, bf16[4112,512]{1,0:T(8,128)(2,1)}, bf16[512,1024]{1,0:T(8,128)(2,1)}, bf16[512,1024]{1,0:T(8,128)(2,1)}) custom-call(bf16[2,32,4096]{2,1,0:T(8,128)(2,1)} %copy-done.14, bf16[2,32,4096]{2,1,0:T(8,128)(2,1)} %copy-done.17, bf16[2,32,4096]{2,1,0:T(8,128)(2,1)} %copy-done.26, ...), custom_call_target="tpu_custom_call" | custom-call | flops 8657043456 | bytes 35651584 | tf_op jit(solution)/shard_map/pallas_call | solution.py:51
  234.5 13.8 %shard_map.85 = (f32[128,2176]{1,0:T(8,128)}, f32[128,2176]{1,0:T(8,128)}, f32[3,128,2176]{2,1,0:T(8,128)}, f32[3,128,2176]{2,1,0:T(8,128)}) custom-call(bf16[4112,512]{1,0:T(8,128)(2,1)} %get-tuple-element.24.refs_0_, bf16[1024,1024]{1,0:T(8,128)(2,1)} %copy-done.4, bf16[1024,1024]{1,0:T(8,128)(2,1)} %copy-done.21, bf16[1024,1024]{1,0:T(8,128)(2,1)} %copy-done.20, ...), custom_call_target="tpu_custom_call" | custom-call | flops 5771362304 | bytes 23068672 | tf_op jit(solution)/shard_map/pallas_call | solution.py:51
  252.8 9.7 %collective-permute-done.24 = f16[128,2176]{1,0:T(8,128)(2,1)S(1)} collective-permute-done((f16[128,2176]{1,0:T(8,128)(2,1)S(1)}, f16[128,2176]{1,0:T(8,128)(2,1)S(1)}, u32[]{:S(2)}, u32[]{:S(2)}) %collective-permute-start.24) | collective-permute-done | bytes 557088 | tf_op jit(solution)/shard_map/ppermute | solution.py:38
  263.1 10.5 %collective-permute-done.25 = f16[128,2176]{1,0:T(8,128)(2,1)S(1)} collective-permute-done((f16[128,2176]{1,0:T(8,128)(2,1)S(1)}, f16[128,2176]{1,0:T(8,128)(2,1)S(1)}, u32[]{:S(2)}, u32[]{:S(2)}) %collective-permute-start.25) | collective-permute-done | bytes 557088 | tf_op jit(solution)/shard_map/ppermute | solution.py:38
  273.8 8.7 %collective-permute-done.26 = f16[128,2176]{1,0:T(8,128)(2,1)S(1)} collective-permute-done((f16[128,2176]{1,0:T(8,128)(2,1)S(1)}, f16[128,2176]{1,0:T(8,128)(2,1)S(1)}, u32[]{:S(2)}, u32[]{:S(2)}) %collective-permute-start.26) | collective-permute-done | bytes 557088 | tf_op jit(solution)/shard_map/ppermute | solution.py:38
  283.4 8.7 %collective-permute-done.27 = f16[128,2176]{1,0:T(8,128)(2,1)S(1)} collective-permute-done((f16[128,2176]{1,0:T(8,128)(2,1)S(1)}, f16[128,2176]{1,0:T(8,128)(2,1)S(1)}, u32[]{:S(2)}, u32[]{:S(2)}) %collective-permute-start.27) | collective-permute-done | bytes 557088 | tf_op jit(solution)/shard_map/ppermute | solution.py:38
  305.8 11.9 %collective-permute-done.29 = f16[128,2176]{1,0:T(8,128)(2,1)S(1)} collective-permute-done((f16[128,2176]{1,0:T(8,128)(2,1)S(1)}, f16[128,2176]{1,0:T(8,128)(2,1)S(1)}, u32[]{:S(2)}, u32[]{:S(2)}) %collective-permute-start.29) | collective-permute-done | bytes 557088 | tf_op jit(solution)/shard_map/ppermute | solution.py:38
  317.7 12.7 %collective-permute-start.64 = (bf16[4112,512]{1,0:T(8,128)(2,1)}, bf16[4112,512]{1,0:T(8,128)(2,1)}, u32[]{:S(2)}, u32[]{:S(2)}) collective-permute-start(bf16[4112,512]{1,0:T(8,128)(2,1)} %get-tuple-element.24.refs_0_), channel_id=1, source_target_pairs={{16,0},{17,1},{18,2},{19,3},{20,4},{21,5},{22,6},{23,7},{24,8},{25... | collective-permute-start | bytes 12632072 | tf_op jit(solution)/shard_map/ppermute | solution.py:38
  380.1 21.5 %collective-permute-start.60 = (bf16[1024,512]{1,0:T(8,128)(2,1)}, bf16[1024,512]{1,0:T(8,128)(2,1)}, u32[]{:S(2)}, u32[]{:S(2)}) collective-permute-start(bf16[1024,512]{1,0:T(8,128)(2,1)} %collective-permute-done.58.refs_1_), channel_id=1, source_target_pairs={{16,0},{17,1},{18,2},{19,3},{20,4},{21,5},{22,6},{23,7},{24,8},{25... | collective-permute-start | bytes 3145736 | tf_op jit(solution)/shard_map/ppermute | solution.py:38
  404.7 12.1 %collective-permute-start.63 = (bf16[1024,512]{1,0:T(8,128)(2,1)}, bf16[1024,512]{1,0:T(8,128)(2,1)S(1)}, u32[]{:S(2)}, u32[]{:S(2)}) collective-permute-start(bf16[1024,512]{1,0:T(8,128)(2,1)} %collective-permute-done.38.refs_5_), channel_id=1, source_target_pairs={{16,0},{17,1},{18,2},{19,3},{20,4},{21,5},{22,6},{23,7},{24,8},{25... | collective-permute-start | bytes 3145736 | tf_op jit(solution)/shard_map/ppermute | solution.py:38
  416.8 11.1 %collective-permute-start.59 = (bf16[1040,512]{1,0:T(8,128)(2,1)}, bf16[1040,512]{1,0:T(8,128)(2,1)S(1)}, u32[]{:S(2)}, u32[]{:S(2)}) collective-permute-start(bf16[1040,512]{1,0:T(8,128)(2,1)} %collective-permute-done.36.refs_0_), channel_id=1, source_target_pairs={{16,0},{17,1},{18,2},{19,3},{20,4},{21,5},{22,6},{23,7},{24,8},{25... | collective-permute-start | bytes 3194888 | tf_op jit(solution)/shard_map/ppermute | solution.py:38
  429.3 9.6 %shard_map.87 = (f32[688,1024]{1,0:T(8,128)}, f32[688,1024]{1,0:T(8,128)}, f32[688,1024]{1,0:T(8,128)}) custom-call(bf16[4112,512]{1,0:T(8,128)(2,1)} %get-tuple-element.24.refs_0_, bf16[4112,512]{1,0:T(8,128)(2,1)} %collective-permute-done.64.refs_1_.refs_4_, bf16[512,1024]{1,0:T(8,128)(2,1)} %get-tuple-element.33.refs_2_, ...), custom_call_target="tpu_custom_call" | custom-call | flops 4328521728 | bytes 25165824 | tf_op jit(solution)/shard_map/pallas_call | solution.py:51
  440.6 16.8 %shard_map.88 = (f32[688,1024]{1,0:T(8,128)}, f32[688,1024]{1,0:T(8,128)}, f32[688,1024]{1,0:T(8,128)}) custom-call(bf16[1040,512]{1,0:T(8,128)(2,1)} %collective-permute-done.36.refs_0_, bf16[1024,512]{1,0:T(8,128)(2,1)} %collective-permute-done.58.refs_1_, bf16[1040,512]{1,0:T(8,128)(2,1)} %copy-done.23, ...), custom_call_target="tpu_custom_call" | custom-call | flops 8657043456 | bytes 33554432 | tf_op jit(solution)/shard_map/pallas_call | solution.py:51
  458.7 10.9 %shard_map.89 = (f32[688,1024]{1,0:T(8,128)}, f32[688,1024]{1,0:T(8,128)}, f32[688,1024]{1,0:T(8,128)}) custom-call(bf16[1040,512]{1,0:T(8,128)(2,1)} %copy-done.9, bf16[1024,512]{1,0:T(8,128)(2,1)} %copy-done.11, bf16[1040,512]{1,0:T(8,128)(2,1)} %copy-done.10, bf16[1024,512]{1,0:T(8,128)(2,1)} %copy-done.12, bf16[4,6,32,1024]{3,2,1,0:T(8,128)(2,1)} %copy-done, ...), custom_call_target="tpu_custom_call" | custom-call | flops 4328521728 | bytes 25165824 | tf_op jit(solution)/shard_map/pallas_call | solution.py:51
  (232 shorter events, 145.7 us)
Async XLA Ops:
  21.1 65.2 %collective-permute-start.3 = (bf16[2,32,4096]{2,1,0:T(8,128)(2,1)S(1)}, bf16[2,32,4096]{2,1,0:T(8,128)(2,1)S(1)}, u32[]{:S(2)}, u32[]{:S(2)}) collective-permute-start(bf16[2,32,4096]{2,1,0:T(8,128)(2,1)S(1)} %pad_maximum_fusion.4.refs_0_), channel_id=1, source_target_pairs={{1,0},{2,1},{3,2},{0,3},{5,4},{6,5},{7,6},{4,7},{9,8},{10,9},{11,1... | collective-permute-start | bytes 1572872 | tf_op jit(solution)/shard_map/ppermute | solution.py:38
  23.9 62.5 %collective-permute-start.4 = (bf16[2,32,4096]{2,1,0:T(8,128)(2,1)S(1)}, bf16[2,32,4096]{2,1,0:T(8,128)(2,1)S(1)}, u32[]{:S(2)}, u32[]{:S(2)}) collective-permute-start(bf16[2,32,4096]{2,1,0:T(8,128)(2,1)S(1)} %constant_dynamic-update-slice_fusion.refs_1_), channel_id=1, source_target_pairs={{1,0},{2,1},{3,2},{0,3},{5,4},{6,5},{7,6},{4,7},{9,8},{10,9},{11,1... | collective-permute-start | bytes 1572872 | tf_op jit(solution)/shard_map/ppermute | solution.py:38
  27.4 129.9 %collective-permute-start.22 = (bf16[1040,1024]{1,0:T(8,128)(2,1)S(1)}, bf16[1040,1024]{1,0:T(8,128)(2,1)S(1)}, u32[]{:S(2)}, u32[]{:S(2)}) collective-permute-start(bf16[1040,1024]{1,0:T(8,128)(2,1)S(1)} %pad_maximum_fusion.refs_20_.refs_5_), channel_id=1, source_target_pairs={{96,0},{97,1},{98,2},{99,3},{100,4},{101,5},{102,6},{103,7},{104,8... | collective-permute-start | bytes 6389768 | tf_op jit(solution)/shard_map/ppermute | solution.py:38
  27.8 57.4 %collective-permute-start.44 = (bf16[4,32,1024]{2,1,0:T(8,128)(2,1)S(1)}, bf16[4,32,1024]{2,1,0:T(8,128)(2,1)S(1)}, u32[]{:S(2)}, u32[]{:S(2)}) collective-permute-start(bf16[4,32,1024]{2,1,0:T(8,128)(2,1)S(1)} %pad_maximum_fusion.8), channel_id=1, source_target_pairs={{96,0},{97,1},{98,2},{99,3},{100,4},{101,5},{102,6},{103,7},{104,8... | collective-permute-start | bytes 786440 | tf_op jit(solution)/shard_map/ppermute | solution.py:38
  32.6 52.6 %collective-permute-start.43 = (bf16[4,32,1024]{2,1,0:T(8,128)(2,1)S(1)}, bf16[4,32,1024]{2,1,0:T(8,128)(2,1)S(1)}, u32[]{:S(2)}, u32[]{:S(2)}) collective-permute-start(bf16[4,32,1024]{2,1,0:T(8,128)(2,1)S(1)} %pad_maximum_fusion.8), channel_id=1, source_target_pairs={{32,0},{33,1},{34,2},{35,3},{36,4},{37,5},{38,6},{39,7},{40,8},{41... | collective-permute-start | bytes 786440 | tf_op jit(solution)/shard_map/ppermute | solution.py:38
  85.2 75.4 %collective-permute-start.19 = (bf16[1024,1024]{1,0:T(8,128)(2,1)S(1)}, bf16[1024,1024]{1,0:T(8,128)(2,1)S(1)}, u32[]{:S(2)}, u32[]{:S(2)}) collective-permute-start(bf16[1024,1024]{1,0:T(8,128)(2,1)S(1)} %pad_maximum_fusion.1.refs_16_.refs_1_), channel_id=1, source_target_pairs={{32,0},{33,1},{34,2},{35,3},{36,4},{37,5},{38,6},{39,7},{40,8},{41... | collective-permute-start | bytes 6291464 | tf_op jit(solution)/shard_map/ppermute | solution.py:38
  144.0 67.2 %collective-permute-start.21 = (bf16[1040,1024]{1,0:T(8,128)(2,1)S(1)}, bf16[1040,1024]{1,0:T(8,128)(2,1)S(1)}, u32[]{:S(2)}, u32[]{:S(2)}) collective-permute-start(bf16[1040,1024]{1,0:T(8,128)(2,1)S(1)} %pad_maximum_fusion.refs_20_.refs_5_), channel_id=1, source_target_pairs={{16,0},{17,1},{18,2},{19,3},{20,4},{21,5},{22,6},{23,7},{24,8},{25... | collective-permute-start | bytes 6389768 | tf_op jit(solution)/shard_map/ppermute | solution.py:38
  157.4 57.1 %collective-permute-start.23 = (bf16[1040,1024]{1,0:T(8,128)(2,1)S(1)}, bf16[1040,1024]{1,0:T(8,128)(2,1)}, u32[]{:S(2)}, u32[]{:S(2)}) collective-permute-start(bf16[1040,1024]{1,0:T(8,128)(2,1)S(1)} %collective-permute-done.22.refs_22_.refs_7_), channel_id=1, source_target_pairs={{16,0},{17,1},{18,2},{19,3},{20,4},{21,5},{22,6},{23,7},{24,8},{25... | collective-permute-start | bytes 6389768 | tf_op jit(solution)/shard_map/ppermute | solution.py:38
  158.5 51.5 %collective-permute-start.18 = (bf16[1024,1024]{1,0:T(8,128)(2,1)S(1)}, bf16[1024,1024]{1,0:T(8,128)(2,1)S(1)}, u32[]{:S(2)}, u32[]{:S(2)}) collective-permute-start(bf16[1024,1024]{1,0:T(8,128)(2,1)S(1)} %pad_maximum_fusion.1.refs_16_.refs_1_), channel_id=1, source_target_pairs={{16,0},{17,1},{18,2},{19,3},{20,4},{21,5},{22,6},{23,7},{24,8},{25... | collective-permute-start | bytes 6291464 | tf_op jit(solution)/shard_map/ppermute | solution.py:38
  160.6 52.5 %collective-permute-start.20 = (bf16[1024,1024]{1,0:T(8,128)(2,1)S(1)}, bf16[1024,1024]{1,0:T(8,128)(2,1)S(1)}, u32[]{:S(2)}, u32[]{:S(2)}) collective-permute-start(bf16[1024,1024]{1,0:T(8,128)(2,1)S(1)} %collective-permute-done.19.refs_18_.refs_3_), channel_id=1, source_target_pairs={{16,0},{17,1},{18,2},{19,3},{20,4},{21,5},{22,6},{23,7},{24,8},{25... | collective-permute-start | bytes 6291464 | tf_op jit(solution)/shard_map/ppermute | solution.py:38
  207.9 85.8 %collective-permute-start.49 = (bf16[4,6,32,1024]{3,2,1,0:T(8,128)(2,1)S(1)}, bf16[4,6,32,1024]{3,2,1,0:T(8,128)(2,1)}, u32[]{:S(2)}, u32[]{:S(2)}) collective-permute-start(bf16[4,6,32,1024]{3,2,1,0:T(8,128)(2,1)S(1)} %pad_maximum_fusion.2.refs_8_.refs_4_), channel_id=1, source_target_pairs={{1,0},{2,1},{3,2},{0,3},{5,4},{6,5},{7,6},{4,7},{9,8},{10,9},{11,1... | collective-permute-start | bytes 4718600 | tf_op jit(solution)/shard_map/ppermute | solution.py:38
  210.0 86.9 %collective-permute-start.50 = (bf16[4,6,32,1024]{3,2,1,0:T(8,128)(2,1)S(1)}, bf16[4,6,32,1024]{3,2,1,0:T(8,128)(2,1)S(1)}, u32[]{:S(2)}, u32[]{:S(2)}) collective-permute-start(bf16[4,6,32,1024]{3,2,1,0:T(8,128)(2,1)S(1)} %pad_maximum_fusion.2.refs_8_.refs_4_), channel_id=1, source_target_pairs={{3,0},{0,1},{1,2},{2,3},{7,4},{4,5},{5,6},{6,7},{11,8},{8,9},{9,10... | collective-permute-start | bytes 4718600 | tf_op jit(solution)/shard_map/ppermute | solution.py:38
  211.3 129.0 %collective-permute-start.51 = (bf16[4,6,32,1024]{3,2,1,0:T(8,128)(2,1)S(1)}, bf16[4,6,32,1024]{3,2,1,0:T(8,128)(2,1)S(1)}, u32[]{:S(2)}, u32[]{:S(2)}) collective-permute-start(bf16[4,6,32,1024]{3,2,1,0:T(8,128)(2,1)S(1)} %pad_maximum_fusion.2.refs_8_.refs_4_), channel_id=1, source_target_pairs={{2,0},{3,1},{0,2},{1,3},{6,4},{7,5},{4,6},{5,7},{10,8},{11,9},{8,1... | collective-permute-start | bytes 4718600 | tf_op jit(solution)/shard_map/ppermute | solution.py:38
  213.1 130.9 %collective-permute-start.55 = (bf16[4,6,32,1024]{3,2,1,0:T(8,128)(2,1)S(1)}, bf16[4,6,32,1024]{3,2,1,0:T(8,128)(2,1)}, u32[]{:S(2)}, u32[]{:S(2)}) collective-permute-start(bf16[4,6,32,1024]{3,2,1,0:T(8,128)(2,1)S(1)} %pad_maximum_fusion.3.refs_12_.refs_8_), channel_id=1, source_target_pairs={{4,0},{5,1},{6,2},{7,3},{8,4},{9,5},{10,6},{11,7},{12,8},{13,9},{1... | collective-permute-start | bytes 4718600 | tf_op jit(solution)/shard_map/ppermute | solution.py:38
  293.7 56.1 %collective-permute-start.56 = (bf16[4,6,32,1024]{3,2,1,0:T(8,128)(2,1)S(1)}, bf16[4,6,32,1024]{3,2,1,0:T(8,128)(2,1)}, u32[]{:S(2)}, u32[]{:S(2)}) collective-permute-start(bf16[4,6,32,1024]{3,2,1,0:T(8,128)(2,1)S(1)} %pad_maximum_fusion.3.refs_12_.refs_8_), channel_id=1, source_target_pairs={{12,0},{13,1},{14,2},{15,3},{0,4},{1,5},{2,6},{3,7},{4,8},{5,9},{6... | collective-permute-start | bytes 4718600 | tf_op jit(solution)/shard_map/ppermute | solution.py:38
  296.9 55.7 %collective-permute-start.57 = (bf16[4,6,32,1024]{3,2,1,0:T(8,128)(2,1)S(1)}, bf16[4,6,32,1024]{3,2,1,0:T(8,128)(2,1)}, u32[]{:S(2)}, u32[]{:S(2)}) collective-permute-start(bf16[4,6,32,1024]{3,2,1,0:T(8,128)(2,1)S(1)} %pad_maximum_fusion.3.refs_12_.refs_8_), channel_id=1, source_target_pairs={{8,0},{9,1},{10,2},{11,3},{12,4},{13,5},{14,6},{15,7},{0,8},{1,9},... | collective-permute-start | bytes 4718600 | tf_op jit(solution)/shard_map/ppermute | solution.py:38
  317.7 111.5 %collective-permute-start.64 = (bf16[4112,512]{1,0:T(8,128)(2,1)}, bf16[4112,512]{1,0:T(8,128)(2,1)}, u32[]{:S(2)}, u32[]{:S(2)}) collective-permute-start(bf16[4112,512]{1,0:T(8,128)(2,1)} %get-tuple-element.24.refs_0_), channel_id=1, source_target_pairs={{16,0},{17,1},{18,2},{19,3},{20,4},{21,5},{22,6},{23,7},{24,8},{25... | collective-permute-start | bytes 12632072 | tf_op jit(solution)/shard_map/ppermute | solution.py:38
  344.0 34.3 %collective-permute-start.38 = (bf16[1024,512]{1,0:T(8,128)(2,1)}, bf16[1024,512]{1,0:T(8,128)(2,1)}, u32[]{:S(2)}, u32[]{:S(2)}) collective-permute-start(bf16[1024,512]{1,0:T(8,128)(2,1)} %get-tuple-element.32), channel_id=1, source_target_pairs={{96,0},{97,1},{98,2},{99,3},{100,4},{101,5},{102,6},{103,7},{104,8... | collective-permute-start | bytes 3145736 | tf_op jit(solution)/shard_map/ppermute | solution.py:38
  349.8 30.3 %collective-permute-start.58 = (bf16[1024,512]{1,0:T(8,128)(2,1)}, bf16[1024,512]{1,0:T(8,128)(2,1)}, u32[]{:S(2)}, u32[]{:S(2)}) collective-permute-start(bf16[1024,512]{1,0:T(8,128)(2,1)} %get-tuple-element.32), channel_id=1, source_target_pairs={{32,0},{33,1},{34,2},{35,3},{36,4},{37,5},{38,6},{39,7},{40,8},{41... | collective-permute-start | bytes 3145736 | tf_op jit(solution)/shard_map/ppermute | solution.py:38
  366.1 36.6 %collective-permute-start.36 = (bf16[1040,512]{1,0:T(8,128)(2,1)}, bf16[1040,512]{1,0:T(8,128)(2,1)}, u32[]{:S(2)}, u32[]{:S(2)}) collective-permute-start(bf16[1040,512]{1,0:T(8,128)(2,1)} %get-tuple-element.31), channel_id=1, source_target_pairs={{32,0},{33,1},{34,2},{35,3},{36,4},{37,5},{38,6},{39,7},{40,8},{41... | collective-permute-start | bytes 3194888 | tf_op jit(solution)/shard_map/ppermute | solution.py:38
  378.3 38.5 %collective-permute-start.39 = (bf16[1024,512]{1,0:T(8,128)(2,1)}, bf16[1024,512]{1,0:T(8,128)(2,1)S(1)}, u32[]{:S(2)}, u32[]{:S(2)}) collective-permute-start(bf16[1024,512]{1,0:T(8,128)(2,1)} %collective-permute-done.38.refs_5_), channel_id=1, source_target_pairs={{96,0},{97,1},{98,2},{99,3},{100,4},{101,5},{102,6},{103,7},{104,8... | collective-permute-start | bytes 3145736 | tf_op jit(solution)/shard_map/ppermute | solution.py:38
  380.1 47.9 %collective-permute-start.60 = (bf16[1024,512]{1,0:T(8,128)(2,1)}, bf16[1024,512]{1,0:T(8,128)(2,1)}, u32[]{:S(2)}, u32[]{:S(2)}) collective-permute-start(bf16[1024,512]{1,0:T(8,128)(2,1)} %collective-permute-done.58.refs_1_), channel_id=1, source_target_pairs={{16,0},{17,1},{18,2},{19,3},{20,4},{21,5},{22,6},{23,7},{24,8},{25... | collective-permute-start | bytes 3145736 | tf_op jit(solution)/shard_map/ppermute | solution.py:38
  404.7 34.2 %collective-permute-start.63 = (bf16[1024,512]{1,0:T(8,128)(2,1)}, bf16[1024,512]{1,0:T(8,128)(2,1)S(1)}, u32[]{:S(2)}, u32[]{:S(2)}) collective-permute-start(bf16[1024,512]{1,0:T(8,128)(2,1)} %collective-permute-done.38.refs_5_), channel_id=1, source_target_pairs={{16,0},{17,1},{18,2},{19,3},{20,4},{21,5},{22,6},{23,7},{24,8},{25... | collective-permute-start | bytes 3145736 | tf_op jit(solution)/shard_map/ppermute | solution.py:38
  428.8 28.6 %collective-permute-start.41 = (bf16[1024,512]{1,0:T(8,128)(2,1)S(1)}, bf16[1024,512]{1,0:T(8,128)(2,1)S(1)}, u32[]{:S(2)}, u32[]{:S(2)}) collective-permute-start(bf16[1024,512]{1,0:T(8,128)(2,1)S(1)} %collective-permute-done.39.refs_1_), channel_id=1, source_target_pairs={{16,0},{17,1},{18,2},{19,3},{20,4},{21,5},{22,6},{23,7},{24,8},{25... | collective-permute-start | bytes 3145736 | tf_op jit(solution)/shard_map/ppermute | solution.py:38
  (81 other events, 2201.1 us)

commit v4 on v3

--- a/solution.py
+++ b/solution.py
@@ -276,20 +276,22 @@
     )
 
 
-def join_kernel(own_a, own_b, got, to_a, to_b):
+def join_kernel(*refs):
     z, y = place()
-    for own, first, to, at in ((own_a, 0, to_a, y), (own_b, 3, to_b, z)):
+    for side, at in ((0, y), (1, z)):
+        own, got, out = refs[side], refs[2 + 3 * side:5 + 3 * side], refs[8 + 4 * side:12 + 4 * side]
         for s in range(4):
             r = pl.ds(pl.multiple_of(lax.rem(at + s, 4) * ROWS, ROWS), ROWS)
             v = own[r, :HALF] * jnp.exp2(own[r, HALF:HALF + 1] - 14.0)
-            for i in range(first, first + 3):
-                v = v + got[i, r, :HALF] * jnp.exp2(got[i, r, HALF:HALF + 1] - 14.0)
-            to[s] = v
+            for g in got:
+                v = v + g[r, :HALF] * jnp.exp2(g[r, HALF:HALF + 1] - 14.0)
+            out[s][...] = v
 
 
 def joined(own_a, own_b, got):
-    out = jax.ShapeDtypeStruct((4, ROWS, HALF), F32)
-    return call(join_kernel, (out, out), [], 1 << 30, [VMEM] * 3, (VMEM,) * 2, (own_a, own_b, got), 12 << 20)
+    out = jax.ShapeDtypeStruct((ROWS, HALF), F32)
+    kept = call(join_kernel, (out,) * 8, [], 1 << 30, [VMEM] * 8, (VMEM,) * 8, (own_a, own_b, *got), 12 << 20)
+    return kept[:4], kept[4:]
 
 
 def weight_kernel(acts, n_acts, columns, has_base, n_in, *refs):
@@ -452,7 +454,7 @@
     own_a, own_b, qa, qb = input_sums(own, was, wbs)
     qa, qb = qa.astype(F16), qb.astype(F16)
     got = [moved(qa[d - 1], dz=-d) for d in (1, 2, 3)] + [moved(qb[d - 1], dy=-d) for d in (1, 2, 3)]
-    fa, fb = joined(own_a, own_b, jnp.stack(got).astype(F32))
+    fa, fb = joined(own_a, own_b, [g.astype(F32) for g in got])
     fa = fa[0] + moved(fa[1], dy=-1) + moved(fa[2], dy=-2) + moved(fa[3], dy=-3)
     fb = fb[0] + moved(fb[1], dz=-1) + moved(fb[2], dz=-2) + moved(fb[3], dz=-3)
     total = jnp.concatenate([fa, fb], axis=1)

time: 470 us -> 490 us (1.043)
  waiting for transfers between devices: 227 us -> 260 us
  starting transfers between devices: 144 us -> 125 us
    ppermute x65, waiting for transfers between devices: 227 us -> 260 us  [moved(): return lax.ppermute(array, AXES, pairs)]
    ppermute x65, starting transfers between devices: 144 us -> 125 us  [moved(): return lax.ppermute(array, AXES, pairs)]
  transfers between devices with their start and end apart: 65 -> 65, of which waited for: 27 -> 28; matrix products, arithmetic and copies ran while one was open for 3% -> 3% of each run, Pallas kernels for 14% -> 13%
where the time goes in v4:
time: 490 us; the launch traced here: 488 us
  waiting for transfers between devices  260 us (53%)
  starting transfers between devices  125 us (26%)
  Pallas kernels  76.3 us (16%)
  other arithmetic  15.9 us (3%)
  local copies, waits for them, and re-layouts  8.68 us (2%)
    ppermute x65, waiting for transfers between devices, moved(): return lax.ppermute(array, AXES, pairs)  260 us
    ppermute x65, starting transfers between devices, moved(): return lax.ppermute(array, AXES, pairs)  125 us
    pallas_call x6, Pallas kernels, call(): pl.pallas_call(body, out_shape=out_shape, in_specs=ins, out_specs=outs, s...  76.3 us
  transfers between devices with their start and end apart: 65, of which 28 were waited for; matrix products, arithmetic and copies ran while one was open for 3% of the time, Pallas kernels for 13%

profile of v4, /device:TPU:1, one launch (start us, length us, event | category | flops | bytes accessed | tf_op | source)
XLA Modules:
  0.0 487.7 jit_solution(340595199642977147)
XLA Ops:
  29.5 42.4 %collective-permute-done.45 = bf16[4,32,1024]{2,1,0:T(8,128)(2,1)S(1)} collective-permute-done((bf16[4,32,1024]{2,1,0:T(8,128)(2,1)S(1)}, bf16[4,32,1024]{2,1,0:T(8,128)(2,1)S(1)}, u32[]{:S(2)}, u32[]{:S(2)}) %collective-permute-start.45) | collective-permute-done | bytes 262176 | tf_op jit(solution)/shard_map/ppermute | solution.py:38
  77.9 41.7 %collective-permute-done.43 = bf16[4,32,1024]{2,1,0:T(8,128)(2,1)S(1)} collective-permute-done((bf16[4,32,1024]{2,1,0:T(8,128)(2,1)S(1)}, bf16[4,32,1024]{2,1,0:T(8,128)(2,1)S(1)}, u32[]{:S(2)}, u32[]{:S(2)}) %collective-permute-start.43) | collective-permute-done | bytes 262176 | tf_op jit(solution)/shard_map/ppermute | solution.py:38
  130.3 9.1 %collective-permute-done.6.refs_5_ = bf16[2,32,4096]{2,1,0:T(8,128)(2,1)S(1)} collective-permute-done((bf16[2,32,4096]{2,1,0:T(8,128)(2,1)S(1)}, bf16[2,32,4096]{2,1,0:T(8,128)(2,1)S(1)}, u32[]{:S(2)}, u32[]{:S(2)}) %collective-permute-start.6) | collective-permute-done | bytes 524320 | tf_op jit(solution)/shard_map/ppermute | solution.py:38
  158.9 11.2 %collective-permute-done.48 = bf16[1,6,32,1024]{3,2,1,0:T(8,128)(2,1)S(1)} collective-permute-done((bf16[1,6,32,1024]{3,2,1,0:T(8,128)(2,1)S(1)}, bf16[1,6,32,1024]{3,2,1,0:T(8,128)(2,1)S(1)}, u32[]{:S(2)}, u32[]{:S(2)}) %collective-permute-start.48) | collective-permute-done | bytes 393248 | tf_op jit(solution)/shard_map/ppermute | solution.py:38
  185.6 9.6 %collective-permute-done.8.refs_7_ = bf16[2,32,4096]{2,1,0:T(8,128)(2,1)S(1)} collective-permute-done((bf16[2,32,4096]{2,1,0:T(8,128)(2,1)S(1)}, bf16[2,32,4096]{2,1,0:T(8,128)(2,1)S(1)}, u32[]{:S(2)}, u32[]{:S(2)}) %collective-permute-start.8) | collective-permute-done | bytes 524320 | tf_op jit(solution)/shard_map/ppermute | solution.py:38
  195.1 7.8 %collective-permute-start.16 = (bf16[2,32,4096]{2,1,0:T(8,128)(2,1)S(1)}, bf16[2,32,4096]{2,1,0:T(8,128)(2,1)S(1)}, u32[]{:S(2)}, u32[]{:S(2)}) collective-permute-start(bf16[2,32,4096]{2,1,0:T(8,128)(2,1)S(1)} %collective-permute-done.12.refs_10_), channel_id=1, source_target_pairs={{4,0},{5,1},{6,2},{7,3},{8,4},{9,5},{10,6},{11,7},{12,8},{13,9},{1... | collective-permute-start | bytes 1572872 | tf_op jit(solution)/shard_map/ppermute | solution.py:38
  203.0 9.2 %collective-permute-done.16.refs_14_ = bf16[2,32,4096]{2,1,0:T(8,128)(2,1)S(1)} collective-permute-done((bf16[2,32,4096]{2,1,0:T(8,128)(2,1)S(1)}, bf16[2,32,4096]{2,1,0:T(8,128)(2,1)S(1)}, u32[]{:S(2)}, u32[]{:S(2)}) %collective-permute-start.16) | collective-permute-done | bytes 524320 | tf_op jit(solution)/shard_map/ppermute | solution.py:38
  213.6 11.3 %collective-permute-done.17.refs_15_ = bf16[2,32,4096]{2,1,0:T(8,128)(2,1)S(1)} collective-permute-done((bf16[2,32,4096]{2,1,0:T(8,128)(2,1)S(1)}, bf16[2,32,4096]{2,1,0:T(8,128)(2,1)S(1)}, u32[]{:S(2)}, u32[]{:S(2)}) %collective-permute-start.17) | collective-permute-done | bytes 524320 | tf_op jit(solution)/shard_map/ppermute | solution.py:38
  231.5 19.9 %shard_map.84 = (bf16[1040,512]{1,0:T(8,128)(2,1)}, bf16[1024,512]{1,0:T(8,128)(2,1)}, bf16[4112,512]{1,0:T(8,128)(2,1)}, bf16[512,1024]{1,0:T(8,128)(2,1)}, bf16[512,1024]{1,0:T(8,128)(2,1)}) custom-call(bf16[2,32,4096]{2,1,0:T(8,128)(2,1)} %copy-done.16, bf16[2,32,4096]{2,1,0:T(8,128)(2,1)} %copy-done.22, bf16[2,32,4096]{2,1,0:T(8,128)(2,1)} %copy-done.32, ...), custom_call_target="tpu_custom_call" | custom-call | flops 8657043456 | bytes 35651584 | tf_op jit(solution)/shard_map/pallas_call | solution.py:51
  251.4 13.8 %shard_map.85 = (f32[128,2176]{1,0:T(8,128)}, f32[128,2176]{1,0:T(8,128)}, f32[3,128,2176]{2,1,0:T(8,128)}, f32[3,128,2176]{2,1,0:T(8,128)}) custom-call(bf16[4112,512]{1,0:T(8,128)(2,1)} %get-tuple-element.30.refs_0_, bf16[1024,1024]{1,0:T(8,128)(2,1)} %copy-done.4, bf16[1024,1024]{1,0:T(8,128)(2,1)} %copy-done.27, bf16[1024,1024]{1,0:T(8,128)(2,1)} %copy-done.26, ...), custom_call_target="tpu_custom_call" | custom-call | flops 5771362304 | bytes 23068672 | tf_op jit(solution)/shard_map/pallas_call | solution.py:51
  272.2 6.2 %collective-permute-done.49.refs_9_.refs_5_ = bf16[4,6,32,1024]{3,2,1,0:T(8,128)(2,1)S(1)} collective-permute-done((bf16[4,6,32,1024]{3,2,1,0:T(8,128)(2,1)S(1)}, bf16[4,6,32,1024]{3,2,1,0:T(8,128)(2,1)S(1)}, u32[]{:S(2)}, u32[]{:S(2)}) %collective-permute-start.49) | collective-permute-done | bytes 1572896 | tf_op jit(solution)/shard_map/ppermute | solution.py:38
  283.0 8.1 %collective-permute-done.25 = f16[128,2176]{1,0:T(8,128)(2,1)S(1)} collective-permute-done((f16[128,2176]{1,0:T(8,128)(2,1)S(1)}, f16[128,2176]{1,0:T(8,128)(2,1)S(1)}, u32[]{:S(2)}, u32[]{:S(2)}) %collective-permute-start.25) | collective-permute-done | bytes 557088 | tf_op jit(solution)/shard_map/ppermute | solution.py:38
  299.4 7.6 %collective-permute-done.28 = f16[128,2176]{1,0:T(8,128)(2,1)S(1)} collective-permute-done((f16[128,2176]{1,0:T(8,128)(2,1)S(1)}, f16[128,2176]{1,0:T(8,128)(2,1)S(1)}, u32[]{:S(2)}, u32[]{:S(2)}) %collective-permute-start.28) | collective-permute-done | bytes 557088 | tf_op jit(solution)/shard_map/ppermute | solution.py:38
  324.2 16.6 %collective-permute-done.51.refs_11_.refs_7_ = bf16[4,6,32,1024]{3,2,1,0:T(8,128)(2,1)S(1)} collective-permute-done((bf16[4,6,32,1024]{3,2,1,0:T(8,128)(2,1)S(1)}, bf16[4,6,32,1024]{3,2,1,0:T(8,128)(2,1)S(1)}, u32[]{:S(2)}, u32[]{:S(2)}) %collective-permute-start.51) | collective-permute-done | bytes 1572896 | tf_op jit(solution)/shard_map/ppermute | solution.py:38
  343.6 23.7 %collective-permute-done.57.refs_15_.refs_11_ = bf16[4,6,32,1024]{3,2,1,0:T(8,128)(2,1)} collective-permute-done((bf16[4,6,32,1024]{3,2,1,0:T(8,128)(2,1)S(1)}, bf16[4,6,32,1024]{3,2,1,0:T(8,128)(2,1)}, u32[]{:S(2)}, u32[]{:S(2)}) %collective-permute-start.57) | collective-permute-done | bytes 1572896 | tf_op jit(solution)/shard_map/ppermute | solution.py:38
  384.4 7.9 %collective-permute-start.30 = (f32[32,2048]{1,0:T(8,128)}, f32[32,2048]{1,0:T(8,128)S(1)}, u32[]{:S(2)}, u32[]{:S(2)}) collective-permute-start(f32[32,2048]{1,0:T(8,128)} %get-tuple-element.36), channel_id=1, source_target_pairs={{12,0},{13,1},{14,2},{15,3},{0,4},{1,5},{2,6},{3,7},{4,8},{5,9},{6... | collective-permute-start | bytes 786440 | tf_op jit(solution)/shard_map/ppermute | solution.py:38
  396.1 6.5 %collective-permute-start.60 = (bf16[1024,512]{1,0:T(8,128)(2,1)}, bf16[1024,512]{1,0:T(8,128)(2,1)}, u32[]{:S(2)}, u32[]{:S(2)}) collective-permute-start(bf16[1024,512]{1,0:T(8,128)(2,1)} %collective-permute-done.58.refs_1_), channel_id=1, source_target_pairs={{16,0},{17,1},{18,2},{19,3},{20,4},{21,5},{22,6},{23,7},{24,8},{25... | collective-permute-start | bytes 3145736 | tf_op jit(solution)/shard_map/ppermute | solution.py:38
  407.6 8.5 %collective-permute-done.61.refs_4_ = bf16[1040,512]{1,0:T(8,128)(2,1)} collective-permute-done((bf16[1040,512]{1,0:T(8,128)(2,1)}, bf16[1040,512]{1,0:T(8,128)(2,1)}, u32[]{:S(2)}, u32[]{:S(2)}) %collective-permute-start.61) | collective-permute-done | bytes 1064992 | tf_op jit(solution)/shard_map/ppermute | solution.py:38
  416.0 14.2 %collective-permute-start.63 = (bf16[1024,512]{1,0:T(8,128)(2,1)}, bf16[1024,512]{1,0:T(8,128)(2,1)S(1)}, u32[]{:S(2)}, u32[]{:S(2)}) collective-permute-start(bf16[1024,512]{1,0:T(8,128)(2,1)} %collective-permute-done.38.refs_5_), channel_id=1, source_target_pairs={{16,0},{17,1},{18,2},{19,3},{20,4},{21,5},{22,6},{23,7},{24,8},{25... | collective-permute-start | bytes 3145736 | tf_op jit(solution)/shard_map/ppermute | solution.py:38
  430.3 8.2 %collective-permute-done.39.refs_1_ = bf16[1024,512]{1,0:T(8,128)(2,1)S(1)} collective-permute-done((bf16[1024,512]{1,0:T(8,128)(2,1)}, bf16[1024,512]{1,0:T(8,128)(2,1)S(1)}, u32[]{:S(2)}, u32[]{:S(2)}) %collective-permute-start.39) | collective-permute-done | bytes 1048608 | tf_op jit(solution)/shard_map/ppermute | solution.py:38
  438.4 7.3 %collective-permute-start.59 = (bf16[1040,512]{1,0:T(8,128)(2,1)}, bf16[1040,512]{1,0:T(8,128)(2,1)S(1)}, u32[]{:S(2)}, u32[]{:S(2)}) collective-permute-start(bf16[1040,512]{1,0:T(8,128)(2,1)} %collective-permute-done.36.refs_0_), channel_id=1, source_target_pairs={{16,0},{17,1},{18,2},{19,3},{20,4},{21,5},{22,6},{23,7},{24,8},{25... | collective-permute-start | bytes 3194888 | tf_op jit(solution)/shard_map/ppermute | solution.py:38
  447.1 9.6 %shard_map.87 = (f32[688,1024]{1,0:T(8,128)}, f32[688,1024]{1,0:T(8,128)}, f32[688,1024]{1,0:T(8,128)}) custom-call(bf16[4112,512]{1,0:T(8,128)(2,1)} %get-tuple-element.30.refs_0_, bf16[4112,512]{1,0:T(8,128)(2,1)} %collective-permute-done.64.refs_1_.refs_4_, bf16[512,1024]{1,0:T(8,128)(2,1)} %get-tuple-element.45.refs_2_, ...), custom_call_target="tpu_custom_call" | custom-call | flops 4328521728 | bytes 25165824 | tf_op jit(solution)/shard_map/pallas_call | solution.py:51
  458.4 16.7 %shard_map.88 = (f32[688,1024]{1,0:T(8,128)}, f32[688,1024]{1,0:T(8,128)}, f32[688,1024]{1,0:T(8,128)}) custom-call(bf16[1040,512]{1,0:T(8,128)(2,1)} %collective-permute-done.36.refs_0_, bf16[1024,512]{1,0:T(8,128)(2,1)} %collective-permute-done.58.refs_1_, bf16[1040,512]{1,0:T(8,128)(2,1)} %copy-done.29, ...), custom_call_target="tpu_custom_call" | custom-call | flops 8657043456 | bytes 33554432 | tf_op jit(solution)/shard_map/pallas_call | solution.py:51
  476.6 10.9 %shard_map.89 = (f32[688,1024]{1,0:T(8,128)}, f32[688,1024]{1,0:T(8,128)}, f32[688,1024]{1,0:T(8,128)}) custom-call(bf16[1040,512]{1,0:T(8,128)(2,1)} %copy-done.12, bf16[1024,512]{1,0:T(8,128)(2,1)} %copy-done.14, bf16[1040,512]{1,0:T(8,128)(2,1)} %copy-done.13, bf16[1024,512]{1,0:T(8,128)(2,1)} %copy-done.15, bf16[4,6,32,1024]{3,2,1,0:T(8,128)(2,1)} %copy-done, ...), custom_call_target="tpu_custom_call" | custom-call | flops 4328521728 | bytes 25165824 | tf_op jit(solution)/shard_map/pallas_call | solution.py:51
  (239 shorter events, 158.1 us)
Async XLA Ops:
  18.1 157.9 %collective-permute-start.22 = (bf16[1040,1024]{1,0:T(8,128)(2,1)S(1)}, bf16[1040,1024]{1,0:T(8,128)(2,1)S(1)}, u32[]{:S(2)}, u32[]{:S(2)}) collective-permute-start(bf16[1040,1024]{1,0:T(8,128)(2,1)S(1)} %pad_maximum_fusion.refs_20_.refs_5_), channel_id=1, source_target_pairs={{96,0},{97,1},{98,2},{99,3},{100,4},{101,5},{102,6},{103,7},{104,8... | collective-permute-start | bytes 6389768 | tf_op jit(solution)/shard_map/ppermute | solution.py:38
  23.0 97.8 %collective-permute-start.3 = (bf16[2,32,4096]{2,1,0:T(8,128)(2,1)S(1)}, bf16[2,32,4096]{2,1,0:T(8,128)(2,1)S(1)}, u32[]{:S(2)}, u32[]{:S(2)}) collective-permute-start(bf16[2,32,4096]{2,1,0:T(8,128)(2,1)S(1)} %pad_maximum_fusion.4.refs_0_), channel_id=1, source_target_pairs={{1,0},{2,1},{3,2},{0,3},{5,4},{6,5},{7,6},{4,7},{9,8},{10,9},{11,1... | collective-permute-start | bytes 1572872 | tf_op jit(solution)/shard_map/ppermute | solution.py:38
  25.9 96.0 %collective-permute-start.4 = (bf16[2,32,4096]{2,1,0:T(8,128)(2,1)S(1)}, bf16[2,32,4096]{2,1,0:T(8,128)(2,1)S(1)}, u32[]{:S(2)}, u32[]{:S(2)}) collective-permute-start(bf16[2,32,4096]{2,1,0:T(8,128)(2,1)S(1)} %constant_dynamic-update-slice_fusion.refs_1_), channel_id=1, source_target_pairs={{1,0},{2,1},{3,2},{0,3},{5,4},{6,5},{7,6},{4,7},{9,8},{10,9},{11,1... | collective-permute-start | bytes 1572872 | tf_op jit(solution)/shard_map/ppermute | solution.py:38
  26.4 45.5 %collective-permute-start.45 = (bf16[4,32,1024]{2,1,0:T(8,128)(2,1)S(1)}, bf16[4,32,1024]{2,1,0:T(8,128)(2,1)S(1)}, u32[]{:S(2)}, u32[]{:S(2)}) collective-permute-start(bf16[4,32,1024]{2,1,0:T(8,128)(2,1)S(1)} %pad_maximum_fusion.9), channel_id=1, source_target_pairs={{64,0},{65,1},{66,2},{67,3},{68,4},{69,5},{70,6},{71,7},{72,8},{73... | collective-permute-start | bytes 786440 | tf_op jit(solution)/shard_map/ppermute | solution.py:38
  29.1 47.2 %collective-permute-start.44 = (bf16[4,32,1024]{2,1,0:T(8,128)(2,1)S(1)}, bf16[4,32,1024]{2,1,0:T(8,128)(2,1)S(1)}, u32[]{:S(2)}, u32[]{:S(2)}) collective-permute-start(bf16[4,32,1024]{2,1,0:T(8,128)(2,1)S(1)} %pad_maximum_fusion.8), channel_id=1, source_target_pairs={{96,0},{97,1},{98,2},{99,3},{100,4},{101,5},{102,6},{103,7},{104,8... | collective-permute-start | bytes 786440 | tf_op jit(solution)/shard_map/ppermute | solution.py:38
  71.9 109.2 %collective-permute-start.19 = (bf16[1024,1024]{1,0:T(8,128)(2,1)S(1)}, bf16[1024,1024]{1,0:T(8,128)(2,1)S(1)}, u32[]{:S(2)}, u32[]{:S(2)}) collective-permute-start(bf16[1024,1024]{1,0:T(8,128)(2,1)S(1)} %pad_maximum_fusion.1.refs_16_.refs_1_), channel_id=1, source_target_pairs={{32,0},{33,1},{34,2},{35,3},{36,4},{37,5},{38,6},{39,7},{40,8},{41... | collective-permute-start | bytes 6291464 | tf_op jit(solution)/shard_map/ppermute | solution.py:38
  76.4 43.1 %collective-permute-start.43 = (bf16[4,32,1024]{2,1,0:T(8,128)(2,1)S(1)}, bf16[4,32,1024]{2,1,0:T(8,128)(2,1)S(1)}, u32[]{:S(2)}, u32[]{:S(2)}) collective-permute-start(bf16[4,32,1024]{2,1,0:T(8,128)(2,1)S(1)} %pad_maximum_fusion.8), channel_id=1, source_target_pairs={{32,0},{33,1},{34,2},{35,3},{36,4},{37,5},{38,6},{39,7},{40,8},{41... | collective-permute-start | bytes 786440 | tf_op jit(solution)/shard_map/ppermute | solution.py:38
  170.1 56.6 %collective-permute-start.21 = (bf16[1040,1024]{1,0:T(8,128)(2,1)S(1)}, bf16[1040,1024]{1,0:T(8,128)(2,1)S(1)}, u32[]{:S(2)}, u32[]{:S(2)}) collective-permute-start(bf16[1040,1024]{1,0:T(8,128)(2,1)S(1)} %pad_maximum_fusion.refs_20_.refs_5_), channel_id=1, source_target_pairs={{16,0},{17,1},{18,2},{19,3},{20,4},{21,5},{22,6},{23,7},{24,8},{25... | collective-permute-start | bytes 6389768 | tf_op jit(solution)/shard_map/ppermute | solution.py:38
  176.1 52.2 %collective-permute-start.23 = (bf16[1040,1024]{1,0:T(8,128)(2,1)S(1)}, bf16[1040,1024]{1,0:T(8,128)(2,1)S(1)}, u32[]{:S(2)}, u32[]{:S(2)}) collective-permute-start(bf16[1040,1024]{1,0:T(8,128)(2,1)S(1)} %collective-permute-done.22.refs_22_.refs_7_), channel_id=1, source_target_pairs={{16,0},{17,1},{18,2},{19,3},{20,4},{21,5},{22,6},{23,7},{24,8},{25... | collective-permute-start | bytes 6389768 | tf_op jit(solution)/shard_map/ppermute | solution.py:38
  176.6 48.3 %collective-permute-start.18 = (bf16[1024,1024]{1,0:T(8,128)(2,1)S(1)}, bf16[1024,1024]{1,0:T(8,128)(2,1)S(1)}, u32[]{:S(2)}, u32[]{:S(2)}) collective-permute-start(bf16[1024,1024]{1,0:T(8,128)(2,1)S(1)} %pad_maximum_fusion.1.refs_16_.refs_1_), channel_id=1, source_target_pairs={{16,0},{17,1},{18,2},{19,3},{20,4},{21,5},{22,6},{23,7},{24,8},{25... | collective-permute-start | bytes 6291464 | tf_op jit(solution)/shard_map/ppermute | solution.py:38
  181.2 46.5 %collective-permute-start.20 = (bf16[1024,1024]{1,0:T(8,128)(2,1)S(1)}, bf16[1024,1024]{1,0:T(8,128)(2,1)S(1)}, u32[]{:S(2)}, u32[]{:S(2)}) collective-permute-start(bf16[1024,1024]{1,0:T(8,128)(2,1)S(1)} %collective-permute-done.19.refs_18_.refs_3_), channel_id=1, source_target_pairs={{16,0},{17,1},{18,2},{19,3},{20,4},{21,5},{22,6},{23,7},{24,8},{25... | collective-permute-start | bytes 6291464 | tf_op jit(solution)/shard_map/ppermute | solution.py:38
  224.9 43.8 %collective-permute-start.54 = (bf16[1,6,32,1024]{3,2,1,0:T(8,128)(2,1)S(1)}, bf16[1,6,32,1024]{3,2,1,0:T(8,128)(2,1)S(1)}, u32[]{:S(2)}, u32[]{:S(2)}) collective-permute-start(bf16[1,6,32,1024]{3,2,1,0:T(8,128)(2,1)S(1)} %maximum_bitcast_fusion.1), channel_id=1, source_target_pairs={{3,0},{0,1},{1,2},{2,3},{7,4},{4,5},{5,6},{6,7},{11,8},{8,9},{9,10... | collective-permute-start | bytes 1179656 | tf_op jit(solution)/shard_map/ppermute | solution.py:38
  224.9 43.9 %collective-permute-start.53 = (bf16[1,6,32,1024]{3,2,1,0:T(8,128)(2,1)S(1)}, bf16[1,6,32,1024]{3,2,1,0:T(8,128)(2,1)S(1)}, u32[]{:S(2)}, u32[]{:S(2)}) collective-permute-start(bf16[1,6,32,1024]{3,2,1,0:T(8,128)(2,1)S(1)} %maximum_bitcast_fusion.1), channel_id=1, source_target_pairs={{2,0},{3,1},{0,2},{1,3},{6,4},{7,5},{4,6},{5,7},{10,8},{11,9},{8,1... | collective-permute-start | bytes 1179656 | tf_op jit(solution)/shard_map/ppermute | solution.py:38
  226.7 44.7 %collective-permute-start.52 = (bf16[1,6,32,1024]{3,2,1,0:T(8,128)(2,1)S(1)}, bf16[1,6,32,1024]{3,2,1,0:T(8,128)(2,1)S(1)}, u32[]{:S(2)}, u32[]{:S(2)}) collective-permute-start(bf16[1,6,32,1024]{3,2,1,0:T(8,128)(2,1)S(1)} %maximum_bitcast_fusion.1), channel_id=1, source_target_pairs={{1,0},{2,1},{3,2},{0,3},{5,4},{6,5},{7,6},{4,7},{9,8},{10,9},{11,1... | collective-permute-start | bytes 1179656 | tf_op jit(solution)/shard_map/ppermute | solution.py:38
  227.7 50.8 %collective-permute-start.49 = (bf16[4,6,32,1024]{3,2,1,0:T(8,128)(2,1)S(1)}, bf16[4,6,32,1024]{3,2,1,0:T(8,128)(2,1)S(1)}, u32[]{:S(2)}, u32[]{:S(2)}) collective-permute-start(bf16[4,6,32,1024]{3,2,1,0:T(8,128)(2,1)S(1)} %pad_maximum_fusion.2.refs_8_.refs_4_), channel_id=1, source_target_pairs={{1,0},{2,1},{3,2},{0,3},{5,4},{6,5},{7,6},{4,7},{9,8},{10,9},{11,1... | collective-permute-start | bytes 4718600 | tf_op jit(solution)/shard_map/ppermute | solution.py:38
  230.3 48.8 %collective-permute-start.50 = (bf16[4,6,32,1024]{3,2,1,0:T(8,128)(2,1)S(1)}, bf16[4,6,32,1024]{3,2,1,0:T(8,128)(2,1)S(1)}, u32[]{:S(2)}, u32[]{:S(2)}) collective-permute-start(bf16[4,6,32,1024]{3,2,1,0:T(8,128)(2,1)S(1)} %pad_maximum_fusion.2.refs_8_.refs_4_), channel_id=1, source_target_pairs={{3,0},{0,1},{1,2},{2,3},{7,4},{4,5},{5,6},{6,7},{11,8},{8,9},{9,10... | collective-permute-start | bytes 4718600 | tf_op jit(solution)/shard_map/ppermute | solution.py:38
  291.1 49.7 %collective-permute-start.51 = (bf16[4,6,32,1024]{3,2,1,0:T(8,128)(2,1)S(1)}, bf16[4,6,32,1024]{3,2,1,0:T(8,128)(2,1)S(1)}, u32[]{:S(2)}, u32[]{:S(2)}) collective-permute-start(bf16[4,6,32,1024]{3,2,1,0:T(8,128)(2,1)S(1)} %pad_maximum_fusion.2.refs_8_.refs_4_), channel_id=1, source_target_pairs={{2,0},{3,1},{0,2},{1,3},{6,4},{7,5},{4,6},{5,7},{10,8},{11,9},{8,1... | collective-permute-start | bytes 4718600 | tf_op jit(solution)/shard_map/ppermute | solution.py:38
  296.0 44.8 %collective-permute-start.55 = (bf16[4,6,32,1024]{3,2,1,0:T(8,128)(2,1)S(1)}, bf16[4,6,32,1024]{3,2,1,0:T(8,128)(2,1)S(1)}, u32[]{:S(2)}, u32[]{:S(2)}) collective-permute-start(bf16[4,6,32,1024]{3,2,1,0:T(8,128)(2,1)S(1)} %pad_maximum_fusion.3.refs_12_.refs_8_), channel_id=1, source_target_pairs={{4,0},{5,1},{6,2},{7,3},{8,4},{9,5},{10,6},{11,7},{12,8},{13,9},{1... | collective-permute-start | bytes 4718600 | tf_op jit(solution)/shard_map/ppermute | solution.py:38
  307.0 60.3 %collective-permute-start.57 = (bf16[4,6,32,1024]{3,2,1,0:T(8,128)(2,1)S(1)}, bf16[4,6,32,1024]{3,2,1,0:T(8,128)(2,1)}, u32[]{:S(2)}, u32[]{:S(2)}) collective-permute-start(bf16[4,6,32,1024]{3,2,1,0:T(8,128)(2,1)S(1)} %pad_maximum_fusion.3.refs_12_.refs_8_), channel_id=1, source_target_pairs={{8,0},{9,1},{10,2},{11,3},{12,4},{13,5},{14,6},{15,7},{0,8},{1,9},... | collective-permute-start | bytes 4718600 | tf_op jit(solution)/shard_map/ppermute | solution.py:38
  307.3 139.8 %collective-permute-start.64 = (bf16[4112,512]{1,0:T(8,128)(2,1)}, bf16[4112,512]{1,0:T(8,128)(2,1)}, u32[]{:S(2)}, u32[]{:S(2)}) collective-permute-start(bf16[4112,512]{1,0:T(8,128)(2,1)} %get-tuple-element.30.refs_0_), channel_id=1, source_target_pairs={{16,0},{17,1},{18,2},{19,3},{20,4},{21,5},{22,6},{23,7},{24,8},{25... | collective-permute-start | bytes 12632072 | tf_op jit(solution)/shard_map/ppermute | solution.py:38
  340.8 55.1 %collective-permute-start.38 = (bf16[1024,512]{1,0:T(8,128)(2,1)}, bf16[1024,512]{1,0:T(8,128)(2,1)}, u32[]{:S(2)}, u32[]{:S(2)}) collective-permute-start(bf16[1024,512]{1,0:T(8,128)(2,1)} %get-tuple-element.44), channel_id=1, source_target_pairs={{96,0},{97,1},{98,2},{99,3},{100,4},{101,5},{102,6},{103,7},{104,8... | collective-permute-start | bytes 3145736 | tf_op jit(solution)/shard_map/ppermute | solution.py:38
  340.9 55.2 %collective-permute-start.58 = (bf16[1024,512]{1,0:T(8,128)(2,1)}, bf16[1024,512]{1,0:T(8,128)(2,1)}, u32[]{:S(2)}, u32[]{:S(2)}) collective-permute-start(bf16[1024,512]{1,0:T(8,128)(2,1)} %get-tuple-element.44), channel_id=1, source_target_pairs={{32,0},{33,1},{34,2},{35,3},{36,4},{37,5},{38,6},{39,7},{40,8},{41... | collective-permute-start | bytes 3145736 | tf_op jit(solution)/shard_map/ppermute | solution.py:38
  396.1 49.6 %collective-permute-start.60 = (bf16[1024,512]{1,0:T(8,128)(2,1)}, bf16[1024,512]{1,0:T(8,128)(2,1)}, u32[]{:S(2)}, u32[]{:S(2)}) collective-permute-start(bf16[1024,512]{1,0:T(8,128)(2,1)} %collective-permute-done.58.refs_1_), channel_id=1, source_target_pairs={{16,0},{17,1},{18,2},{19,3},{20,4},{21,5},{22,6},{23,7},{24,8},{25... | collective-permute-start | bytes 3145736 | tf_op jit(solution)/shard_map/ppermute | solution.py:38
  403.6 42.9 %collective-permute-start.37 = (bf16[1040,512]{1,0:T(8,128)(2,1)}, bf16[1040,512]{1,0:T(8,128)(2,1)S(1)}, u32[]{:S(2)}, u32[]{:S(2)}) collective-permute-start(bf16[1040,512]{1,0:T(8,128)(2,1)} %collective-permute-done.36.refs_0_), channel_id=1, source_target_pairs={{32,0},{33,1},{34,2},{35,3},{36,4},{37,5},{38,6},{39,7},{40,8},{41... | collective-permute-start | bytes 3194888 | tf_op jit(solution)/shard_map/ppermute | solution.py:38
  (86 other events, 2424.0 us)

commit v5 on v4

--- a/solution.py
+++ b/solution.py
@@ -47,14 +47,14 @@
     return tp // 4, tp % 4
 
 
-def call(body, out_shape, scratch, flops, ins, outs, args, nbytes):
+def call(name, body, out_shape, scratch, flops, ins, outs, args, nbytes):
     return pl.pallas_call(
         body,
         out_shape=out_shape,
         in_specs=ins,
         out_specs=outs,
         scratch_shapes=scratch,
-        compiler_params=pltpu.CompilerParams(vmem_limit_bytes=LIMIT),
+        compiler_params=pltpu.CompilerParams(vmem_limit_bytes=LIMIT if name != "k_join" else 24 << 20),
         cost_estimate=pl.CostEstimate(flops=flops, bytes_accessed=nbytes, transcendentals=0),
     )(*args)
 
@@ -164,6 +164,7 @@
 def forward(xs, ds, was, wbs):
     shape = jax.ShapeDtypeStruct
     return call(
+        "k_fwd",
         forward_kernel,
         (shape((LOW, TOK), BF), shape((HIGH, TOK), BF), shape((3 * UNITS + 4 * TOK, TOK), BF),
          shape((TOK, DEPTH), BF), shape((TOK, DEPTH), BF)),
@@ -258,6 +259,7 @@
     shape = jax.ShapeDtypeStruct
     own, away = shape((4 * ROWS, HALF + TAIL), F32), shape((3, 4 * ROWS, HALF + TAIL), F32)
     return call(
+        "k_in",
         input_kernel,
         (own, own, away, away),
         [
@@ -290,7 +292,7 @@
 
 def joined(own_a, own_b, got):
     out = jax.ShapeDtypeStruct((ROWS, HALF), F32)
-    kept = call(join_kernel, (out,) * 8, [], 1 << 30, [VMEM] * 8, (VMEM,) * 8, (own_a, own_b, *got), 12 << 20)
+    kept = call("k_join", join_kernel, (out,) * 8, [], 1 << 30, [VMEM] * 8, (VMEM,) * 8, (own_a, own_b, *got), 12 << 20)
     return kept[:4], kept[4:]
 
 
@@ -362,7 +364,7 @@
             add(refs[4 * kind + i].at[j, pl.ds(first_group, count)], buf.at[:, a * 4 + b])
 
 
-def weight_sums(groups, columns, arrays, base):
+def weight_sums(name, groups, columns, arrays, base):
     ins, acts = [], []
     for pieces in groups:
         row, marks = 0, []
@@ -377,6 +379,7 @@
     col = (2, n, TOK, DEPTH) if columns is near_columns else (2, n, 16, ROWS, DEPTH)
     out = jax.ShapeDtypeStruct((UNITS, DEPTH), F32)
     return call(
+        name,
         functools.partial(weight_kernel, acts, n_acts, columns, base is not None, len(ins)),
         (out,) * 3,
         [
@@ -466,12 +469,12 @@
         return [(low, LOW), (high, HIGH)]
 
     sums = weight_sums(
-        [[(own, full)], [(side, full)]], near_columns, (x_cols, d_cols, side), None)
+        "k_near", [[(own, full)], [(side, full)]], near_columns, (x_cols, d_cols, side), None)
     sums = weight_sums(
-        [halves(aml, amh), halves(sml, smh), halves(apl, aph), halves(spl, sph)],
+        "k_mid", [halves(aml, amh), halves(sml, smh), halves(apl, aph), halves(spl, sph)],
         functools.partial(plane_columns, 0, 4), (*xcs, *dcs), sums)
     sums = weight_sums(
-        [halves(oa, ob), halves(soa, sob)], functools.partial(plane_columns, 4, 2), (*xcs, *dcs), sums)
+        "k_far", [halves(oa, ob), halves(soa, sob)], functools.partial(plane_columns, 4, 2), (*xcs, *dcs), sums)
     return grad_inputs, sums[0].T, sums[1].T, sums[2]
 
 

time: 490 us -> 492 us (level)
  waiting for transfers between devices: 260 us -> 278 us
  other arithmetic: 15.9 us -> 6.78 us
    ppermute x65, waiting for transfers between devices: 260 us -> 278 us  [moved(): return lax.ppermute(array, AXES, pairs)]
    convert_element_type x6, other arithmetic: 6.44 us -> 0.45 us  [block(): fa, fb = joined(own_a, own_b, [g.astype(F32) for g in got])]
  transfers between devices with their start and end apart: 65 -> 65, of which waited for: 28 -> 28; matrix products, arithmetic and copies ran while one was open for 3% -> 1% of each run, Pallas kernels for 13% -> 12%
where the time goes in v5:
time: 492 us; the launch traced here: 491 us
  waiting for transfers between devices  278 us (57%)
  starting transfers between devices  124 us (25%)
  Pallas kernels  71.7 us (15%)
  local copies, waits for them, and re-layouts  9.69 us (2%)
  other arithmetic  6.78 us (1%)
    ppermute x65, waiting for transfers between devices, moved(): return lax.ppermute(array, AXES, pairs)  278 us
    ppermute x65, starting transfers between devices, moved(): return lax.ppermute(array, AXES, pairs)  124 us
    pallas_call x6, Pallas kernels, call(): pl.pallas_call(body, out_shape=out_shape, in_specs=ins, out_specs=outs, s...  71.7 us
  transfers between devices with their start and end apart: 65, of which 28 were waited for; matrix products, arithmetic and copies ran while one was open for 1% of the time, Pallas kernels for 12%

profile of v5, /device:TPU:1, one launch (start us, length us, event | category | flops | bytes accessed | tf_op | source)
XLA Modules:
  0.0 491.4 jit_solution(3731761368247839661)
XLA Ops:
  29.5 42.4 %collective-permute-done.45 = bf16[4,32,1024]{2,1,0:T(8,128)(2,1)S(1)} collective-permute-done((bf16[4,32,1024]{2,1,0:T(8,128)(2,1)S(1)}, bf16[4,32,1024]{2,1,0:T(8,128)(2,1)S(1)}, u32[]{:S(2)}, u32[]{:S(2)}) %collective-permute-start.45) | collective-permute-done | bytes 262176 | tf_op jit(solution)/shard_map/ppermute | solution.py:38
  77.9 41.7 %collective-permute-done.43 = bf16[4,32,1024]{2,1,0:T(8,128)(2,1)S(1)} collective-permute-done((bf16[4,32,1024]{2,1,0:T(8,128)(2,1)S(1)}, bf16[4,32,1024]{2,1,0:T(8,128)(2,1)S(1)}, u32[]{:S(2)}, u32[]{:S(2)}) %collective-permute-start.43) | collective-permute-done | bytes 262176 | tf_op jit(solution)/shard_map/ppermute | solution.py:38
  130.3 9.1 %collective-permute-done.6.refs_5_ = bf16[2,32,4096]{2,1,0:T(8,128)(2,1)S(1)} collective-permute-done((bf16[2,32,4096]{2,1,0:T(8,128)(2,1)S(1)}, bf16[2,32,4096]{2,1,0:T(8,128)(2,1)S(1)}, u32[]{:S(2)}, u32[]{:S(2)}) %collective-permute-start.6) | collective-permute-done | bytes 524320 | tf_op jit(solution)/shard_map/ppermute | solution.py:38
  143.8 6.0 %collective-permute-done.13.refs_11_ = bf16[2,32,4096]{2,1,0:T(8,128)(2,1)} collective-permute-done((bf16[2,32,4096]{2,1,0:T(8,128)(2,1)S(1)}, bf16[2,32,4096]{2,1,0:T(8,128)(2,1)}, u32[]{:S(2)}, u32[]{:S(2)}) %collective-permute-start.13) | collective-permute-done | bytes 524320 | tf_op jit(solution)/shard_map/ppermute | solution.py:38
  158.9 11.2 %collective-permute-done.48 = bf16[1,6,32,1024]{3,2,1,0:T(8,128)(2,1)S(1)} collective-permute-done((bf16[1,6,32,1024]{3,2,1,0:T(8,128)(2,1)S(1)}, bf16[1,6,32,1024]{3,2,1,0:T(8,128)(2,1)S(1)}, u32[]{:S(2)}, u32[]{:S(2)}) %collective-permute-start.48) | collective-permute-done | bytes 393248 | tf_op jit(solution)/shard_map/ppermute | solution.py:38
  170.1 6.0 %collective-permute-start.21 = (bf16[1040,1024]{1,0:T(8,128)(2,1)S(1)}, bf16[1040,1024]{1,0:T(8,128)(2,1)S(1)}, u32[]{:S(2)}, u32[]{:S(2)}) collective-permute-start(bf16[1040,1024]{1,0:T(8,128)(2,1)S(1)} %pad_maximum_fusion.refs_20_.refs_5_), channel_id=1, source_target_pairs={{16,0},{17,1},{18,2},{19,3},{20,4},{21,5},{22,6},{23,7},{24,8},{25... | collective-permute-start | bytes 6389768 | tf_op jit(solution)/shard_map/ppermute | solution.py:38
  185.6 9.6 %collective-permute-done.8.refs_7_ = bf16[2,32,4096]{2,1,0:T(8,128)(2,1)S(1)} collective-permute-done((bf16[2,32,4096]{2,1,0:T(8,128)(2,1)S(1)}, bf16[2,32,4096]{2,1,0:T(8,128)(2,1)S(1)}, u32[]{:S(2)}, u32[]{:S(2)}) %collective-permute-start.8) | collective-permute-done | bytes 524320 | tf_op jit(solution)/shard_map/ppermute | solution.py:38
  195.1 7.8 %collective-permute-start.16 = (bf16[2,32,4096]{2,1,0:T(8,128)(2,1)S(1)}, bf16[2,32,4096]{2,1,0:T(8,128)(2,1)S(1)}, u32[]{:S(2)}, u32[]{:S(2)}) collective-permute-start(bf16[2,32,4096]{2,1,0:T(8,128)(2,1)S(1)} %collective-permute-done.12.refs_10_), channel_id=1, source_target_pairs={{4,0},{5,1},{6,2},{7,3},{8,4},{9,5},{10,6},{11,7},{12,8},{13,9},{1... | collective-permute-start | bytes 1572872 | tf_op jit(solution)/shard_map/ppermute | solution.py:38
  203.0 9.2 %collective-permute-done.16.refs_14_ = bf16[2,32,4096]{2,1,0:T(8,128)(2,1)S(1)} collective-permute-done((bf16[2,32,4096]{2,1,0:T(8,128)(2,1)S(1)}, bf16[2,32,4096]{2,1,0:T(8,128)(2,1)S(1)}, u32[]{:S(2)}, u32[]{:S(2)}) %collective-permute-start.16) | collective-permute-done | bytes 524320 | tf_op jit(solution)/shard_map/ppermute | solution.py:38
  213.6 11.3 %collective-permute-done.17.refs_15_ = bf16[2,32,4096]{2,1,0:T(8,128)(2,1)S(1)} collective-permute-done((bf16[2,32,4096]{2,1,0:T(8,128)(2,1)S(1)}, bf16[2,32,4096]{2,1,0:T(8,128)(2,1)S(1)}, u32[]{:S(2)}, u32[]{:S(2)}) %collective-permute-start.17) | collective-permute-done | bytes 524320 | tf_op jit(solution)/shard_map/ppermute | solution.py:38
  231.6 20.0 %shard_map.84 = (bf16[1040,512]{1,0:T(8,128)(2,1)}, bf16[1024,512]{1,0:T(8,128)(2,1)}, bf16[4112,512]{1,0:T(8,128)(2,1)}, bf16[512,1024]{1,0:T(8,128)(2,1)}, bf16[512,1024]{1,0:T(8,128)(2,1)}) custom-call(bf16[2,32,4096]{2,1,0:T(8,128)(2,1)} %copy-done.19, bf16[2,32,4096]{2,1,0:T(8,128)(2,1)} %copy-done.22, bf16[2,32,4096]{2,1,0:T(8,128)(2,1)} %copy-done.32, ...), custom_call_target="tpu_custom_call" | custom-call | flops 8657043456 | bytes 35651584 | tf_op jit(solution)/shard_map/pallas_call | solution.py:51
  251.5 13.8 %shard_map.85 = (f32[128,2176]{1,0:T(8,128)}, f32[128,2176]{1,0:T(8,128)}, f32[3,128,2176]{2,1,0:T(8,128)}, f32[3,128,2176]{2,1,0:T(8,128)}) custom-call(bf16[4112,512]{1,0:T(8,128)(2,1)} %get-tuple-element.30.refs_0_, bf16[1024,1024]{1,0:T(8,128)(2,1)} %copy-done.6, bf16[1024,1024]{1,0:T(8,128)(2,1)} %copy-done.27, bf16[1024,1024]{1,0:T(8,128)(2,1)} %copy-done.26, ...), custom_call_target="tpu_custom_call" | custom-call | flops 5771362304 | bytes 23068672 | tf_op jit(solution)/shard_map/pallas_call | solution.py:51
  271.9 6.6 %collective-permute-done.49.refs_9_.refs_5_ = bf16[4,6,32,1024]{3,2,1,0:T(8,128)(2,1)S(1)} collective-permute-done((bf16[4,6,32,1024]{3,2,1,0:T(8,128)(2,1)S(1)}, bf16[4,6,32,1024]{3,2,1,0:T(8,128)(2,1)S(1)}, u32[]{:S(2)}, u32[]{:S(2)}) %collective-permute-start.49) | collective-permute-done | bytes 1572896 | tf_op jit(solution)/shard_map/ppermute | solution.py:38
  283.0 8.1 %collective-permute-done.25 = f16[128,2176]{1,0:T(8,128)(2,1)S(1)} collective-permute-done((f16[128,2176]{1,0:T(8,128)(2,1)S(1)}, f16[128,2176]{1,0:T(8,128)(2,1)S(1)}, u32[]{:S(2)}, u32[]{:S(2)}) %collective-permute-start.25) | collective-permute-done | bytes 557088 | tf_op jit(solution)/shard_map/ppermute | solution.py:38
  299.5 7.5 %collective-permute-done.28 = f16[128,2176]{1,0:T(8,128)(2,1)S(1)} collective-permute-done((f16[128,2176]{1,0:T(8,128)(2,1)S(1)}, f16[128,2176]{1,0:T(8,128)(2,1)S(1)}, u32[]{:S(2)}, u32[]{:S(2)}) %collective-permute-start.28) | collective-permute-done | bytes 557088 | tf_op jit(solution)/shard_map/ppermute | solution.py:38
  315.1 25.6 %collective-permute-done.51.refs_11_.refs_7_ = bf16[4,6,32,1024]{3,2,1,0:T(8,128)(2,1)S(1)} collective-permute-done((bf16[4,6,32,1024]{3,2,1,0:T(8,128)(2,1)S(1)}, bf16[4,6,32,1024]{3,2,1,0:T(8,128)(2,1)S(1)}, u32[]{:S(2)}, u32[]{:S(2)}) %collective-permute-start.51) | collective-permute-done | bytes 1572896 | tf_op jit(solution)/shard_map/ppermute | solution.py:38
  340.7 25.4 %collective-permute-done.55.refs_13_.refs_9_ = bf16[4,6,32,1024]{3,2,1,0:T(8,128)(2,1)S(1)} collective-permute-done((bf16[4,6,32,1024]{3,2,1,0:T(8,128)(2,1)S(1)}, bf16[4,6,32,1024]{3,2,1,0:T(8,128)(2,1)S(1)}, u32[]{:S(2)}, u32[]{:S(2)}) %collective-permute-start.55) | collective-permute-done | bytes 1572896 | tf_op jit(solution)/shard_map/ppermute | solution.py:38
  386.5 8.5 %collective-permute-start.30 = (f32[32,2048]{1,0:T(8,128)S(1)}, f32[32,2048]{1,0:T(8,128)S(1)}, u32[]{:S(2)}, u32[]{:S(2)}) collective-permute-start(f32[32,2048]{1,0:T(8,128)S(1)} %get-tuple-element.36), channel_id=1, source_target_pairs={{12,0},{13,1},{14,2},{15,3},{0,4},{1,5},{2,6},{3,7},{4,8},{5,9},{6... | collective-permute-start | bytes 786440 | tf_op jit(solution)/shard_map/ppermute | solution.py:38
  413.3 9.7 %collective-permute-done.61.refs_4_ = bf16[1040,512]{1,0:T(8,128)(2,1)} collective-permute-done((bf16[1040,512]{1,0:T(8,128)(2,1)}, bf16[1040,512]{1,0:T(8,128)(2,1)}, u32[]{:S(2)}, u32[]{:S(2)}) %collective-permute-start.61) | collective-permute-done | bytes 1064992 | tf_op jit(solution)/shard_map/ppermute | solution.py:38
  423.0 8.8 %collective-permute-start.63 = (bf16[1024,512]{1,0:T(8,128)(2,1)}, bf16[1024,512]{1,0:T(8,128)(2,1)}, u32[]{:S(2)}, u32[]{:S(2)}) collective-permute-start(bf16[1024,512]{1,0:T(8,128)(2,1)} %collective-permute-done.38.refs_5_), channel_id=1, source_target_pairs={{16,0},{17,1},{18,2},{19,3},{20,4},{21,5},{22,6},{23,7},{24,8},{25... | collective-permute-start | bytes 3145736 | tf_op jit(solution)/shard_map/ppermute | solution.py:38
  431.7 13.6 %collective-permute-done.39.refs_1_ = bf16[1024,512]{1,0:T(8,128)(2,1)S(1)} collective-permute-done((bf16[1024,512]{1,0:T(8,128)(2,1)}, bf16[1024,512]{1,0:T(8,128)(2,1)S(1)}, u32[]{:S(2)}, u32[]{:S(2)}) %collective-permute-start.39) | collective-permute-done | bytes 1048608 | tf_op jit(solution)/shard_map/ppermute | solution.py:38
  451.3 9.6 %shard_map.87 = (f32[688,1024]{1,0:T(8,128)}, f32[688,1024]{1,0:T(8,128)}, f32[688,1024]{1,0:T(8,128)}) custom-call(bf16[4112,512]{1,0:T(8,128)(2,1)} %get-tuple-element.30.refs_0_, bf16[4112,512]{1,0:T(8,128)(2,1)} %collective-permute-done.64.refs_1_.refs_4_, bf16[512,1024]{1,0:T(8,128)(2,1)} %get-tuple-element.45.refs_2_, ...), custom_call_target="tpu_custom_call" | custom-call | flops 4328521728 | bytes 25165824 | tf_op jit(solution)/shard_map/pallas_call | solution.py:51
  462.3 16.7 %shard_map.88 = (f32[688,1024]{1,0:T(8,128)}, f32[688,1024]{1,0:T(8,128)}, f32[688,1024]{1,0:T(8,128)}) custom-call(bf16[1040,512]{1,0:T(8,128)(2,1)} %collective-permute-done.36.refs_0_, bf16[1024,512]{1,0:T(8,128)(2,1)} %collective-permute-done.58.refs_1_, bf16[1040,512]{1,0:T(8,128)(2,1)} %copy-done.29, ...), custom_call_target="tpu_custom_call" | custom-call | flops 8657043456 | bytes 33554432 | tf_op jit(solution)/shard_map/pallas_call | solution.py:51
  480.3 10.9 %shard_map.89 = (f32[688,1024]{1,0:T(8,128)}, f32[688,1024]{1,0:T(8,128)}, f32[688,1024]{1,0:T(8,128)}) custom-call(bf16[1040,512]{1,0:T(8,128)(2,1)} %copy-done.15, bf16[1024,512]{1,0:T(8,128)(2,1)} %copy-done.17, bf16[1040,512]{1,0:T(8,128)(2,1)} %copy-done.16, bf16[1024,512]{1,0:T(8,128)(2,1)} %copy-done.18, bf16[4,6,32,1024]{3,2,1,0:T(8,128)(2,1)} %copy-done.2, ...), custom_call_target="tpu_custom_call" | custom-call | flops 4328521728 | bytes 25165824 | tf_op jit(solution)/shard_map/pallas_call | solution.py:51
  (239 shorter events, 150.9 us)
Async XLA Ops:
  18.1 157.9 %collective-permute-start.22 = (bf16[1040,1024]{1,0:T(8,128)(2,1)S(1)}, bf16[1040,1024]{1,0:T(8,128)(2,1)S(1)}, u32[]{:S(2)}, u32[]{:S(2)}) collective-permute-start(bf16[1040,1024]{1,0:T(8,128)(2,1)S(1)} %pad_maximum_fusion.refs_20_.refs_5_), channel_id=1, source_target_pairs={{96,0},{97,1},{98,2},{99,3},{100,4},{101,5},{102,6},{103,7},{104,8... | collective-permute-start | bytes 6389768 | tf_op jit(solution)/shard_map/ppermute | solution.py:38
  23.0 97.8 %collective-permute-start.3 = (bf16[2,32,4096]{2,1,0:T(8,128)(2,1)S(1)}, bf16[2,32,4096]{2,1,0:T(8,128)(2,1)S(1)}, u32[]{:S(2)}, u32[]{:S(2)}) collective-permute-start(bf16[2,32,4096]{2,1,0:T(8,128)(2,1)S(1)} %pad_maximum_fusion.4.refs_0_), channel_id=1, source_target_pairs={{1,0},{2,1},{3,2},{0,3},{5,4},{6,5},{7,6},{4,7},{9,8},{10,9},{11,1... | collective-permute-start | bytes 1572872 | tf_op jit(solution)/shard_map/ppermute | solution.py:38
  25.9 96.0 %collective-permute-start.4 = (bf16[2,32,4096]{2,1,0:T(8,128)(2,1)S(1)}, bf16[2,32,4096]{2,1,0:T(8,128)(2,1)S(1)}, u32[]{:S(2)}, u32[]{:S(2)}) collective-permute-start(bf16[2,32,4096]{2,1,0:T(8,128)(2,1)S(1)} %constant_dynamic-update-slice_fusion.refs_1_), channel_id=1, source_target_pairs={{1,0},{2,1},{3,2},{0,3},{5,4},{6,5},{7,6},{4,7},{9,8},{10,9},{11,1... | collective-permute-start | bytes 1572872 | tf_op jit(solution)/shard_map/ppermute | solution.py:38
  26.4 45.5 %collective-permute-start.45 = (bf16[4,32,1024]{2,1,0:T(8,128)(2,1)S(1)}, bf16[4,32,1024]{2,1,0:T(8,128)(2,1)S(1)}, u32[]{:S(2)}, u32[]{:S(2)}) collective-permute-start(bf16[4,32,1024]{2,1,0:T(8,128)(2,1)S(1)} %pad_maximum_fusion.9), channel_id=1, source_target_pairs={{64,0},{65,1},{66,2},{67,3},{68,4},{69,5},{70,6},{71,7},{72,8},{73... | collective-permute-start | bytes 786440 | tf_op jit(solution)/shard_map/ppermute | solution.py:38
  29.1 47.2 %collective-permute-start.44 = (bf16[4,32,1024]{2,1,0:T(8,128)(2,1)S(1)}, bf16[4,32,1024]{2,1,0:T(8,128)(2,1)S(1)}, u32[]{:S(2)}, u32[]{:S(2)}) collective-permute-start(bf16[4,32,1024]{2,1,0:T(8,128)(2,1)S(1)} %pad_maximum_fusion.8), channel_id=1, source_target_pairs={{96,0},{97,1},{98,2},{99,3},{100,4},{101,5},{102,6},{103,7},{104,8... | collective-permute-start | bytes 786440 | tf_op jit(solution)/shard_map/ppermute | solution.py:38
  71.9 109.2 %collective-permute-start.19 = (bf16[1024,1024]{1,0:T(8,128)(2,1)S(1)}, bf16[1024,1024]{1,0:T(8,128)(2,1)S(1)}, u32[]{:S(2)}, u32[]{:S(2)}) collective-permute-start(bf16[1024,1024]{1,0:T(8,128)(2,1)S(1)} %pad_maximum_fusion.1.refs_16_.refs_1_), channel_id=1, source_target_pairs={{32,0},{33,1},{34,2},{35,3},{36,4},{37,5},{38,6},{39,7},{40,8},{41... | collective-permute-start | bytes 6291464 | tf_op jit(solution)/shard_map/ppermute | solution.py:38
  76.4 43.1 %collective-permute-start.43 = (bf16[4,32,1024]{2,1,0:T(8,128)(2,1)S(1)}, bf16[4,32,1024]{2,1,0:T(8,128)(2,1)S(1)}, u32[]{:S(2)}, u32[]{:S(2)}) collective-permute-start(bf16[4,32,1024]{2,1,0:T(8,128)(2,1)S(1)} %pad_maximum_fusion.8), channel_id=1, source_target_pairs={{32,0},{33,1},{34,2},{35,3},{36,4},{37,5},{38,6},{39,7},{40,8},{41... | collective-permute-start | bytes 786440 | tf_op jit(solution)/shard_map/ppermute | solution.py:38
  170.1 56.6 %collective-permute-start.21 = (bf16[1040,1024]{1,0:T(8,128)(2,1)S(1)}, bf16[1040,1024]{1,0:T(8,128)(2,1)S(1)}, u32[]{:S(2)}, u32[]{:S(2)}) collective-permute-start(bf16[1040,1024]{1,0:T(8,128)(2,1)S(1)} %pad_maximum_fusion.refs_20_.refs_5_), channel_id=1, source_target_pairs={{16,0},{17,1},{18,2},{19,3},{20,4},{21,5},{22,6},{23,7},{24,8},{25... | collective-permute-start | bytes 6389768 | tf_op jit(solution)/shard_map/ppermute | solution.py:38
  176.1 52.2 %collective-permute-start.23 = (bf16[1040,1024]{1,0:T(8,128)(2,1)S(1)}, bf16[1040,1024]{1,0:T(8,128)(2,1)S(1)}, u32[]{:S(2)}, u32[]{:S(2)}) collective-permute-start(bf16[1040,1024]{1,0:T(8,128)(2,1)S(1)} %collective-permute-done.22.refs_22_.refs_7_), channel_id=1, source_target_pairs={{16,0},{17,1},{18,2},{19,3},{20,4},{21,5},{22,6},{23,7},{24,8},{25... | collective-permute-start | bytes 6389768 | tf_op jit(solution)/shard_map/ppermute | solution.py:38
  176.6 48.3 %collective-permute-start.18 = (bf16[1024,1024]{1,0:T(8,128)(2,1)S(1)}, bf16[1024,1024]{1,0:T(8,128)(2,1)S(1)}, u32[]{:S(2)}, u32[]{:S(2)}) collective-permute-start(bf16[1024,1024]{1,0:T(8,128)(2,1)S(1)} %pad_maximum_fusion.1.refs_16_.refs_1_), channel_id=1, source_target_pairs={{16,0},{17,1},{18,2},{19,3},{20,4},{21,5},{22,6},{23,7},{24,8},{25... | collective-permute-start | bytes 6291464 | tf_op jit(solution)/shard_map/ppermute | solution.py:38
  181.2 46.5 %collective-permute-start.20 = (bf16[1024,1024]{1,0:T(8,128)(2,1)S(1)}, bf16[1024,1024]{1,0:T(8,128)(2,1)S(1)}, u32[]{:S(2)}, u32[]{:S(2)}) collective-permute-start(bf16[1024,1024]{1,0:T(8,128)(2,1)S(1)} %collective-permute-done.19.refs_18_.refs_3_), channel_id=1, source_target_pairs={{16,0},{17,1},{18,2},{19,3},{20,4},{21,5},{22,6},{23,7},{24,8},{25... | collective-permute-start | bytes 6291464 | tf_op jit(solution)/shard_map/ppermute | solution.py:38
  224.9 43.9 %collective-permute-start.54 = (bf16[1,6,32,1024]{3,2,1,0:T(8,128)(2,1)S(1)}, bf16[1,6,32,1024]{3,2,1,0:T(8,128)(2,1)S(1)}, u32[]{:S(2)}, u32[]{:S(2)}) collective-permute-start(bf16[1,6,32,1024]{3,2,1,0:T(8,128)(2,1)S(1)} %maximum_bitcast_fusion.1), channel_id=1, source_target_pairs={{3,0},{0,1},{1,2},{2,3},{7,4},{4,5},{5,6},{6,7},{11,8},{8,9},{9,10... | collective-permute-start | bytes 1179656 | tf_op jit(solution)/shard_map/ppermute | solution.py:38
  224.9 43.9 %collective-permute-start.53 = (bf16[1,6,32,1024]{3,2,1,0:T(8,128)(2,1)S(1)}, bf16[1,6,32,1024]{3,2,1,0:T(8,128)(2,1)S(1)}, u32[]{:S(2)}, u32[]{:S(2)}) collective-permute-start(bf16[1,6,32,1024]{3,2,1,0:T(8,128)(2,1)S(1)} %maximum_bitcast_fusion.1), channel_id=1, source_target_pairs={{2,0},{3,1},{0,2},{1,3},{6,4},{7,5},{4,6},{5,7},{10,8},{11,9},{8,1... | collective-permute-start | bytes 1179656 | tf_op jit(solution)/shard_map/ppermute | solution.py:38
  226.7 44.8 %collective-permute-start.52 = (bf16[1,6,32,1024]{3,2,1,0:T(8,128)(2,1)S(1)}, bf16[1,6,32,1024]{3,2,1,0:T(8,128)(2,1)S(1)}, u32[]{:S(2)}, u32[]{:S(2)}) collective-permute-start(bf16[1,6,32,1024]{3,2,1,0:T(8,128)(2,1)S(1)} %maximum_bitcast_fusion.1), channel_id=1, source_target_pairs={{1,0},{2,1},{3,2},{0,3},{5,4},{6,5},{7,6},{4,7},{9,8},{10,9},{11,1... | collective-permute-start | bytes 1179656 | tf_op jit(solution)/shard_map/ppermute | solution.py:38
  227.7 50.8 %collective-permute-start.49 = (bf16[4,6,32,1024]{3,2,1,0:T(8,128)(2,1)S(1)}, bf16[4,6,32,1024]{3,2,1,0:T(8,128)(2,1)S(1)}, u32[]{:S(2)}, u32[]{:S(2)}) collective-permute-start(bf16[4,6,32,1024]{3,2,1,0:T(8,128)(2,1)S(1)} %pad_maximum_fusion.2.refs_8_.refs_4_), channel_id=1, source_target_pairs={{1,0},{2,1},{3,2},{0,3},{5,4},{6,5},{7,6},{4,7},{9,8},{10,9},{11,1... | collective-permute-start | bytes 4718600 | tf_op jit(solution)/shard_map/ppermute | solution.py:38
  230.4 48.7 %collective-permute-start.50 = (bf16[4,6,32,1024]{3,2,1,0:T(8,128)(2,1)S(1)}, bf16[4,6,32,1024]{3,2,1,0:T(8,128)(2,1)S(1)}, u32[]{:S(2)}, u32[]{:S(2)}) collective-permute-start(bf16[4,6,32,1024]{3,2,1,0:T(8,128)(2,1)S(1)} %pad_maximum_fusion.2.refs_8_.refs_4_), channel_id=1, source_target_pairs={{3,0},{0,1},{1,2},{2,3},{7,4},{4,5},{5,6},{6,7},{11,8},{8,9},{9,10... | collective-permute-start | bytes 4718600 | tf_op jit(solution)/shard_map/ppermute | solution.py:38
  291.2 49.5 %collective-permute-start.51 = (bf16[4,6,32,1024]{3,2,1,0:T(8,128)(2,1)S(1)}, bf16[4,6,32,1024]{3,2,1,0:T(8,128)(2,1)S(1)}, u32[]{:S(2)}, u32[]{:S(2)}) collective-permute-start(bf16[4,6,32,1024]{3,2,1,0:T(8,128)(2,1)S(1)} %pad_maximum_fusion.2.refs_8_.refs_4_), channel_id=1, source_target_pairs={{2,0},{3,1},{0,2},{1,3},{6,4},{7,5},{4,6},{5,7},{10,8},{11,9},{8,1... | collective-permute-start | bytes 4718600 | tf_op jit(solution)/shard_map/ppermute | solution.py:38
  296.1 70.1 %collective-permute-start.55 = (bf16[4,6,32,1024]{3,2,1,0:T(8,128)(2,1)S(1)}, bf16[4,6,32,1024]{3,2,1,0:T(8,128)(2,1)S(1)}, u32[]{:S(2)}, u32[]{:S(2)}) collective-permute-start(bf16[4,6,32,1024]{3,2,1,0:T(8,128)(2,1)S(1)} %pad_maximum_fusion.3.refs_12_.refs_8_), channel_id=1, source_target_pairs={{4,0},{5,1},{6,2},{7,3},{8,4},{9,5},{10,6},{11,7},{12,8},{13,9},{1... | collective-permute-start | bytes 4718600 | tf_op jit(solution)/shard_map/ppermute | solution.py:38
  299.5 66.7 %collective-permute-start.56 = (bf16[4,6,32,1024]{3,2,1,0:T(8,128)(2,1)S(1)}, bf16[4,6,32,1024]{3,2,1,0:T(8,128)(2,1)S(1)}, u32[]{:S(2)}, u32[]{:S(2)}) collective-permute-start(bf16[4,6,32,1024]{3,2,1,0:T(8,128)(2,1)S(1)} %pad_maximum_fusion.3.refs_12_.refs_8_), channel_id=1, source_target_pairs={{12,0},{13,1},{14,2},{15,3},{0,4},{1,5},{2,6},{3,7},{4,8},{5,9},{6... | collective-permute-start | bytes 4718600 | tf_op jit(solution)/shard_map/ppermute | solution.py:38
  307.0 61.8 %collective-permute-start.57 = (bf16[4,6,32,1024]{3,2,1,0:T(8,128)(2,1)S(1)}, bf16[4,6,32,1024]{3,2,1,0:T(8,128)(2,1)S(1)}, u32[]{:S(2)}, u32[]{:S(2)}) collective-permute-start(bf16[4,6,32,1024]{3,2,1,0:T(8,128)(2,1)S(1)} %pad_maximum_fusion.3.refs_12_.refs_8_), channel_id=1, source_target_pairs={{8,0},{9,1},{10,2},{11,3},{12,4},{13,5},{14,6},{15,7},{0,8},{1,9},... | collective-permute-start | bytes 4718600 | tf_op jit(solution)/shard_map/ppermute | solution.py:38
  307.3 144.0 %collective-permute-start.64 = (bf16[4112,512]{1,0:T(8,128)(2,1)}, bf16[4112,512]{1,0:T(8,128)(2,1)}, u32[]{:S(2)}, u32[]{:S(2)}) collective-permute-start(bf16[4112,512]{1,0:T(8,128)(2,1)} %get-tuple-element.30.refs_0_), channel_id=1, source_target_pairs={{16,0},{17,1},{18,2},{19,3},{20,4},{21,5},{22,6},{23,7},{24,8},{25... | collective-permute-start | bytes 12632072 | tf_op jit(solution)/shard_map/ppermute | solution.py:38
  400.1 45.2 %collective-permute-start.39 = (bf16[1024,512]{1,0:T(8,128)(2,1)}, bf16[1024,512]{1,0:T(8,128)(2,1)S(1)}, u32[]{:S(2)}, u32[]{:S(2)}) collective-permute-start(bf16[1024,512]{1,0:T(8,128)(2,1)} %collective-permute-done.38.refs_5_), channel_id=1, source_target_pairs={{96,0},{97,1},{98,2},{99,3},{100,4},{101,5},{102,6},{103,7},{104,8... | collective-permute-start | bytes 3145736 | tf_op jit(solution)/shard_map/ppermute | solution.py:38
  402.0 47.9 %collective-permute-start.60 = (bf16[1024,512]{1,0:T(8,128)(2,1)}, bf16[1024,512]{1,0:T(8,128)(2,1)}, u32[]{:S(2)}, u32[]{:S(2)}) collective-permute-start(bf16[1024,512]{1,0:T(8,128)(2,1)} %collective-permute-done.58.refs_1_), channel_id=1, source_target_pairs={{16,0},{17,1},{18,2},{19,3},{20,4},{21,5},{22,6},{23,7},{24,8},{25... | collective-permute-start | bytes 3145736 | tf_op jit(solution)/shard_map/ppermute | solution.py:38
  409.8 41.0 %collective-permute-start.37 = (bf16[1040,512]{1,0:T(8,128)(2,1)}, bf16[1040,512]{1,0:T(8,128)(2,1)S(1)}, u32[]{:S(2)}, u32[]{:S(2)}) collective-permute-start(bf16[1040,512]{1,0:T(8,128)(2,1)} %collective-permute-done.36.refs_0_), channel_id=1, source_target_pairs={{32,0},{33,1},{34,2},{35,3},{36,4},{37,5},{38,6},{39,7},{40,8},{41... | collective-permute-start | bytes 3194888 | tf_op jit(solution)/shard_map/ppermute | solution.py:38
  (86 other events, 2526.6 us)
